TPU v7x, 256 devices: a whole 4x4x8 slice. The times are simulated.
256 devices in a mesh: sp: 64 (over z, x, core), tp: 4 (over y).
Axes of the slice: x: 4, y: 4, z: 8, core: 2. Of those that a mesh axis runs over, the one named last changes fastest.
Arguments:
- query_rows: bfloat16 [16384, 2048], P('sp', 'tp'), may hold values from -6 to 6
- key_rows: bfloat16 [16384, 2048], P('sp', 'tp'), may hold values from -6 to 6
- value_rows: bfloat16 [16384, 2048], P('sp', 'tp'), may hold values from -6 to 6
- gate_rows: bfloat16 [16384, 2048], P('sp', 'tp'), may hold values from -6 to 6
- log_decay: float32 [16384, 16], P('sp', 'tp'), may hold values from -1 to 0
- head_gain: float32 [2048], P('tp'), may hold values from 0.1 to 1.9
- out_weight: bfloat16 [2048, 2048], P('tp'), may hold values from -0.125 to 0.125
- residual: bfloat16 [16384, 2048], P(('sp', 'tp')), may hold values from -6 to 6
- ffn_gain: float32 [2048], replicated, may hold values from 0.1 to 1.9
- gate_weight: bfloat16 [64, 2048, 2048], P('sp', None, 'tp'), may hold values from -0.375 to 0.375
- up_weight: bfloat16 [64, 2048, 2048], P('sp', None, 'tp'), may hold values from -0.375 to 0.375
- down_weight: bfloat16 [64, 2048, 2048], P('sp', 'tp'), may hold values from -0.01953125 to 0.01953125
- routes: int32 [16384, 4], P('sp'), may hold values from 0 to 63, all different within a row; in each aligned block of 64 rows (0 to 63, 64 to 127, ...) at most 6 rows name the same one
- route_weights: float32 [16384, 4], P(('sp', 'tp')), may hold values from 0.05 to 1
Outputs:
- layer_out: bfloat16 [16384, 2048], P(('sp', 'tp'))
Inputs may be any that keep to these rules, and one draw needn't show every extreme that they name: `routes`: each row names 4 different experts. In each aligned block of 64 rows no expert is named by more than 6 rows, and in some block some expert is named by exactly 6 rows.
All inputs are finite; a program needn't handle non-finite values.
Results may differ from a plain program's by a relative error of at most 0.014.
Values may be sent and summed in bfloat16 or wider, within the bound.
No kernel may reach another device: no remote copies, remote signals or barrier semaphores. Data moves between devices by JAX's collectives and lax.ppermute only.
A program may use at most 128 MiB of HBM per device.

v0:
```python
import math

import jax
import jax.numpy as jnp
import numpy as np
from jax import lax
from jax.experimental import pallas as pl
from jax.experimental.pallas import tpu as pltpu
from jax.sharding import Mesh
from jax.sharding import PartitionSpec as P


HEAD_DIM = 128
HALF = HEAD_DIM // 2
TOPK = 4
SP = ("z", "x", "c")
SP_TP = ("z", "x", "c", "tp")
CAP = 6
TILE = 8
WIDE = 128

rope_base = 10000.0
group_eps = 1e-05
square_eps = 1e-06
clamp_limit = 7.0
swish_alpha = 1.702

F32 = jnp.float32
BF16 = jnp.bfloat16


def dims(lhs, rhs):
    return (((lhs,), (rhs,)), ((), ()))


def dot(a, b, lhs=1, rhs=0):
    return lax.dot_general(a, b, dims(lhs, rhs), preferred_element_type=F32)


def iota(shape, dim):
    return lax.broadcasted_iota(jnp.int32, shape, dim)


def call(kernel, out_shape, *args, flops=0, smem=(), scratch=()):
    moved = sum(math.prod(a.shape) * a.dtype.itemsize for a in args)
    specs = [
        pl.BlockSpec(memory_space=pltpu.SMEM if i in smem else pltpu.VMEM)
        for i in range(len(args))
    ]
    multi = isinstance(out_shape, (list, tuple))
    outs = [pl.BlockSpec(memory_space=pltpu.VMEM)] * len(out_shape) if multi else pl.BlockSpec(memory_space=pltpu.VMEM)
    return pl.pallas_call(
        kernel,
        out_shape=out_shape,
        in_specs=specs,
        out_specs=outs,
        scratch_shapes=list(scratch),
        compiler_params=pltpu.CompilerParams(vmem_limit_bytes=56 * 1024 * 1024),
        cost_estimate=pl.CostEstimate(flops=flops, bytes_accessed=moved, transcendentals=0),
    )(*args)


def shape(dims_, kind=BF16):
    return jax.ShapeDtypeStruct(dims_, kind)


def three_parts(value):
    first = value.astype(BF16)
    rest = value - first.astype(F32)
    second = rest.astype(BF16)
    return first, second, (rest - second.astype(F32)).astype(BF16)


def tables(cos_ref, sin_ref, base_ref):
    cos_own, sin_own = cos_ref[...], sin_ref[...]
    cos_base, sin_base = base_ref[0:1, :], base_ref[1:2, :]
    cosine = cos_base * cos_own - sin_base * sin_own
    sine = sin_base * cos_own + cos_base * sin_own
    return cosine, jnp.where(iota(sine.shape, 1) < HALF, -sine, sine)


def turned(values, cosine, sine):
    return values * cosine + pltpu.roll(values, HALF, 1) * sine


def state_kernel(k_ref, v_ref, decay_ref, cos_ref, sin_ref, base_ref, out_ref):
    rows, heads = decay_ref.shape
    cosine, sine = tables(cos_ref, sin_ref, base_ref)
    lower = (iota((rows, rows), 0) >= iota((rows, rows), 1)).astype(BF16)
    cumulative = sum(dot(lower, part) for part in three_parts(decay_ref[...]))
    share = out_ref.shape[1] - TILE
    per_head = HEAD_DIM // share
    for h in range(heads):
        cols = slice(h * HEAD_DIM, (h + 1) * HEAD_DIM)
        keys = turned(k_ref[:, cols].astype(F32), cosine, sine) * HEAD_DIM ** (-0.5)
        column = cumulative[:, h : h + 1]
        total = column[rows - 1 : rows, :]
        tail = keys * jnp.exp(total - column)
        state = dot(tail.astype(BF16), v_ref[:, cols], 0, 0)
        for i in range(per_head):
            out_ref[h * per_head + i, 0:share, :] = state[i * share : (i + 1) * share].astype(BF16)
            out_ref[h * per_head + i, share : share + TILE, :] = note_of(total)


def note_of(total):
    line = iota((TILE, HEAD_DIM), 0)
    first, second, third = [p.astype(F32) for p in three_parts(total)]
    note = jnp.where(line == 0, first, jnp.where(line == 1, second, jnp.where(line == 2, third, 0.0)))
    return note.astype(BF16)


def total_of(note):
    return note[0:1] + note[1:2] + note[2:3]


def group_kernel(in_ref, before_ref, reach_ref, out_ref):
    share = in_ref.shape[1] - TILE
    state = jnp.zeros((share, HEAD_DIM), F32)
    reach = jnp.zeros((1, HEAD_DIM), F32)
    for j in range(in_ref.shape[0]):
        before_ref[j] = state
        reach_ref[j] = jnp.broadcast_to(reach, (TILE, HEAD_DIM))
        piece = in_ref[j].astype(F32)
        total = total_of(piece[share:])
        state = state * jnp.exp(total) + piece[:share]
        reach = reach + total
    for i in range(out_ref.shape[0]):
        out_ref[i, 0:share, :] = state.astype(BF16)
        out_ref[i, share:, :] = note_of(reach)


def enter_kernel(place_ref, in_ref, before_ref, reach_ref, out_ref):
    share = out_ref.shape[1]
    place = place_ref[0]
    state = jnp.zeros((share, HEAD_DIM), F32)
    for j in range(in_ref.shape[0]):
        piece = in_ref[j].astype(F32)
        later = state * jnp.exp(total_of(piece[share:])) + piece[:share]
        state = jnp.where(j < place, later, state)
    for j in range(out_ref.shape[0]):
        out_ref[j] = (state * jnp.exp(reach_ref[j, 0:1]) + before_ref[j]).astype(BF16)


def inner_kernel(q_ref, k_ref, v_ref, decay_ref, cos_ref, sin_ref, base_ref, out_ref, lead_ref):
    rows, heads = decay_ref.shape
    cosine, sine = tables(cos_ref, sin_ref, base_ref)
    causal = iota((rows, rows), 0) >= iota((rows, rows), 1)
    lower = causal.astype(BF16)
    parts = three_parts(decay_ref[...])
    cumulative = sum(dot(lower, part) for part in parts)
    across = sum(dot(part, lower, 0, 1) for part in parts)
    for h in range(heads):
        cols = slice(h * HEAD_DIM, (h + 1) * HEAD_DIM)
        keys = turned(k_ref[:, cols].astype(F32), cosine, sine) * HEAD_DIM ** (-0.5)
        queries = turned(q_ref[:, cols].astype(F32), cosine, sine)
        column = cumulative[:, h : h + 1]
        gap = column - across[h : h + 1, :]
        weights = jnp.where(causal, jnp.exp(jnp.minimum(gap, 0.0)), 0.0)
        scores = dot(queries.astype(BF16), keys.astype(BF16), 1, 1) * weights
        out_ref[:, cols] = dot(scores.astype(BF16), v_ref[:, cols])
        lead_ref[:, cols] = (queries * jnp.exp(column)).astype(BF16)


def mix_kernel(inner_ref, lead_ref, enter_ref, gate_ref, gain_ref, weight_ref, out_ref, hidden_ref):
    heads = inner_ref.shape[1] // HEAD_DIM
    for h in range(heads):
        cols = slice(h * HEAD_DIM, (h + 1) * HEAD_DIM)
        kept = inner_ref[:, cols] + dot(lead_ref[:, cols], enter_ref[cols, :])
        centred = kept - jnp.mean(kept, axis=-1, keepdims=True)
        variance = jnp.mean(centred * centred, axis=-1, keepdims=True)
        gate = gate_ref[:, cols].astype(F32)
        opened = gate / (1.0 + jnp.exp(-gate))
        scaled = centred * lax.rsqrt(variance + group_eps)
        hidden_ref[:, cols] = (scaled * gain_ref[:, cols] * opened).astype(BF16)
    step = 512

    @pl.loop(0, out_ref.shape[1] // step)
    def _(n):
        cols = pl.ds(pl.multiple_of(n * step, step), step)
        out_ref[:, cols] = dot(hidden_ref[...], weight_ref[:, cols]).astype(BF16)


def norm_kernel(sum_ref, residual_ref, gain_ref, routes_ref, shares_ref, updated_ref, out_ref):
    updated = residual_ref[...].astype(F32)
    for i in range(sum_ref.shape[0]):
        updated = updated + sum_ref[i].astype(F32)
    updated_ref[...] = updated
    factor = lax.rsqrt(jnp.mean(updated * updated, axis=-1, keepdims=True) + square_eps)
    width = updated.shape[1]
    scaled = (updated * factor * gain_ref[...]).astype(BF16)
    rows = updated.shape[0]
    lane = iota((rows, WIDE), 1)
    expert = lane % (WIDE // 2)
    table = jnp.zeros((rows, WIDE), F32)
    for k in range(TOPK):
        table = table + jnp.where(routes_ref[:, k : k + 1] == expert, shares_ref[:, k : k + 1], 0.0)
    first = table.astype(BF16).astype(F32)
    noted = jnp.where(lane < WIDE // 2, first, table - first).astype(BF16)
    for i in range(out_ref.shape[0]):
        out_ref[i, :, 0:width] = scaled
        out_ref[i, :, width : width + WIDE] = noted


def lane_of(dest, place, half):
    return (dest // 2) * 8 + place * 2 + dest % 2 + half * (WIDE // 2)


def gather_kernel(place_ref, rows_ref, *refs):
    out_refs, pick_ref = refs[:-1], refs[-1]
    count = rows_ref.shape[0]
    width = rows_ref.shape[1] - WIDE
    block = count // 4
    dests = 16
    place = place_ref[0]
    table = rows_ref[:, width : width + WIDE]
    choose = (iota((dests, WIDE), 1) == lane_of(iota((dests, WIDE), 0), place, 0)).astype(BF16)
    named = (dot(choose, table, 1, 1) > 0.0).astype(F32)
    early, late = iota((count, count), 0), iota((count, count), 1)
    before = ((early < late) & (early // block == late // block)).astype(BF16)
    rank = dot(named.astype(BF16), before).astype(jnp.int32)
    slot = rank + CAP * (iota((dests, count), 1) // block)
    slot = jnp.where(named > 0.0, slot, -1)
    for c, out_ref in enumerate(out_refs):
        line = iota((dests, TILE, count), 1) + c * TILE
        pick = (slot[:, None, :] == line).astype(F32).reshape(dests * TILE, count).astype(BF16)
        pick_ref[c * dests * TILE : (c + 1) * dests * TILE, :] = pick
    step = 256

    @pl.loop(0, width // step)
    def _(n):
        cols = pl.ds(pl.multiple_of(n * step, step), step)
        chosen = dot(pick_ref[...], rows_ref[:, cols]).astype(BF16)
        for c, out_ref in enumerate(out_refs):
            out_ref[:, cols] = chosen[c * dests * TILE : (c + 1) * dests * TILE]


def merge_kernel(place_ref, table_ref, *refs):
    back_refs, out_ref, mix_refs = refs[:-3], refs[-3], refs[-2:]
    count = table_ref.shape[0]
    block = count // 4
    dests = 16
    place = place_ref[0]
    table = table_ref[...]
    high, low = [
        dot(table, (iota((WIDE, dests), 0) == lane_of(iota((WIDE, dests), 1), place, half)).astype(BF16))
        for half in (0, 1)
    ]
    late, early = iota((count, count), 0), iota((count, count), 1)
    before = ((early < late) & (early // block == late // block)).astype(BF16)
    rank = dot(before, (high > 0.0).astype(F32).astype(BF16))
    slot = rank + (CAP * (iota((count, dests), 0) // block)).astype(F32)
    spread = (iota((dests, dests * TILE), 1) // TILE == iota((dests, dests * TILE), 0)).astype(BF16)
    slot_wide = dot(slot.astype(BF16), spread).astype(jnp.int32)
    high_wide, low_wide = dot(high.astype(BF16), spread), dot(low.astype(BF16), spread)
    place_in = iota(slot_wide.shape, 1) % TILE
    high_ref, low_ref = mix_refs
    span = dests * TILE
    for c in range(len(back_refs)):
        here = slot_wide == place_in + c * TILE
        high_ref[:, c * span : (c + 1) * span] = jnp.where(here, high_wide, 0.0).astype(BF16)
        low_ref[:, c * span : (c + 1) * span] = jnp.where(here, low_wide, 0.0).astype(BF16)
    step = 256

    @pl.loop(0, out_ref.shape[1] // step)
    def _(n):
        cols = pl.ds(pl.multiple_of(n * step, step), step)
        piece = jnp.concatenate([ref[:, cols] for ref in back_refs], axis=0)
        out_ref[:, cols] = (dot(high_ref[...], piece) + dot(low_ref[...], piece)).astype(BF16)


def expert_kernel(own_ref, right_ref, left_ref, far_ref, gate_ref, up_ref, down_ref, *refs):
    outs, (all_ref, act_ref) = refs[:-2], refs[-2:]
    rows = own_ref.shape[0]
    for i, ref in enumerate((own_ref, right_ref, left_ref, far_ref)):
        all_ref[i * rows : (i + 1) * rows, :] = ref[...]
    step = 256

    @pl.loop(0, gate_ref.shape[1] // step)
    def _(n):
        cols = pl.ds(pl.multiple_of(n * step, step), step)
        gate = jnp.minimum(dot(all_ref[...], gate_ref[:, cols]), clamp_limit)
        up = jnp.clip(dot(all_ref[...], up_ref[:, cols]), -clamp_limit, clamp_limit)
        act_ref[:, cols] = ((up + 1.0) * (gate / (1.0 + jnp.exp(-swish_alpha * gate)))).astype(BF16)

    @pl.loop(0, down_ref.shape[1] // step)
    def _(n):
        cols = pl.ds(pl.multiple_of(n * step, step), step)
        part = dot(act_ref[...], down_ref[:, cols]).astype(BF16)
        for i, out_ref in enumerate(outs):
            out_ref[:, cols] = part[i * rows : (i + 1) * rows]


def ring(size, shift):
    return [(i, (i + shift) % size) for i in range(size)]


def add(a, b):
    return (a.astype(F32) + b.astype(F32)).astype(BF16)


def body(
    query_rows,
    key_rows,
    value_rows,
    gate_rows,
    log_decay,
    head_gain,
    out_weight,
    residual,
    ffn_gain,
    gate_weight,
    up_weight,
    down_weight,
    routes,
    route_weights,
):
    tok_count, heads = log_decay.shape
    local = heads * HEAD_DIM
    rows_own, width = residual.shape
    sp_count = lax.axis_size(SP)
    tp_count = lax.axis_size("tp")
    sp_index = lax.axis_index(SP)

    inverse = rope_base ** (-np.arange(HALF, dtype=np.float64) / HALF)
    inverse = np.concatenate([inverse, inverse])
    inside = np.arange(tok_count, dtype=np.float64)[:, None] * inverse[None]
    starts = (np.arange(sp_count, dtype=np.float64) * tok_count)[:, None] * inverse[None]
    cos_own, sin_own = jnp.asarray(np.cos(inside), F32), jnp.asarray(np.sin(inside), F32)
    base_all = jnp.asarray(np.stack([np.cos(starts), np.sin(starts)], axis=1), F32)
    base = lax.dynamic_index_in_dim(base_all, sp_index, 0, keepdims=False)

    near_count = lax.axis_size(("x", "c"))
    far_count = lax.axis_size("z")
    share = local // near_count
    message = call(
        state_kernel,
        shape((near_count, share + TILE, HEAD_DIM)),
        key_rows, value_rows, log_decay, cos_own, sin_own, base,
        flops=2 * tok_count * local * HEAD_DIM,
    )
    spans = lax.all_to_all(message, ("x", "c"), 0, 0, tiled=True)
    inner, lead = call(
        inner_kernel,
        [shape((tok_count, local), F32), shape((tok_count, local))],
        query_rows, key_rows, value_rows, log_decay, cos_own, sin_own, base,
        flops=4 * tok_count * tok_count * local,
    )
    before, reach, group = call(
        group_kernel,
        [shape((near_count, share, HEAD_DIM), F32), shape((near_count, TILE, HEAD_DIM), F32), shape((far_count, share + TILE, HEAD_DIM))],
        spans,
    )
    groups = lax.all_to_all(group, "z", 0, 0, tiled=True)
    entering = call(
        enter_kernel,
        shape((near_count, share, HEAD_DIM)),
        lax.axis_index("z").astype(jnp.int32).reshape(1), groups, before, reach,
        smem=(0,),
    )
    entering = lax.all_to_all(entering, ("x", "c"), 0, 0, tiled=True).reshape(local, HEAD_DIM)
    mixed = call(
        mix_kernel,
        shape((tok_count, width)),
        inner, lead, entering, gate_rows, head_gain.reshape(1, local), out_weight,
        flops=2 * tok_count * local * width,
        scratch=[pltpu.VMEM((tok_count, local), BF16)],
    )
    pieces = lax.all_to_all(mixed.reshape(tp_count, rows_own, width), "tp", 0, 0, tiled=True)
    own_routes = lax.dynamic_slice_in_dim(routes, lax.axis_index("tp") * rows_own, rows_own, 0)
    x_count = lax.axis_size("x")
    updated, spread = call(
        norm_kernel,
        [shape((rows_own, width), F32), shape((x_count, rows_own, width + WIDE))],
        pieces, residual, ffn_gain.reshape(1, width), own_routes, route_weights,
    )

    place = lax.axis_index("x").astype(jnp.int32).reshape(1)
    near = lax.all_to_all(spread, "x", 0, 0, tiled=True).reshape(x_count * rows_own, width + WIDE)
    dests = sp_count // x_count
    chunks = x_count * CAP // TILE
    outgoing = call(
        gather_kernel,
        [shape((dests * TILE, width))] * chunks,
        place, near,
        flops=2 * chunks * dests * TILE * near.shape[0] * width,
        smem=(0,),
        scratch=[pltpu.VMEM((chunks * dests * TILE, near.shape[0]), BF16)],
    )
    gate_part, up_part, down_part = gate_weight[0], up_weight[0], down_weight[0]
    ahead, behind = ring(tp_count, 1), ring(tp_count, -1)
    returned = []
    for c, piece in enumerate(outgoing, 1):
        first, second = (ahead, behind) if c % 2 else (behind, ahead)
        own = lax.all_to_all(piece.reshape(dests, TILE, width), ("z", "c"), 0, 0, tiled=True)
        own = own.reshape(dests * TILE, width)
        rows = own.shape[0]
        one = lax.ppermute(own, "tp", first)
        two = lax.ppermute(own, "tp", second)
        far = lax.ppermute(one, "tp", first)
        out_own, out_one, out_two, out_far = call(
            expert_kernel,
            [shape((rows, width))] * 4,
            own, one, two, far, gate_part, up_part, down_part,
            flops=6 * 4 * rows * width * gate_part.shape[1],
            scratch=[pltpu.VMEM((4 * rows, width), BF16), pltpu.VMEM((4 * rows, gate_part.shape[1]), BF16)],
        )
        via = lax.ppermute(out_far, "tp", second)
        back_one = lax.ppermute(add(out_one, via), "tp", second)
        back_two = lax.ppermute(out_two, "tp", first)
        total = (out_own.astype(F32) + back_one.astype(F32) + back_two.astype(F32)).astype(BF16)
        back = lax.all_to_all(total.reshape(dests, TILE, width), ("z", "c"), 0, 0, tiled=True)
        returned.append(back.reshape(dests * TILE, width))
    merged = call(
        merge_kernel,
        shape((x_count * rows_own, width)),
        place, near[:, width:], *returned,
        flops=4 * chunks * dests * TILE * near.shape[0] * width,
        smem=(0,),
        scratch=[pltpu.VMEM((near.shape[0], chunks * dests * TILE), BF16)] * 2,
    )
    parts = lax.all_to_all(merged.reshape(x_count, rows_own, width), "x", 0, 0, tiled=True)
    return (updated + jnp.sum(parts.astype(F32), axis=0)).astype(BF16)


def solution(mesh):
    finer = Mesh(mesh.devices.reshape(8, 4, 2, mesh.shape["tp"]), SP_TP)
    return jax.shard_map(
        body,
        mesh=finer,
        in_specs=(
            P(SP, "tp"),
            P(SP, "tp"),
            P(SP, "tp"),
            P(SP, "tp"),
            P(SP, "tp"),
            P("tp"),
            P("tp", None),
            P(SP_TP, None),
            P(),
            P(SP, None, "tp"),
            P(SP, None, "tp"),
            P(SP, "tp", None),
            P(SP, None),
            P(SP_TP, None),
        ),
        out_specs=P(SP_TP, None),
        check_vma=False,
    )
```

profile of v0, /device:TPU:2, one launch (start us, length us, event | category | flops | bytes accessed | tf_op | source)
XLA Modules:
  0.0 320.3 jit_solution(5341830938811410786)
XLA Ops:
  5.4 11.0 %all_to_all.60.in_ref = bf16[8,72,128]{2,1,0:T(8,128)(2,1)} all-to-all(bf16[8,72,128]{2,1,0:T(8,128)(2,1)} %shard_map.164), channel_id=1, replica_groups=mesh['z'=8,'x'=4,'c'=2,'tp'=4] {'x','c'}, dimensions={0} | all-to-all | bytes 294912 | tf_op jit(solution)/shard_map/all_to_all | solution.py:341
  18.1 16.5 %all_to_all.61.in_ref = bf16[8,72,128]{2,1,0:T(8,128)(2,1)} all-to-all(bf16[8,72,128]{2,1,0:T(8,128)(2,1)} %get-tuple-element.29), channel_id=1, replica_groups=mesh['z'=8,'x'=4,'c'=2,'tp'=4] {'z'}, dimensions={0} | all-to-all | bytes 294912 | tf_op jit(solution)/shard_map/all_to_all | solution.py:353
  36.3 4.7 %all-to-all-start.2 = ((bf16[8,64,128]{2,1,0:T(8,128)(2,1)}), bf16[8,64,128]{2,1,0:T(8,128)(2,1)S(1)}, u32[]{:S(2)}, u32[]{:S(2)}) async-start(bf16[8,64,128]{2,1,0:T(8,128)(2,1)} %shard_map.166), calls=%async_computation.2 | async-start | bytes 262144 | tf_op jit(solution)/shard_map/all_to_all | solution.py:360
  41.1 3.0 shard_map.163
  46.4 4.8 %shard_map.167 = bf16[256,2048]{1,0:T(8,128)(2,1)} custom-call(f32[256,512]{1,0:T(8,128)} %get-tuple-element.27.inner_ref, bf16[256,512]{1,0:T(8,128)(2,1)} %get-tuple-element.28.lead_ref, bf16[512,128]{1,0:T(8,128)(2,1)} %bitcast.32, bf16[256,512]{1,0:T(8,128)(2,1)} %gate_ref.1, f32[1,512]{1,0:T(1,128)} %bitcast.48, bf16[512,2048]{1,0:T(8,128)(2,1)} %weight_ref.1), custom_call_target="tpu_custom_call" | custom-call | flops 536870912 | bytes 3278848 | tf_op jit(solution)/shard_map/pallas_call | solution.py:52
  51.2 4.6 %all-to-all-start.3 = ((bf16[4,64,2048]{2,1,0:T(8,128)(2,1)}), bf16[4,64,2048]{2,1,0:T(8,128)(2,1)S(1)}, u32[]{:S(2)}, u32[]{:S(2)}) async-start(bf16[4,64,2048]{2,1,0:T(8,128)(2,1)} %bitcast.28), calls=%async_computation.3 | async-start | bytes 2097152 | tf_op jit(solution)/shard_map/all_to_all | solution.py:368
  57.3 13.4 %all-to-all-done.3.sum_ref = bf16[4,64,2048]{2,1,0:T(8,128)(2,1)S(1)} async-done(((bf16[4,64,2048]{2,1,0:T(8,128)(2,1)}), bf16[4,64,2048]{2,1,0:T(8,128)(2,1)S(1)}, u32[]{:S(2)}, u32[]{:S(2)}) %all-to-all-start.3) | async-done | bytes 1048608 | tf_op jit(solution)/shard_map/all_to_all | solution.py:368
  74.4 19.1 %all_to_all.62 = bf16[4,64,2176]{2,1,0:T(8,128)(2,1)} all-to-all(bf16[4,64,2176]{2,1,0:T(8,128)(2,1)} %get-tuple-element.33), channel_id=1, replica_groups=mesh['z'=8,'x'=4,'c'=2,'tp'=4] {'x'}, dimensions={0} | all-to-all | bytes 2228224 | tf_op jit(solution)/shard_map/all_to_all | solution.py:378
  93.4 4.5 %shard_map.169 = (bf16[128,2048]{1,0:T(8,128)(2,1)}, bf16[128,2048]{1,0:T(8,128)(2,1)}, bf16[128,2048]{1,0:T(8,128)(2,1)}) custom-call(s32[1]{0:T(128)} %bitcast.6.place_ref, bf16[256,2176]{1,0:T(8,128)(2,1)} %bitcast.29), custom_call_target="tpu_custom_call" | custom-call | flops 402653184 | bytes 1114116 | tf_op jit(solution)/shard_map/pallas_call | solution.py:52
  97.9 19.5 %all_to_all.63 = bf16[16,8,2048]{2,1,0:T(8,128)(2,1)S(1)} all-to-all(bf16[16,8,2048]{2,1,0:T(8,128)(2,1)} %bitcast.46), channel_id=1, replica_groups=mesh['z'=8,'x'=4,'c'=2,'tp'=4] {'z','c'}, dimensions={0} | all-to-all | bytes 1048576 | tf_op jit(solution)/shard_map/all_to_all | solution.py:394
  117.3 4.2 %all-to-all-start.5 = ((bf16[16,8,2048]{2,1,0:T(8,128)(2,1)}), bf16[16,8,2048]{2,1,0:T(8,128)(2,1)S(1)}, u32[]{:S(2)}, u32[]{:S(2)}) async-start(bf16[16,8,2048]{2,1,0:T(8,128)(2,1)} %bitcast.45), calls=%async_computation.5 | async-start | bytes 1048576 | tf_op jit(solution)/shard_map/all_to_all | solution.py:394
  122.2 15.5 %all-to-all-done.5 = bf16[16,8,2048]{2,1,0:T(8,128)(2,1)S(1)} async-done(((bf16[16,8,2048]{2,1,0:T(8,128)(2,1)}), bf16[16,8,2048]{2,1,0:T(8,128)(2,1)S(1)}, u32[]{:S(2)}, u32[]{:S(2)}) %all-to-all-start.5) | async-done | bytes 524320 | tf_op jit(solution)/shard_map/all_to_all | solution.py:394
  137.7 4.0 %all-to-all-start.7 = ((bf16[16,8,2048]{2,1,0:T(8,128)(2,1)}), bf16[16,8,2048]{2,1,0:T(8,128)(2,1)S(1)}, u32[]{:S(2)}, u32[]{:S(2)}) async-start(bf16[16,8,2048]{2,1,0:T(8,128)(2,1)} %bitcast.15), calls=%async_computation.7 | async-start | bytes 1048576 | tf_op jit(solution)/shard_map/all_to_all | solution.py:394
  145.1 3.2 %collective-permute-start.1 = (bf16[128,2048]{1,0:T(8,128)(2,1)S(1)}, bf16[128,2048]{1,0:T(8,128)(2,1)S(1)}, u32[]{:S(2)}, u32[]{:S(2)}) collective-permute-start(bf16[128,2048]{1,0:T(8,128)(2,1)S(1)} %bitcast.37), channel_id=1, source_target_pairs={{0,3},{1,0},{2,1},{3,2},{4,7},{5,4},{6,5},{7,6},{8,11},{9,8},{10,9... | collective-permute-start | bytes 1572872 | tf_op jit(solution)/shard_map/ppermute | solution.py:398
  148.3 9.6 %all-to-all-done.7 = bf16[16,8,2048]{2,1,0:T(8,128)(2,1)S(1)} async-done(((bf16[16,8,2048]{2,1,0:T(8,128)(2,1)}), bf16[16,8,2048]{2,1,0:T(8,128)(2,1)S(1)}, u32[]{:S(2)}, u32[]{:S(2)}) %all-to-all-start.7) | async-done | bytes 524320 | tf_op jit(solution)/shard_map/all_to_all | solution.py:394
  159.9 9.2 %collective-permute-done.14.far_ref = bf16[128,2048]{1,0:T(8,128)(2,1)} collective-permute-done((bf16[128,2048]{1,0:T(8,128)(2,1)}, bf16[128,2048]{1,0:T(8,128)(2,1)}, u32[]{:S(2)}, u32[]{:S(2)}) %collective-permute-start.14) | collective-permute-done | bytes 524320 | tf_op jit(solution)/shard_map/ppermute | solution.py:399
  169.2 10.0 %shard_map.172 = (bf16[128,2048]{1,0:T(8,128)(2,1)}, bf16[128,2048]{1,0:T(8,128)(2,1)}, bf16[128,2048]{1,0:T(8,128)(2,1)}, bf16[128,2048]{1,0:T(8,128)(2,1)}) custom-call(bf16[128,2048]{1,0:T(8,128)(2,1)} %bitcast.42, bf16[128,2048]{1,0:T(8,128)(2,1)} %collective-permute-done.12.right_ref, bf16[128,2048]{1,0:T(8,128)(2,1)} %collective-permute-done.13.left_ref, ...), custom_call_target="tpu_custom_call" | custom-call | flops 3221225472 | bytes 8388608 | tf_op jit(solution)/shard_map/pallas_call | solution.py:52
  185.0 10.0 %shard_map.170 = (bf16[128,2048]{1,0:T(8,128)(2,1)}, bf16[128,2048]{1,0:T(8,128)(2,1)}, bf16[128,2048]{1,0:T(8,128)(2,1)}, bf16[128,2048]{1,0:T(8,128)(2,1)}) custom-call(bf16[128,2048]{1,0:T(8,128)(2,1)} %bitcast.38, bf16[128,2048]{1,0:T(8,128)(2,1)} %copy-done.18, bf16[128,2048]{1,0:T(8,128)(2,1)} %copy-done.19, bf16[128,2048]{1,0:T(8,128)(2,1)} %copy-done.22, ...), custom_call_target="tpu_custom_call" | custom-call | flops 3221225472 | bytes 8388608 | tf_op jit(solution)/shard_map/pallas_call | solution.py:52
  195.0 3.1 collective-permute-start.3
  198.3 3.3 %collective-permute-start.16 = (bf16[128,2048]{1,0:T(8,128)(2,1)S(1)}, bf16[128,2048]{1,0:T(8,128)(2,1)S(1)}, u32[]{:S(2)}, u32[]{:S(2)}) collective-permute-start(bf16[128,2048]{1,0:T(8,128)(2,1)S(1)} %add_convert_fusion.1), channel_id=1, source_target_pairs={{0,3},{1,0},{2,1},{3,2},{4,7},{5,4},{6,5},{7,6},{8,11},{9,8},{10,9... | collective-permute-start | bytes 1572872 | tf_op jit(solution)/shard_map/ppermute | solution.py:408
  201.6 3.9 %collective-permute-done.8.far_ref = bf16[128,2048]{1,0:T(8,128)(2,1)S(1)} collective-permute-done((bf16[128,2048]{1,0:T(8,128)(2,1)S(1)}, bf16[128,2048]{1,0:T(8,128)(2,1)S(1)}, u32[]{:S(2)}, u32[]{:S(2)}) %collective-permute-start.8) | collective-permute-done | bytes 524320 | tf_op jit(solution)/shard_map/ppermute | solution.py:399
  206.3 10.0 %shard_map.171 = (bf16[128,2048]{1,0:T(8,128)(2,1)}, bf16[128,2048]{1,0:T(8,128)(2,1)}, bf16[128,2048]{1,0:T(8,128)(2,1)}, bf16[128,2048]{1,0:T(8,128)(2,1)}) custom-call(bf16[128,2048]{1,0:T(8,128)(2,1)} %bitcast.35, bf16[128,2048]{1,0:T(8,128)(2,1)} %copy-done.17, bf16[128,2048]{1,0:T(8,128)(2,1)} %copy-done.20, bf16[128,2048]{1,0:T(8,128)(2,1)} %copy-done.21, ...), custom_call_target="tpu_custom_call" | custom-call | flops 3221225472 | bytes 8388608 | tf_op jit(solution)/shard_map/pallas_call | solution.py:52
  216.8 2.8 collective-permute-start.11
  219.8 8.2 %collective-permute-done.16 = bf16[128,2048]{1,0:T(8,128)(2,1)S(1)} collective-permute-done((bf16[128,2048]{1,0:T(8,128)(2,1)S(1)}, bf16[128,2048]{1,0:T(8,128)(2,1)S(1)}, u32[]{:S(2)}, u32[]{:S(2)}) %collective-permute-start.16) | collective-permute-done | bytes 524320 | tf_op jit(solution)/shard_map/ppermute | solution.py:408
  229.0 7.1 %all-to-all-start.10 = ((bf16[16,8,2048]{2,1,0:T(8,128)(2,1)}), bf16[16,8,2048]{2,1,0:T(8,128)(2,1)S(1)}, u32[]{:S(2)}, u32[]{:S(2)}) async-start(bf16[16,8,2048]{2,1,0:T(8,128)(2,1)} %fusion.2), calls=%async_computation.10 | async-start | bytes 1048576 | tf_op jit(solution)/shard_map/all_to_all | solution.py:411
  236.5 13.1 %collective-permute-done.4 = bf16[128,2048]{1,0:T(8,128)(2,1)} collective-permute-done((bf16[128,2048]{1,0:T(8,128)(2,1)S(1)}, bf16[128,2048]{1,0:T(8,128)(2,1)}, u32[]{:S(2)}, u32[]{:S(2)}) %collective-permute-start.4) | collective-permute-done | bytes 524320 | tf_op jit(solution)/shard_map/ppermute | solution.py:408
  252.1 5.3 %all-to-all-start.6 = ((bf16[16,8,2048]{2,1,0:T(8,128)(2,1)}), bf16[16,8,2048]{2,1,0:T(8,128)(2,1)S(1)}, u32[]{:S(2)}, u32[]{:S(2)}) async-start(bf16[16,8,2048]{2,1,0:T(8,128)(2,1)} %fusion), calls=%async_computation.6 | async-start | bytes 1048576 | tf_op jit(solution)/shard_map/all_to_all | solution.py:411
  259.7 13.6 %all-to-all-done.6 = bf16[16,8,2048]{2,1,0:T(8,128)(2,1)S(1)} async-done(((bf16[16,8,2048]{2,1,0:T(8,128)(2,1)}), bf16[16,8,2048]{2,1,0:T(8,128)(2,1)S(1)}, u32[]{:S(2)}, u32[]{:S(2)}) %all-to-all-start.6) | async-done | bytes 524320 | tf_op jit(solution)/shard_map/all_to_all | solution.py:411
  273.4 4.2 %all-to-all-start.8 = ((bf16[16,8,2048]{2,1,0:T(8,128)(2,1)}), bf16[16,8,2048]{2,1,0:T(8,128)(2,1)S(1)}, u32[]{:S(2)}, u32[]{:S(2)}) async-start(bf16[16,8,2048]{2,1,0:T(8,128)(2,1)} %fusion.1), calls=%async_computation.8 | async-start | bytes 1048576 | tf_op jit(solution)/shard_map/all_to_all | solution.py:411
  279.1 14.7 %all-to-all-done.8 = bf16[16,8,2048]{2,1,0:T(8,128)(2,1)S(1)} async-done(((bf16[16,8,2048]{2,1,0:T(8,128)(2,1)}), bf16[16,8,2048]{2,1,0:T(8,128)(2,1)S(1)}, u32[]{:S(2)}, u32[]{:S(2)}) %all-to-all-start.8) | async-done | bytes 524320 | tf_op jit(solution)/shard_map/all_to_all | solution.py:411
  294.6 5.2 %shard_map.173 = bf16[256,2048]{1,0:T(8,128)(2,1)} custom-call(s32[1]{0:T(128)} %bitcast.6.place_ref, bf16[256,128]{1,0:T(8,128)(2,1)} %slice.4.table_ref, bf16[128,2048]{1,0:T(8,128)(2,1)} %bitcast.43, bf16[128,2048]{1,0:T(8,128)(2,1)} %bitcast.44, bf16[128,2048]{1,0:T(8,128)(2,1)} %bitcast.39), custom_call_target="tpu_custom_call" | custom-call | flops 805306368 | bytes 1638404 | tf_op jit(solution)/shard_map/pallas_call | solution.py:52
  299.7 19.6 %all_to_all.64 = bf16[4,64,2048]{2,1,0:T(8,128)(2,1)S(1)} all-to-all(bf16[4,64,2048]{2,1,0:T(8,128)(2,1)} %bitcast.31), channel_id=1, replica_groups=mesh['z'=8,'x'=4,'c'=2,'tp'=4] {'x'}, dimensions={0} | all-to-all | bytes 2097152 | tf_op jit(solution)/shard_map/all_to_all | solution.py:421
  (94 shorter events, 39.0 us)
Async XLA Ops:
  0.0 55.8 %copy-start = (s32[256,4]{0,1:T(4,128)S(1)}, s32[256,4]{0,1:T(4,128)}, u32[]{:S(2)}) copy-start(s32[256,4]{0,1:T(4,128)} %param.29) | copy-start | bytes 12292
  36.3 9.4 %all-to-all-start.2 = ((bf16[8,64,128]{2,1,0:T(8,128)(2,1)}), bf16[8,64,128]{2,1,0:T(8,128)(2,1)S(1)}, u32[]{:S(2)}, u32[]{:S(2)}) async-start(bf16[8,64,128]{2,1,0:T(8,128)(2,1)} %shard_map.166), calls=%async_computation.2 | async-start | bytes 262144 | tf_op jit(solution)/shard_map/all_to_all | solution.py:360
  51.2 19.5 %all-to-all-start.3 = ((bf16[4,64,2048]{2,1,0:T(8,128)(2,1)}), bf16[4,64,2048]{2,1,0:T(8,128)(2,1)S(1)}, u32[]{:S(2)}, u32[]{:S(2)}) async-start(bf16[4,64,2048]{2,1,0:T(8,128)(2,1)} %bitcast.28), calls=%async_computation.3 | async-start | bytes 2097152 | tf_op jit(solution)/shard_map/all_to_all | solution.py:368
  117.3 51.8 %copy-start.10 = (bf16[16,8,2048]{2,1,0:T(8,128)(2,1)}, bf16[16,8,2048]{2,1,0:T(8,128)(2,1)S(1)}, u32[]{:S(2)}) copy-start(bf16[16,8,2048]{2,1,0:T(8,128)(2,1)S(1)} %all_to_all.63) | copy-start | bytes 1572868
  117.3 20.4 %all-to-all-start.5 = ((bf16[16,8,2048]{2,1,0:T(8,128)(2,1)}), bf16[16,8,2048]{2,1,0:T(8,128)(2,1)S(1)}, u32[]{:S(2)}, u32[]{:S(2)}) async-start(bf16[16,8,2048]{2,1,0:T(8,128)(2,1)} %bitcast.45), calls=%async_computation.5 | async-start | bytes 1048576 | tf_op jit(solution)/shard_map/all_to_all | solution.py:394
  121.6 23.5 %collective-permute-start.12 = (bf16[128,2048]{1,0:T(8,128)(2,1)S(1)}, bf16[128,2048]{1,0:T(8,128)(2,1)}, u32[]{:S(2)}, u32[]{:S(2)}) collective-permute-start(bf16[128,2048]{1,0:T(8,128)(2,1)S(1)} %bitcast.40), channel_id=1, source_target_pairs={{0,1},{1,2},{2,3},{3,0},{4,5},{5,6},{6,7},{7,4},{8,9},{9,10},{10,1... | collective-permute-start | bytes 1572872 | tf_op jit(solution)/shard_map/ppermute | solution.py:397
  137.7 41.5 %copy-start.8 = (bf16[16,8,2048]{2,1,0:T(8,128)(2,1)}, bf16[16,8,2048]{2,1,0:T(8,128)(2,1)S(1)}, u32[]{:S(2)}) copy-start(bf16[16,8,2048]{2,1,0:T(8,128)(2,1)S(1)} %all-to-all-done.5) | copy-start | bytes 1572868
  137.7 20.2 %all-to-all-start.7 = ((bf16[16,8,2048]{2,1,0:T(8,128)(2,1)}), bf16[16,8,2048]{2,1,0:T(8,128)(2,1)S(1)}, u32[]{:S(2)}, u32[]{:S(2)}) async-start(bf16[16,8,2048]{2,1,0:T(8,128)(2,1)} %bitcast.15), calls=%async_computation.7 | async-start | bytes 1048576 | tf_op jit(solution)/shard_map/all_to_all | solution.py:394
  141.8 17.3 %collective-permute-start = (bf16[128,2048]{1,0:T(8,128)(2,1)S(1)}, bf16[128,2048]{1,0:T(8,128)(2,1)S(1)}, u32[]{:S(2)}, u32[]{:S(2)}) collective-permute-start(bf16[128,2048]{1,0:T(8,128)(2,1)S(1)} %bitcast.36), channel_id=1, source_target_pairs={{0,1},{1,2},{2,3},{3,0},{4,5},{5,6},{6,7},{7,4},{8,9},{9,10},{10,1... | collective-permute-start | bytes 1572872 | tf_op jit(solution)/shard_map/ppermute | solution.py:397
  142.4 17.5 %collective-permute-start.13 = (bf16[128,2048]{1,0:T(8,128)(2,1)S(1)}, bf16[128,2048]{1,0:T(8,128)(2,1)}, u32[]{:S(2)}, u32[]{:S(2)}) collective-permute-start(bf16[128,2048]{1,0:T(8,128)(2,1)S(1)} %bitcast.41), channel_id=1, source_target_pairs={{0,3},{1,0},{2,1},{3,2},{4,7},{5,4},{6,5},{7,6},{8,11},{9,8},{10,9... | collective-permute-start | bytes 1572872 | tf_op jit(solution)/shard_map/ppermute | solution.py:398
  145.1 24.1 %collective-permute-start.14 = (bf16[128,2048]{1,0:T(8,128)(2,1)}, bf16[128,2048]{1,0:T(8,128)(2,1)}, u32[]{:S(2)}, u32[]{:S(2)}) collective-permute-start(bf16[128,2048]{1,0:T(8,128)(2,1)} %collective-permute-done.12.right_ref), channel_id=1, source_target_pairs={{0,1},{1,2},{2,3},{3,0},{4,5},{5,6},{6,7},{7,4},{8,9},{9,10},{10,1... | collective-permute-start | bytes 1572872 | tf_op jit(solution)/shard_map/ppermute | solution.py:399
  145.1 38.1 %collective-permute-start.1 = (bf16[128,2048]{1,0:T(8,128)(2,1)S(1)}, bf16[128,2048]{1,0:T(8,128)(2,1)S(1)}, u32[]{:S(2)}, u32[]{:S(2)}) collective-permute-start(bf16[128,2048]{1,0:T(8,128)(2,1)S(1)} %bitcast.37), channel_id=1, source_target_pairs={{0,3},{1,0},{2,1},{3,2},{4,7},{5,4},{6,5},{7,6},{8,11},{9,8},{10,9... | collective-permute-start | bytes 1572872 | tf_op jit(solution)/shard_map/ppermute | solution.py:398
  157.9 21.4 %copy-start.7 = (bf16[16,8,2048]{2,1,0:T(8,128)(2,1)}, bf16[16,8,2048]{2,1,0:T(8,128)(2,1)S(1)}, u32[]{:S(2)}) copy-start(bf16[16,8,2048]{2,1,0:T(8,128)(2,1)S(1)} %all-to-all-done.7) | copy-start | bytes 1572868
  157.9 23.4 %collective-permute-start.6 = (bf16[128,2048]{1,0:T(8,128)(2,1)S(1)}, bf16[128,2048]{1,0:T(8,128)(2,1)S(1)}, u32[]{:S(2)}, u32[]{:S(2)}) collective-permute-start(bf16[128,2048]{1,0:T(8,128)(2,1)S(1)} %bitcast.33), channel_id=1, source_target_pairs={{0,3},{1,0},{2,1},{3,2},{4,7},{5,4},{6,5},{7,6},{8,11},{9,8},{10,9... | collective-permute-start | bytes 1572872 | tf_op jit(solution)/shard_map/ppermute | solution.py:397
  159.1 25.1 %collective-permute-start.2 = (bf16[128,2048]{1,0:T(8,128)(2,1)S(1)}, bf16[128,2048]{1,0:T(8,128)(2,1)S(1)}, u32[]{:S(2)}, u32[]{:S(2)}) collective-permute-start(bf16[128,2048]{1,0:T(8,128)(2,1)S(1)} %collective-permute-done.right_ref), channel_id=1, source_target_pairs={{0,1},{1,2},{2,3},{3,0},{4,5},{5,6},{6,7},{7,4},{8,9},{9,10},{10,1... | collective-permute-start | bytes 1572872 | tf_op jit(solution)/shard_map/ppermute | solution.py:399
  179.2 18.9 %collective-permute-start.15 = (bf16[128,2048]{1,0:T(8,128)(2,1)}, bf16[128,2048]{1,0:T(8,128)(2,1)S(1)}, u32[]{:S(2)}, u32[]{:S(2)}) collective-permute-start(bf16[128,2048]{1,0:T(8,128)(2,1)} %get-tuple-element.47), channel_id=1, source_target_pairs={{0,3},{1,0},{2,1},{3,2},{4,7},{5,4},{6,5},{7,6},{8,11},{9,8},{10,9... | collective-permute-start | bytes 1572872 | tf_op jit(solution)/shard_map/ppermute | solution.py:407
  179.3 19.0 %collective-permute-start.7 = (bf16[128,2048]{1,0:T(8,128)(2,1)S(1)}, bf16[128,2048]{1,0:T(8,128)(2,1)S(1)}, u32[]{:S(2)}, u32[]{:S(2)}) collective-permute-start(bf16[128,2048]{1,0:T(8,128)(2,1)S(1)} %bitcast.34), channel_id=1, source_target_pairs={{0,1},{1,2},{2,3},{3,0},{4,5},{5,6},{6,7},{7,4},{8,9},{9,10},{10,1... | collective-permute-start | bytes 1572872 | tf_op jit(solution)/shard_map/ppermute | solution.py:398
  181.3 24.2 %collective-permute-start.8 = (bf16[128,2048]{1,0:T(8,128)(2,1)S(1)}, bf16[128,2048]{1,0:T(8,128)(2,1)S(1)}, u32[]{:S(2)}, u32[]{:S(2)}) collective-permute-start(bf16[128,2048]{1,0:T(8,128)(2,1)S(1)} %collective-permute-done.6.right_ref), channel_id=1, source_target_pairs={{0,3},{1,0},{2,1},{3,2},{4,7},{5,4},{6,5},{7,6},{8,11},{9,8},{10,9... | collective-permute-start | bytes 1572872 | tf_op jit(solution)/shard_map/ppermute | solution.py:399
  184.1 35.6 %collective-permute-start.17 = (bf16[128,2048]{1,0:T(8,128)(2,1)}, bf16[128,2048]{1,0:T(8,128)(2,1)S(1)}, u32[]{:S(2)}, u32[]{:S(2)}) collective-permute-start(bf16[128,2048]{1,0:T(8,128)(2,1)} %get-tuple-element.48), channel_id=1, source_target_pairs={{0,1},{1,2},{2,3},{3,0},{4,5},{5,6},{6,7},{7,4},{8,9},{9,10},{10,1... | collective-permute-start | bytes 1572872 | tf_op jit(solution)/shard_map/ppermute | solution.py:409
  195.0 21.8 %collective-permute-start.3 = (bf16[128,2048]{1,0:T(8,128)(2,1)}, bf16[128,2048]{1,0:T(8,128)(2,1)S(1)}, u32[]{:S(2)}, u32[]{:S(2)}) collective-permute-start(bf16[128,2048]{1,0:T(8,128)(2,1)} %get-tuple-element.37), channel_id=1, source_target_pairs={{0,3},{1,0},{2,1},{3,2},{4,7},{5,4},{6,5},{7,6},{8,11},{9,8},{10,9... | collective-permute-start | bytes 1572872 | tf_op jit(solution)/shard_map/ppermute | solution.py:407
  198.1 38.4 %collective-permute-start.5 = (bf16[128,2048]{1,0:T(8,128)(2,1)}, bf16[128,2048]{1,0:T(8,128)(2,1)}, u32[]{:S(2)}, u32[]{:S(2)}) collective-permute-start(bf16[128,2048]{1,0:T(8,128)(2,1)} %get-tuple-element.38), channel_id=1, source_target_pairs={{0,1},{1,2},{2,3},{3,0},{4,5},{5,6},{6,7},{7,4},{8,9},{9,10},{10,1... | collective-permute-start | bytes 1572872 | tf_op jit(solution)/shard_map/ppermute | solution.py:409
  198.2 21.3 %copy-start.3 = (bf16[128,2048]{1,0:T(8,128)(2,1)S(1)}, bf16[128,2048]{1,0:T(8,128)(2,1)}, u32[]{:S(2)}) copy-start(bf16[128,2048]{1,0:T(8,128)(2,1)} %get-tuple-element.36) | copy-start | bytes 1572868
  198.2 29.8 %copy-start.13 = (bf16[128,2048]{1,0:T(8,128)(2,1)S(1)}, bf16[128,2048]{1,0:T(8,128)(2,1)}, u32[]{:S(2)}) copy-start(bf16[128,2048]{1,0:T(8,128)(2,1)} %get-tuple-element.45) | copy-start | bytes 1572868
  198.3 29.7 %collective-permute-start.16 = (bf16[128,2048]{1,0:T(8,128)(2,1)S(1)}, bf16[128,2048]{1,0:T(8,128)(2,1)S(1)}, u32[]{:S(2)}, u32[]{:S(2)}) collective-permute-start(bf16[128,2048]{1,0:T(8,128)(2,1)S(1)} %add_convert_fusion.1), channel_id=1, source_target_pairs={{0,3},{1,0},{2,1},{3,2},{4,7},{5,4},{6,5},{7,6},{8,11},{9,8},{10,9... | collective-permute-start | bytes 1572872 | tf_op jit(solution)/shard_map/ppermute | solution.py:408
  216.3 19.9 %collective-permute-start.9 = (bf16[128,2048]{1,0:T(8,128)(2,1)}, bf16[128,2048]{1,0:T(8,128)(2,1)S(1)}, u32[]{:S(2)}, u32[]{:S(2)}) collective-permute-start(bf16[128,2048]{1,0:T(8,128)(2,1)} %get-tuple-element.42), channel_id=1, source_target_pairs={{0,1},{1,2},{2,3},{3,0},{4,5},{5,6},{6,7},{7,4},{8,9},{9,10},{10,1... | collective-permute-start | bytes 1572872 | tf_op jit(solution)/shard_map/ppermute | solution.py:407
  216.8 40.7 %collective-permute-start.11 = (bf16[128,2048]{1,0:T(8,128)(2,1)}, bf16[128,2048]{1,0:T(8,128)(2,1)}, u32[]{:S(2)}, u32[]{:S(2)}) collective-permute-start(bf16[128,2048]{1,0:T(8,128)(2,1)} %get-tuple-element.43), channel_id=1, source_target_pairs={{0,3},{1,0},{2,1},{3,2},{4,7},{5,4},{6,5},{7,6},{8,11},{9,8},{10,9... | collective-permute-start | bytes 1572872 | tf_op jit(solution)/shard_map/ppermute | solution.py:409
  219.7 29.8 %collective-permute-start.4 = (bf16[128,2048]{1,0:T(8,128)(2,1)S(1)}, bf16[128,2048]{1,0:T(8,128)(2,1)}, u32[]{:S(2)}, u32[]{:S(2)}) collective-permute-start(bf16[128,2048]{1,0:T(8,128)(2,1)S(1)} %add_convert_fusion.5), channel_id=1, source_target_pairs={{0,3},{1,0},{2,1},{3,2},{4,7},{5,4},{6,5},{7,6},{8,11},{9,8},{10,9... | collective-permute-start | bytes 1572872 | tf_op jit(solution)/shard_map/ppermute | solution.py:408
  228.0 21.5 %copy-start.14 = (bf16[128,2048]{1,0:T(8,128)(2,1)S(1)}, bf16[128,2048]{1,0:T(8,128)(2,1)}, u32[]{:S(2)}) copy-start(bf16[128,2048]{1,0:T(8,128)(2,1)} %get-tuple-element.35) | copy-start | bytes 1572868
  229.0 23.1 %all-to-all-start.10 = ((bf16[16,8,2048]{2,1,0:T(8,128)(2,1)}), bf16[16,8,2048]{2,1,0:T(8,128)(2,1)S(1)}, u32[]{:S(2)}, u32[]{:S(2)}) async-start(bf16[16,8,2048]{2,1,0:T(8,128)(2,1)} %fusion.2), calls=%async_computation.10 | async-start | bytes 1048576 | tf_op jit(solution)/shard_map/all_to_all | solution.py:411
  236.4 21.1 %collective-permute-start.10 = (bf16[128,2048]{1,0:T(8,128)(2,1)S(1)}, bf16[128,2048]{1,0:T(8,128)(2,1)}, u32[]{:S(2)}, u32[]{:S(2)}) collective-permute-start(bf16[128,2048]{1,0:T(8,128)(2,1)S(1)} %add_convert_fusion.3), channel_id=1, source_target_pairs={{0,1},{1,2},{2,3},{3,0},{4,5},{5,6},{6,7},{7,4},{8,9},{9,10},{10,1... | collective-permute-start | bytes 1572872 | tf_op jit(solution)/shard_map/ppermute | solution.py:408
  252.1 21.2 %all-to-all-start.6 = ((bf16[16,8,2048]{2,1,0:T(8,128)(2,1)}), bf16[16,8,2048]{2,1,0:T(8,128)(2,1)S(1)}, u32[]{:S(2)}, u32[]{:S(2)}) async-start(bf16[16,8,2048]{2,1,0:T(8,128)(2,1)} %fusion), calls=%async_computation.6 | async-start | bytes 1048576 | tf_op jit(solution)/shard_map/all_to_all | solution.py:411
  273.4 20.4 %all-to-all-start.8 = ((bf16[16,8,2048]{2,1,0:T(8,128)(2,1)}), bf16[16,8,2048]{2,1,0:T(8,128)(2,1)S(1)}, u32[]{:S(2)}, u32[]{:S(2)}) async-start(bf16[16,8,2048]{2,1,0:T(8,128)(2,1)} %fusion.1), calls=%async_computation.8 | async-start | bytes 1048576 | tf_op jit(solution)/shard_map/all_to_all | solution.py:411
  (16 other events, 164.6 us)
where the time goes:
time: 324 us; the launch traced here: 320 us
  waiting for transfers between devices  104 us (32%)
  blocking collectives  85.7 us (26%)
  starting transfers between devices  57 us (18%)
  Pallas kernels  56.1 us (17%)
  local copies, waits for them, and re-layouts  10.7 us (3%)
  other arithmetic  6.87 us (2%)
    pallas_call x11, Pallas kernels, call(): pl.pallas_call(kernel, out_shape=out_shape, in_specs=specs, out_specs=out...  56.1 us
    all_to_all x3, waiting for transfers between devices, body(): lax.all_to_all(total.reshape(dests, TILE, width), ('z', 'c'), 0, 0, tiled...  28.6 us
    all_to_all x2, waiting for transfers between devices, body(): lax.all_to_all(piece.reshape(dests, TILE, width), ('z', 'c'), 0, 0, tiled...  25.1 us
    ppermute x3, waiting for transfers between devices, body(): back_one = lax.ppermute(add(out_one, via), 'tp', second)  21.3 us
    all_to_all x1, blocking collectives, body(): lax.all_to_all(merged.reshape(x_count, rows_own, width), 'x', 0, 0, tiled...  19.6 us
    all_to_all x1, blocking collectives, body(): lax.all_to_all(piece.reshape(dests, TILE, width), ('z', 'c'), 0, 0, tiled...  19.5 us
    all_to_all x1, blocking collectives, body(): lax.all_to_all(spread, 'x', 0, 0, tiled=True)  19.1 us
    all_to_all x3, starting transfers between devices, body(): lax.all_to_all(total.reshape(dests, TILE, width), ('z', 'c'), 0, 0, tiled...  16.7 us
  transfers between devices with their start and end apart: 25, of which 12 were waited for; matrix products, arithmetic and copies ran while one was open for 3% of the time, Pallas kernels for 10%

commit v1 on v0

--- a/solution.py
+++ b/solution.py
@@ -1,3 +1,4 @@
+import functools
 import math
 
 import jax
@@ -18,6 +19,7 @@
 CAP = 6
 TILE = 8
 WIDE = 128
+PIECES = 2
 
 rope_base = 10000.0
 group_eps = 1e-05
@@ -41,10 +43,10 @@
     return lax.broadcasted_iota(jnp.int32, shape, dim)
 
 
-def call(kernel, out_shape, *args, flops=0, smem=(), scratch=()):
+def call(kernel, out_shape, *args, flops=0, smem=(), far=(), scratch=(), room=24):
     moved = sum(math.prod(a.shape) * a.dtype.itemsize for a in args)
     specs = [
-        pl.BlockSpec(memory_space=pltpu.SMEM if i in smem else pltpu.VMEM)
+        pl.BlockSpec(memory_space=pltpu.SMEM if i in smem else pltpu.HBM if i in far else pltpu.VMEM)
         for i in range(len(args))
     ]
     multi = isinstance(out_shape, (list, tuple))
@@ -55,7 +57,7 @@
         in_specs=specs,
         out_specs=outs,
         scratch_shapes=list(scratch),
-        compiler_params=pltpu.CompilerParams(vmem_limit_bytes=56 * 1024 * 1024),
+        compiler_params=pltpu.CompilerParams(vmem_limit_bytes=room * 1024 * 1024),
         cost_estimate=pl.CostEstimate(flops=flops, bytes_accessed=moved, transcendentals=0),
     )(*args)
 
@@ -72,7 +74,7 @@
 
 
 def tables(cos_ref, sin_ref, base_ref):
-    cos_own, sin_own = cos_ref[...], sin_ref[...]
+    cos_own, sin_own = [jnp.concatenate([ref[...]] * 2, axis=1) for ref in (cos_ref, sin_ref)]
     cos_base, sin_base = base_ref[0:1, :], base_ref[1:2, :]
     cosine = cos_base * cos_own - sin_base * sin_own
     sine = sin_base * cos_own + cos_base * sin_own
@@ -141,7 +143,7 @@
         out_ref[j] = (state * jnp.exp(reach_ref[j, 0:1]) + before_ref[j]).astype(BF16)
 
 
-def inner_kernel(q_ref, k_ref, v_ref, decay_ref, cos_ref, sin_ref, base_ref, out_ref, lead_ref):
+def inner_kernel(q_ref, k_ref, v_ref, decay_ref, cos_ref, sin_ref, base_ref, out_ref, lead_ref, across_ref):
     rows, heads = decay_ref.shape
     cosine, sine = tables(cos_ref, sin_ref, base_ref)
     causal = iota((rows, rows), 0) >= iota((rows, rows), 1)
@@ -149,12 +151,16 @@
     parts = three_parts(decay_ref[...])
     cumulative = sum(dot(lower, part) for part in parts)
     across = sum(dot(part, lower, 0, 1) for part in parts)
-    for h in range(heads):
-        cols = slice(h * HEAD_DIM, (h + 1) * HEAD_DIM)
+    across_ref[...] = across
+    lane = iota((rows, heads), 1)
+
+    @pl.loop(0, heads)
+    def _(h):
+        cols = pl.ds(pl.multiple_of(h * HEAD_DIM, HEAD_DIM), HEAD_DIM)
         keys = turned(k_ref[:, cols].astype(F32), cosine, sine) * HEAD_DIM ** (-0.5)
         queries = turned(q_ref[:, cols].astype(F32), cosine, sine)
-        column = cumulative[:, h : h + 1]
-        gap = column - across[h : h + 1, :]
+        column = jnp.sum(jnp.where(lane == h, cumulative, 0.0), axis=1, keepdims=True)
+        gap = column - across_ref[pl.ds(h, 1), :]
         weights = jnp.where(causal, jnp.exp(jnp.minimum(gap, 0.0)), 0.0)
         scores = dot(queries.astype(BF16), keys.astype(BF16), 1, 1) * weights
         out_ref[:, cols] = dot(scores.astype(BF16), v_ref[:, cols])
@@ -162,9 +168,9 @@
 
 
 def mix_kernel(inner_ref, lead_ref, enter_ref, gate_ref, gain_ref, weight_ref, out_ref, hidden_ref):
-    heads = inner_ref.shape[1] // HEAD_DIM
-    for h in range(heads):
-        cols = slice(h * HEAD_DIM, (h + 1) * HEAD_DIM)
+    @pl.loop(0, inner_ref.shape[1] // HEAD_DIM)
+    def _(h):
+        cols = pl.ds(pl.multiple_of(h * HEAD_DIM, HEAD_DIM), HEAD_DIM)
         kept = inner_ref[:, cols] + dot(lead_ref[:, cols], enter_ref[cols, :])
         centred = kept - jnp.mean(kept, axis=-1, keepdims=True)
         variance = jnp.mean(centred * centred, axis=-1, keepdims=True)
@@ -172,6 +178,7 @@
         opened = gate / (1.0 + jnp.exp(-gate))
         scaled = centred * lax.rsqrt(variance + group_eps)
         hidden_ref[:, cols] = (scaled * gain_ref[:, cols] * opened).astype(BF16)
+
     step = 512
 
     @pl.loop(0, out_ref.shape[1] // step)
@@ -196,98 +203,151 @@
         table = table + jnp.where(routes_ref[:, k : k + 1] == expert, shares_ref[:, k : k + 1], 0.0)
     first = table.astype(BF16).astype(F32)
     noted = jnp.where(lane < WIDE // 2, first, table - first).astype(BF16)
-    for i in range(out_ref.shape[0]):
-        out_ref[i, :, 0:width] = scaled
-        out_ref[i, :, width : width + WIDE] = noted
+    out_ref[:, 0:width] = scaled
+    out_ref[:, width : width + WIDE] = noted
 
 
 def lane_of(dest, place, half):
     return (dest // 2) * 8 + place * 2 + dest % 2 + half * (WIDE // 2)
 
 
-def gather_kernel(place_ref, rows_ref, *refs):
-    out_refs, pick_ref = refs[:-1], refs[-1]
-    count = rows_ref.shape[0]
-    width = rows_ref.shape[1] - WIDE
-    block = count // 4
-    dests = 16
+def gather_kernel(chunk, place_ref, *refs):
+    blocks, out_ref = refs[:-1], refs[-1]
+    block = blocks[0].shape[0]
+    width = out_ref.shape[1]
+    dests = out_ref.shape[0] // TILE
     place = place_ref[0]
-    table = rows_ref[:, width : width + WIDE]
     choose = (iota((dests, WIDE), 1) == lane_of(iota((dests, WIDE), 0), place, 0)).astype(BF16)
-    named = (dot(choose, table, 1, 1) > 0.0).astype(F32)
-    early, late = iota((count, count), 0), iota((count, count), 1)
-    before = ((early < late) & (early // block == late // block)).astype(BF16)
-    rank = dot(named.astype(BF16), before).astype(jnp.int32)
-    slot = rank + CAP * (iota((dests, count), 1) // block)
-    slot = jnp.where(named > 0.0, slot, -1)
-    for c, out_ref in enumerate(out_refs):
-        line = iota((dests, TILE, count), 1) + c * TILE
-        pick = (slot[:, None, :] == line).astype(F32).reshape(dests * TILE, count).astype(BF16)
-        pick_ref[c * dests * TILE : (c + 1) * dests * TILE, :] = pick
+    earlier = (iota((block, block), 0) < iota((block, block), 1)).astype(BF16)
+    line = iota((dests, TILE, block), 1)
+    picks = []
+    for i, ref in enumerate(blocks):
+        named = (dot(choose, ref[:, width : width + WIDE], 1, 1) > 0.0).astype(F32)
+        slot = dot(named.astype(BF16), earlier).astype(jnp.int32) + (CAP * (chunk + i) - TILE * chunk)
+        slot = jnp.where(named > 0.0, slot, -1)
+        pick = (slot[:, None, :] == line).astype(F32).reshape(dests * TILE, block)
+        picks.append(pick.astype(BF16))
+    pick = jnp.concatenate(picks, axis=1)
     step = 256
 
     @pl.loop(0, width // step)
     def _(n):
         cols = pl.ds(pl.multiple_of(n * step, step), step)
-        chosen = dot(pick_ref[...], rows_ref[:, cols]).astype(BF16)
-        for c, out_ref in enumerate(out_refs):
-            out_ref[:, cols] = chosen[c * dests * TILE : (c + 1) * dests * TILE]
-
-
-def merge_kernel(place_ref, table_ref, *refs):
-    back_refs, out_ref, mix_refs = refs[:-3], refs[-3], refs[-2:]
-    count = table_ref.shape[0]
-    block = count // 4
-    dests = 16
+        rows = jnp.concatenate([ref[:, cols] for ref in blocks], axis=0)
+        out_ref[:, cols] = dot(pick, rows).astype(BF16)
+
+
+def merge_kernel(first_block, place_ref, *refs):
+    count = 2
+    tables, outs = refs[:count], refs[-count:]
+    backs = refs[count:-count]
+    block, dests = tables[0].shape[0], backs[0].shape[0] // TILE
     place = place_ref[0]
-    table = table_ref[...]
-    high, low = [
-        dot(table, (iota((WIDE, dests), 0) == lane_of(iota((WIDE, dests), 1), place, half)).astype(BF16))
-        for half in (0, 1)
-    ]
-    late, early = iota((count, count), 0), iota((count, count), 1)
-    before = ((early < late) & (early // block == late // block)).astype(BF16)
-    rank = dot(before, (high > 0.0).astype(F32).astype(BF16))
-    slot = rank + (CAP * (iota((count, dests), 0) // block)).astype(F32)
+    earlier = (iota((block, block), 1) < iota((block, block), 0)).astype(BF16)
     spread = (iota((dests, dests * TILE), 1) // TILE == iota((dests, dests * TILE), 0)).astype(BF16)
-    slot_wide = dot(slot.astype(BF16), spread).astype(jnp.int32)
-    high_wide, low_wide = dot(high.astype(BF16), spread), dot(low.astype(BF16), spread)
-    place_in = iota(slot_wide.shape, 1) % TILE
-    high_ref, low_ref = mix_refs
-    span = dests * TILE
-    for c in range(len(back_refs)):
-        here = slot_wide == place_in + c * TILE
-        high_ref[:, c * span : (c + 1) * span] = jnp.where(here, high_wide, 0.0).astype(BF16)
-        low_ref[:, c * span : (c + 1) * span] = jnp.where(here, low_wide, 0.0).astype(BF16)
+    place_in = iota((block, dests * TILE), 1) % TILE
+    mixes = []
+    for i, table_ref in enumerate(tables):
+        table = table_ref[...]
+        high, low = [
+            dot(table, (iota((WIDE, dests), 0) == lane_of(iota((WIDE, dests), 1), place, half)).astype(BF16))
+            for half in (0, 1)
+        ]
+        slot = dot(earlier, (high > 0.0).astype(F32).astype(BF16)) + CAP * (first_block + i)
+        slot_wide = dot(slot.astype(BF16), spread).astype(jnp.int32)
+        parts = [dot(part.astype(BF16), spread) for part in (high, low)]
+        chunk_base = first_block // 2
+        mixes.append(
+            [
+                jnp.concatenate(
+                    [
+                        jnp.where(slot_wide == place_in + (chunk_base + c) * TILE, part, 0.0).astype(BF16)
+                        for c in range(len(backs))
+                    ],
+                    axis=1,
+                )
+                for part in parts
+            ]
+        )
+    high = jnp.concatenate([pair[0] for pair in mixes], axis=0)
+    low = jnp.concatenate([pair[1] for pair in mixes], axis=0)
     step = 256
 
-    @pl.loop(0, out_ref.shape[1] // step)
+    @pl.loop(0, outs[0].shape[1] // step)
     def _(n):
         cols = pl.ds(pl.multiple_of(n * step, step), step)
-        piece = jnp.concatenate([ref[:, cols] for ref in back_refs], axis=0)
-        out_ref[:, cols] = (dot(high_ref[...], piece) + dot(low_ref[...], piece)).astype(BF16)
-
-
-def expert_kernel(own_ref, right_ref, left_ref, far_ref, gate_ref, up_ref, down_ref, *refs):
-    outs, (all_ref, act_ref) = refs[:-2], refs[-2:]
-    rows = own_ref.shape[0]
-    for i, ref in enumerate((own_ref, right_ref, left_ref, far_ref)):
+        piece = jnp.concatenate([ref[:, cols] for ref in backs], axis=0)
+        total = (dot(high, piece) + dot(low, piece)).astype(BF16)
+        for i, out_ref in enumerate(outs):
+            out_ref[:, cols] = total[i * block : (i + 1) * block]
+
+
+def expert_kernel(parts, *refs):
+    ins, (gate_ref, up_ref, down_ref) = refs[:parts], refs[parts : parts + 3]
+    outs = refs[parts + 3 : -6]
+    all_ref, act_ref, gate_in, up_in, down_in, sems = refs[-6:]
+    rows = ins[0].shape[0]
+    fetches = [
+        [
+            pltpu.make_async_copy(
+                source.at[0, pl.ds(j * (target.shape[0] // PIECES), target.shape[0] // PIECES)],
+                target.at[pl.ds(j * (target.shape[0] // PIECES), target.shape[0] // PIECES)],
+                sems.at[i, j],
+            )
+            for j in range(PIECES)
+        ]
+        for i, (source, target) in enumerate(((gate_ref, gate_in), (up_ref, up_in), (down_ref, down_in)))
+    ]
+    for group in fetches:
+        for fetch in group:
+            fetch.start()
+    for i, ref in enumerate(ins):
         all_ref[i * rows : (i + 1) * rows, :] = ref[...]
-    step = 256
-
-    @pl.loop(0, gate_ref.shape[1] // step)
+    for fetch in fetches[0]:
+        fetch.wait()
+    for fetch in fetches[1]:
+        fetch.wait()
+    half = 256
+
+    @pl.loop(0, gate_in.shape[1] // half)
+    def _(n):
+        cols = pl.ds(pl.multiple_of(n * half, half), half)
+        gate = jnp.minimum(dot(all_ref[...], gate_in[:, cols]), clamp_limit)
+        gate = gate / (1.0 + jnp.exp(-swish_alpha * gate))
+        up = jnp.clip(dot(all_ref[...], up_in[:, cols]), -clamp_limit, clamp_limit)
+        act_ref[:, cols] = ((up + 1.0) * gate).astype(BF16)
+
+    for fetch in fetches[2]:
+        fetch.wait()
+    step = 512
+
+    @pl.loop(0, down_in.shape[1] // step)
     def _(n):
         cols = pl.ds(pl.multiple_of(n * step, step), step)
-        gate = jnp.minimum(dot(all_ref[...], gate_ref[:, cols]), clamp_limit)
-        up = jnp.clip(dot(all_ref[...], up_ref[:, cols]), -clamp_limit, clamp_limit)
-        act_ref[:, cols] = ((up + 1.0) * (gate / (1.0 + jnp.exp(-swish_alpha * gate)))).astype(BF16)
-
-    @pl.loop(0, down_ref.shape[1] // step)
-    def _(n):
-        cols = pl.ds(pl.multiple_of(n * step, step), step)
-        part = dot(act_ref[...], down_ref[:, cols]).astype(BF16)
+        part = dot(act_ref[...], down_in[:, cols]).astype(BF16)
         for i, out_ref in enumerate(outs):
             out_ref[:, cols] = part[i * rows : (i + 1) * rows]
+
+
+def experts(rows, weights):
+    count, width = rows[0].shape
+    total, hidden = count * len(rows), weights[0].shape[2]
+    return call(
+        functools.partial(expert_kernel, len(rows)),
+        [shape((count, width))] * len(rows),
+        *rows, *weights,
+        flops=6 * total * width * hidden,
+        far=range(len(rows), len(rows) + 3),
+        room=56,
+        scratch=[
+            pltpu.VMEM((total, width), BF16),
+            pltpu.VMEM((total, hidden), BF16),
+            pltpu.VMEM((width, hidden), BF16),
+            pltpu.VMEM((width, hidden), BF16),
+            pltpu.VMEM((hidden, width), BF16),
+            pltpu.SemaphoreType.DMA((3, PIECES)),
+        ],
+    )
 
 
 def ring(size, shift):
@@ -322,9 +382,8 @@
     sp_index = lax.axis_index(SP)
 
     inverse = rope_base ** (-np.arange(HALF, dtype=np.float64) / HALF)
-    inverse = np.concatenate([inverse, inverse])
     inside = np.arange(tok_count, dtype=np.float64)[:, None] * inverse[None]
-    starts = (np.arange(sp_count, dtype=np.float64) * tok_count)[:, None] * inverse[None]
+    starts = (np.arange(sp_count, dtype=np.float64) * tok_count)[:, None] * np.tile(inverse, 2)[None]
     cos_own, sin_own = jnp.asarray(np.cos(inside), F32), jnp.asarray(np.sin(inside), F32)
     base_all = jnp.asarray(np.stack([np.cos(starts), np.sin(starts)], axis=1), F32)
     base = lax.dynamic_index_in_dim(base_all, sp_index, 0, keepdims=False)
@@ -344,6 +403,7 @@
         [shape((tok_count, local), F32), shape((tok_count, local))],
         query_rows, key_rows, value_rows, log_decay, cos_own, sin_own, base,
         flops=4 * tok_count * tok_count * local,
+        scratch=[pltpu.VMEM((heads, tok_count), F32)],
     )
     before, reach, group = call(
         group_kernel,
@@ -367,59 +427,63 @@
     )
     pieces = lax.all_to_all(mixed.reshape(tp_count, rows_own, width), "tp", 0, 0, tiled=True)
     own_routes = lax.dynamic_slice_in_dim(routes, lax.axis_index("tp") * rows_own, rows_own, 0)
+    updated, extended = call(
+        norm_kernel,
+        [shape((rows_own, width), F32), shape((rows_own, width + WIDE))],
+        pieces, residual, ffn_gain.reshape(1, width), own_routes, route_weights,
+    )
+
+    place = lax.axis_index("x").astype(jnp.int32).reshape(1)
     x_count = lax.axis_size("x")
-    updated, spread = call(
-        norm_kernel,
-        [shape((rows_own, width), F32), shape((x_count, rows_own, width + WIDE))],
-        pieces, residual, ffn_gain.reshape(1, width), own_routes, route_weights,
-    )
-
-    place = lax.axis_index("x").astype(jnp.int32).reshape(1)
-    near = lax.all_to_all(spread, "x", 0, 0, tiled=True).reshape(x_count * rows_own, width + WIDE)
+    shifts = range(x_count)
+    near = [extended]
+    for d in shifts[1:]:
+        near.append(lax.ppermute(extended, "x", ring(x_count, -d)))
     dests = sp_count // x_count
     chunks = x_count * CAP // TILE
-    outgoing = call(
-        gather_kernel,
-        [shape((dests * TILE, width))] * chunks,
-        place, near,
-        flops=2 * chunks * dests * TILE * near.shape[0] * width,
-        smem=(0,),
-        scratch=[pltpu.VMEM((chunks * dests * TILE, near.shape[0]), BF16)],
-    )
-    gate_part, up_part, down_part = gate_weight[0], up_weight[0], down_weight[0]
+    outgoing = []
+    for c in range(chunks):
+        outgoing.append(
+            call(
+                functools.partial(gather_kernel, c),
+                shape((dests * TILE, width)),
+                place, near[c], near[c + 1],
+                flops=4 * dests * TILE * rows_own * width,
+                smem=(0,),
+            )
+        )
+    weights = gate_weight, up_weight, down_weight
     ahead, behind = ring(tp_count, 1), ring(tp_count, -1)
     returned = []
     for c, piece in enumerate(outgoing, 1):
         first, second = (ahead, behind) if c % 2 else (behind, ahead)
         own = lax.all_to_all(piece.reshape(dests, TILE, width), ("z", "c"), 0, 0, tiled=True)
         own = own.reshape(dests * TILE, width)
-        rows = own.shape[0]
         one = lax.ppermute(own, "tp", first)
         two = lax.ppermute(own, "tp", second)
         far = lax.ppermute(one, "tp", first)
-        out_own, out_one, out_two, out_far = call(
-            expert_kernel,
-            [shape((rows, width))] * 4,
-            own, one, two, far, gate_part, up_part, down_part,
-            flops=6 * 4 * rows * width * gate_part.shape[1],
-            scratch=[pltpu.VMEM((4 * rows, width), BF16), pltpu.VMEM((4 * rows, gate_part.shape[1]), BF16)],
-        )
+        out_own, out_one, out_two = experts([own, one, two], weights)
+        (out_far,) = experts([far], weights)
         via = lax.ppermute(out_far, "tp", second)
         back_one = lax.ppermute(add(out_one, via), "tp", second)
         back_two = lax.ppermute(out_two, "tp", first)
         total = (out_own.astype(F32) + back_one.astype(F32) + back_two.astype(F32)).astype(BF16)
         back = lax.all_to_all(total.reshape(dests, TILE, width), ("z", "c"), 0, 0, tiled=True)
         returned.append(back.reshape(dests * TILE, width))
-    merged = call(
-        merge_kernel,
-        shape((x_count * rows_own, width)),
-        place, near[:, width:], *returned,
-        flops=4 * chunks * dests * TILE * near.shape[0] * width,
-        smem=(0,),
-        scratch=[pltpu.VMEM((near.shape[0], chunks * dests * TILE), BF16)] * 2,
-    )
-    parts = lax.all_to_all(merged.reshape(x_count, rows_own, width), "x", 0, 0, tiled=True)
-    return (updated + jnp.sum(parts.astype(F32), axis=0)).astype(BF16)
+    tables = [rows[:, width:] for rows in near]
+    merged = []
+    for i in range(2):
+        merged += call(
+            functools.partial(merge_kernel, 2 * i),
+            [shape((rows_own, width))] * 2,
+            place, tables[2 * i], tables[2 * i + 1], returned[i], returned[i + 1],
+            flops=8 * dests * TILE * rows_own * width,
+            smem=(0,),
+        )
+    total = updated + merged[0].astype(F32)
+    for d in shifts[1:]:
+        total = total + lax.ppermute(merged[d], "x", ring(x_count, d)).astype(F32)
+    return total.astype(BF16)
 
 
 def solution(mesh):

time: 324 us -> 321 us (level)
  blocking collectives: 85.7 us -> 27 us
  waiting for transfers between devices: 104 us -> 148 us
  Pallas kernels: 56.1 us -> 62 us
    all_to_all x3 -> x0, blocking collectives: 58.1 us -> none  [the longest x1 19.6 us: body(): lax.all_to_all(merged.reshape(x_count, rows_own, width), 'x', 0, 0, tiled...]
    ppermute x0 -> x6, waiting for transfers between devices: none -> 33.9 us  [the longest x3 20.3 us: body(): near.append(lax.ppermute(extended, 'x', ring(x_count, -d)))]
    ppermute x3, waiting for transfers between devices: 21.3 us -> 0.01 us  [body(): back_one = lax.ppermute(add(out_one, via), 'tp', second)]
    ppermute x3, waiting for transfers between devices: 0.01 us -> 15.2 us  [body(): one = lax.ppermute(own, 'tp', first)]
    ppermute x3, waiting for transfers between devices: 13.2 us -> 22 us  [body(): far = lax.ppermute(one, 'tp', first)]
    all_to_all x3, waiting for transfers between devices: 28.6 us -> 37.1 us  [body(): lax.all_to_all(total.reshape(dests, TILE, width), ('z', 'c'), 0, 0, tiled...]
    ppermute x0 -> x6, starting transfers between devices: none -> 7.77 us  [the longest x3 4.32 us: body(): near.append(lax.ppermute(extended, 'x', ring(x_count, -d)))]
    all_to_all x2 -> x3, waiting for transfers between devices: 25.1 us -> 17.6 us  [body(): lax.all_to_all(piece.reshape(dests, TILE, width), ('z', 'c'), 0, 0, tiled...]
  transfers between devices with their start and end apart: 25 -> 32, of which waited for: 12 -> 20; matrix products, arithmetic and copies ran while one was open for 3% -> 3% of each run, Pallas kernels for 10% -> 17%
where the time goes in v1:
time: 321 us; the launch traced here: 318 us
  waiting for transfers between devices  148 us (46%)
  Pallas kernels  62 us (19%)
  starting transfers between devices  58.8 us (18%)
  blocking collectives  27 us (8%)
  local copies, waits for them, and re-layouts  12.6 us (4%)
  other arithmetic  8.99 us (3%)
    pallas_call x17, Pallas kernels, call(): pl.pallas_call(kernel, out_shape=out_shape, in_specs=specs, out_specs=out...  62 us
    all_to_all x3, waiting for transfers between devices, body(): lax.all_to_all(total.reshape(dests, TILE, width), ('z', 'c'), 0, 0, tiled...  37.1 us
    ppermute x3, waiting for transfers between devices, body(): far = lax.ppermute(one, 'tp', first)  22 us
    ppermute x3, waiting for transfers between devices, body(): near.append(lax.ppermute(extended, 'x', ring(x_count, -d)))  20.3 us
    all_to_all x3, waiting for transfers between devices, body(): lax.all_to_all(piece.reshape(dests, TILE, width), ('z', 'c'), 0, 0, tiled...  17.6 us
    all_to_all x1, blocking collectives, body(): groups = lax.all_to_all(group, 'z', 0, 0, tiled=True)  17.5 us
    all_to_all x3, starting transfers between devices, body(): lax.all_to_all(total.reshape(dests, TILE, width), ('z', 'c'), 0, 0, tiled...  15.5 us
    ppermute x3, waiting for transfers between devices, body(): one = lax.ppermute(own, 'tp', first)  15.2 us
  transfers between devices with their start and end apart: 32, of which 20 were waited for; matrix products, arithmetic and copies ran while one was open for 3% of the time, Pallas kernels for 17%

profile of v1, /device:TPU:2, one launch (start us, length us, event | category | flops | bytes accessed | tf_op | source)
XLA Modules:
  0.0 318.1 jit_solution(16380639930250832419)
XLA Ops:
  6.2 9.5 %all_to_all.50.in_ref = bf16[8,72,128]{2,1,0:T(8,128)(2,1)S(1)} all-to-all(bf16[8,72,128]{2,1,0:T(8,128)(2,1)S(1)} %shard_map.164), channel_id=1, replica_groups=mesh['z'=8,'x'=4,'c'=2,'tp'=4] {'x','c'}, dimensions={0} | all-to-all | bytes 294912 | tf_op jit(solution)/shard_map/all_to_all | solution.py:400
  15.7 17.5 %all_to_all.51.in_ref = bf16[8,72,128]{2,1,0:T(8,128)(2,1)S(1)} all-to-all(bf16[8,72,128]{2,1,0:T(8,128)(2,1)S(1)} %get-tuple-element.27), channel_id=1, replica_groups=mesh['z'=8,'x'=4,'c'=2,'tp'=4] {'z'}, dimensions={0} | all-to-all | bytes 294912 | tf_op jit(solution)/shard_map/all_to_all | solution.py:413
  33.9 4.7 %all-to-all-start.2 = ((bf16[8,64,128]{2,1,0:T(8,128)(2,1)}), bf16[8,64,128]{2,1,0:T(8,128)(2,1)S(1)}, u32[]{:S(2)}, u32[]{:S(2)}) async-start(bf16[8,64,128]{2,1,0:T(8,128)(2,1)} %shard_map.166), calls=%async_computation.2 | async-start | bytes 262144 | tf_op jit(solution)/shard_map/all_to_all | solution.py:420
  45.3 3.6 %shard_map.167 = bf16[256,2048]{1,0:T(8,128)(2,1)} custom-call(f32[256,512]{1,0:T(8,128)S(1)} %get-tuple-element.25.inner_ref, bf16[256,512]{1,0:T(8,128)(2,1)S(1)} %copy-done.14, bf16[512,128]{1,0:T(8,128)(2,1)S(1)} %bitcast.27, bf16[256,512]{1,0:T(8,128)(2,1)S(1)} %copy-done.12, f32[1,512]{1,0:T(1,128)S(1)} %bitcast.29, bf16[512,2048]{1,0:T(8,128)(2,1)S(1)} %copy-done.1), custom_call_target="tpu_custom_call" | custom-call | flops 536870912 | bytes 3278848 | tf_op jit(solution)/shard_map/pallas_call | solution.py:54
  48.8 4.6 %all-to-all-start.3 = ((bf16[4,64,2048]{2,1,0:T(8,128)(2,1)}), bf16[4,64,2048]{2,1,0:T(8,128)(2,1)S(1)}, u32[]{:S(2)}, u32[]{:S(2)}) async-start(bf16[4,64,2048]{2,1,0:T(8,128)(2,1)} %bitcast.4), calls=%async_computation.3 | async-start | bytes 2097152 | tf_op jit(solution)/shard_map/all_to_all | solution.py:428
  53.7 15.0 %all-to-all-done.3.sum_ref = bf16[4,64,2048]{2,1,0:T(8,128)(2,1)S(1)} async-done(((bf16[4,64,2048]{2,1,0:T(8,128)(2,1)}), bf16[4,64,2048]{2,1,0:T(8,128)(2,1)S(1)}, u32[]{:S(2)}, u32[]{:S(2)}) %all-to-all-start.3) | async-done | bytes 1048608 | tf_op jit(solution)/shard_map/all_to_all | solution.py:428
  72.7 7.5 %collective-permute-done.7.refs_1_.refs_0_ = bf16[64,2176]{1,0:T(8,128)(2,1)S(1)} collective-permute-done((bf16[64,2176]{1,0:T(8,128)(2,1)S(1)}, bf16[64,2176]{1,0:T(8,128)(2,1)S(1)}, u32[]{:S(2)}, u32[]{:S(2)}) %collective-permute-start.7) | collective-permute-done | bytes 278560 | tf_op jit(solution)/shard_map/ppermute | solution.py:441
  80.2 3.9 %collective-permute-done.refs_1_.refs_0_ = bf16[64,2176]{1,0:T(8,128)(2,1)S(1)} collective-permute-done((bf16[64,2176]{1,0:T(8,128)(2,1)S(1)}, bf16[64,2176]{1,0:T(8,128)(2,1)S(1)}, u32[]{:S(2)}, u32[]{:S(2)}) %collective-permute-start) | collective-permute-done | bytes 278560 | tf_op jit(solution)/shard_map/ppermute | solution.py:441
  86.6 3.6 %all-to-all-start.6 = ((bf16[16,8,2048]{2,1,0:T(8,128)(2,1)}), bf16[16,8,2048]{2,1,0:T(8,128)(2,1)S(1)}, u32[]{:S(2)}, u32[]{:S(2)}) async-start(bf16[16,8,2048]{2,1,0:T(8,128)(2,1)} %bitcast.11), calls=%async_computation.6 | async-start | bytes 1048576 | tf_op jit(solution)/shard_map/all_to_all | solution.py:460
  92.7 13.4 %all-to-all-done.6 = bf16[16,8,2048]{2,1,0:T(8,128)(2,1)S(1)} async-done(((bf16[16,8,2048]{2,1,0:T(8,128)(2,1)}), bf16[16,8,2048]{2,1,0:T(8,128)(2,1)S(1)}, u32[]{:S(2)}, u32[]{:S(2)}) %all-to-all-start.6) | async-done | bytes 524320 | tf_op jit(solution)/shard_map/all_to_all | solution.py:460
  106.1 4.2 %all-to-all-start.4 = ((bf16[16,8,2048]{2,1,0:T(8,128)(2,1)}), bf16[16,8,2048]{2,1,0:T(8,128)(2,1)S(1)}, u32[]{:S(2)}, u32[]{:S(2)}) async-start(bf16[16,8,2048]{2,1,0:T(8,128)(2,1)} %bitcast.7), calls=%async_computation.4 | async-start | bytes 1048576 | tf_op jit(solution)/shard_map/all_to_all | solution.py:460
  111.0 8.9 %collective-permute-done.15.refs_1_ = bf16[64,2176]{1,0:T(8,128)(2,1)S(1)} collective-permute-done((bf16[64,2176]{1,0:T(8,128)(2,1)S(1)}, bf16[64,2176]{1,0:T(8,128)(2,1)S(1)}, u32[]{:S(2)}, u32[]{:S(2)}) %collective-permute-start.15) | collective-permute-done | bytes 278560 | tf_op jit(solution)/shard_map/ppermute | solution.py:441
  122.4 4.0 %all-to-all-done.4 = bf16[16,8,2048]{2,1,0:T(8,128)(2,1)S(1)} async-done(((bf16[16,8,2048]{2,1,0:T(8,128)(2,1)}), bf16[16,8,2048]{2,1,0:T(8,128)(2,1)S(1)}, u32[]{:S(2)}, u32[]{:S(2)}) %all-to-all-start.4) | async-done | bytes 524320 | tf_op jit(solution)/shard_map/all_to_all | solution.py:460
  126.5 4.3 %all-to-all-start.8 = ((bf16[16,8,2048]{2,1,0:T(8,128)(2,1)}), bf16[16,8,2048]{2,1,0:T(8,128)(2,1)}, u32[]{:S(2)}, u32[]{:S(2)}) async-start(bf16[16,8,2048]{2,1,0:T(8,128)(2,1)} %bitcast.15), calls=%async_computation.8 | async-start | bytes 1048576 | tf_op jit(solution)/shard_map/all_to_all | solution.py:460
  134.1 12.5 %collective-permute-done.1.refs_1_ = bf16[128,2048]{1,0:T(8,128)(2,1)} collective-permute-done((bf16[128,2048]{1,0:T(8,128)(2,1)S(1)}, bf16[128,2048]{1,0:T(8,128)(2,1)}, u32[]{:S(2)}, u32[]{:S(2)}) %collective-permute-start.1) | collective-permute-done | bytes 524320 | tf_op jit(solution)/shard_map/ppermute | solution.py:462
  146.7 3.1 collective-permute-start.17
  149.8 8.3 %shard_map.170 = (bf16[128,2048]{1,0:T(8,128)(2,1)}, bf16[128,2048]{1,0:T(8,128)(2,1)}, bf16[128,2048]{1,0:T(8,128)(2,1)}) custom-call(bf16[128,2048]{1,0:T(8,128)(2,1)} %bitcast.35, bf16[128,2048]{1,0:T(8,128)(2,1)} %collective-permute-done.1.refs_1_, bf16[128,2048]{1,0:T(8,128)(2,1)} %collective-permute-done.2.refs_2_, bf16[1,2048,512]{2,1,0:T(8,128)(2,1)} %refs_1_.5, ...), custom_call_target="tpu_custom_call" | custom-call | flops 2415919104 | bytes 7864320 | tf_op jit(solution)/shard_map/pallas_call | solution.py:54
  163.6 6.0 %shard_map.171 = bf16[128,2048]{1,0:T(8,128)(2,1)} custom-call(bf16[128,2048]{1,0:T(8,128)(2,1)} %copy-done.18, bf16[1,2048,512]{2,1,0:T(8,128)(2,1)} %refs_1_.5, bf16[1,2048,512]{2,1,0:T(8,128)(2,1)} %refs_2_.5, bf16[1,512,2048]{2,1,0:T(8,128)(2,1)} %refs_3_.11), custom_call_target="tpu_custom_call" | custom-call | flops 805306368 | bytes 6815744 | tf_op jit(solution)/shard_map/pallas_call | solution.py:54
  169.6 4.5 %collective-permute-done.9.refs_2_ = bf16[128,2048]{1,0:T(8,128)(2,1)} collective-permute-done((bf16[128,2048]{1,0:T(8,128)(2,1)S(1)}, bf16[128,2048]{1,0:T(8,128)(2,1)}, u32[]{:S(2)}, u32[]{:S(2)}) %collective-permute-start.9) | collective-permute-done | bytes 524320 | tf_op jit(solution)/shard_map/ppermute | solution.py:463
  174.1 8.3 %shard_map.173 = (bf16[128,2048]{1,0:T(8,128)(2,1)}, bf16[128,2048]{1,0:T(8,128)(2,1)}, bf16[128,2048]{1,0:T(8,128)(2,1)}) custom-call(bf16[128,2048]{1,0:T(8,128)(2,1)} %bitcast.32, bf16[128,2048]{1,0:T(8,128)(2,1)} %collective-permute-done.8.refs_1_, bf16[128,2048]{1,0:T(8,128)(2,1)} %collective-permute-done.9.refs_2_, bf16[1,2048,512]{2,1,0:T(8,128)(2,1)} %refs_1_.5, ...), custom_call_target="tpu_custom_call" | custom-call | flops 2415919104 | bytes 7864320 | tf_op jit(solution)/shard_map/pallas_call | solution.py:54
  186.1 8.2 %shard_map.177 = (bf16[128,2048]{1,0:T(8,128)(2,1)}, bf16[128,2048]{1,0:T(8,128)(2,1)}, bf16[128,2048]{1,0:T(8,128)(2,1)}) custom-call(bf16[128,2048]{1,0:T(8,128)(2,1)} %bitcast.16.refs_0_, bf16[128,2048]{1,0:T(8,128)(2,1)} %copy-done.27, bf16[128,2048]{1,0:T(8,128)(2,1)} %copy-done.28, bf16[1,2048,512]{2,1,0:T(8,128)(2,1)} %refs_1_.5, ...), custom_call_target="tpu_custom_call" | custom-call | flops 2415919104 | bytes 7864320 | tf_op jit(solution)/shard_map/pallas_call | solution.py:54
  195.8 6.0 %shard_map.174 = bf16[128,2048]{1,0:T(8,128)(2,1)} custom-call(bf16[128,2048]{1,0:T(8,128)(2,1)} %copy-done.17, bf16[1,2048,512]{2,1,0:T(8,128)(2,1)} %refs_1_.5, bf16[1,2048,512]{2,1,0:T(8,128)(2,1)} %refs_2_.5, bf16[1,512,2048]{2,1,0:T(8,128)(2,1)} %refs_3_.11), custom_call_target="tpu_custom_call" | custom-call | flops 805306368 | bytes 6815744 | tf_op jit(solution)/shard_map/pallas_call | solution.py:54
  202.8 19.1 %collective-permute-done.18.refs_0_ = bf16[128,2048]{1,0:T(8,128)(2,1)S(1)} collective-permute-done((bf16[128,2048]{1,0:T(8,128)(2,1)}, bf16[128,2048]{1,0:T(8,128)(2,1)S(1)}, u32[]{:S(2)}, u32[]{:S(2)}) %collective-permute-start.18) | collective-permute-done | bytes 524320 | tf_op jit(solution)/shard_map/ppermute | solution.py:464
  222.7 6.0 %shard_map.178 = bf16[128,2048]{1,0:T(8,128)(2,1)} custom-call(bf16[128,2048]{1,0:T(8,128)(2,1)} %copy-done.19, bf16[1,2048,512]{2,1,0:T(8,128)(2,1)} %refs_1_.5, bf16[1,2048,512]{2,1,0:T(8,128)(2,1)} %refs_2_.5, bf16[1,512,2048]{2,1,0:T(8,128)(2,1)} %refs_3_.11), custom_call_target="tpu_custom_call" | custom-call | flops 805306368 | bytes 6815744 | tf_op jit(solution)/shard_map/pallas_call | solution.py:54
  234.9 7.3 %all-to-all-start.5 = ((bf16[16,8,2048]{2,1,0:T(8,128)(2,1)}), bf16[16,8,2048]{2,1,0:T(8,128)(2,1)S(1)}, u32[]{:S(2)}, u32[]{:S(2)}) async-start(bf16[16,8,2048]{2,1,0:T(8,128)(2,1)} %fusion), calls=%async_computation.5 | async-start | bytes 1048576 | tf_op jit(solution)/shard_map/all_to_all | solution.py:471
  248.1 10.1 %all-to-all-done.5 = bf16[16,8,2048]{2,1,0:T(8,128)(2,1)S(1)} async-done(((bf16[16,8,2048]{2,1,0:T(8,128)(2,1)}), bf16[16,8,2048]{2,1,0:T(8,128)(2,1)S(1)}, u32[]{:S(2)}, u32[]{:S(2)}) %all-to-all-start.5) | async-done | bytes 524320 | tf_op jit(solution)/shard_map/all_to_all | solution.py:471
  258.1 4.2 %all-to-all-start.7 = ((bf16[16,8,2048]{2,1,0:T(8,128)(2,1)}), bf16[16,8,2048]{2,1,0:T(8,128)(2,1)S(1)}, u32[]{:S(2)}, u32[]{:S(2)}) async-start(bf16[16,8,2048]{2,1,0:T(8,128)(2,1)} %fusion.1), calls=%async_computation.7 | async-start | bytes 1048576 | tf_op jit(solution)/shard_map/all_to_all | solution.py:471
  264.8 13.7 %all-to-all-done.7 = bf16[16,8,2048]{2,1,0:T(8,128)(2,1)S(1)} async-done(((bf16[16,8,2048]{2,1,0:T(8,128)(2,1)}), bf16[16,8,2048]{2,1,0:T(8,128)(2,1)S(1)}, u32[]{:S(2)}, u32[]{:S(2)}) %all-to-all-start.7) | async-done | bytes 524320 | tf_op jit(solution)/shard_map/all_to_all | solution.py:471
  278.5 4.0 %all-to-all-start.9 = ((bf16[16,8,2048]{2,1,0:T(8,128)(2,1)}), bf16[16,8,2048]{2,1,0:T(8,128)(2,1)S(1)}, u32[]{:S(2)}, u32[]{:S(2)}) async-start(bf16[16,8,2048]{2,1,0:T(8,128)(2,1)} %fusion.2), calls=%async_computation.9 | async-start | bytes 1048576 | tf_op jit(solution)/shard_map/all_to_all | solution.py:471
  285.4 13.3 %all-to-all-done.9 = bf16[16,8,2048]{2,1,0:T(8,128)(2,1)S(1)} async-done(((bf16[16,8,2048]{2,1,0:T(8,128)(2,1)}), bf16[16,8,2048]{2,1,0:T(8,128)(2,1)S(1)}, u32[]{:S(2)}, u32[]{:S(2)}) %all-to-all-start.9) | async-done | bytes 524320 | tf_op jit(solution)/shard_map/all_to_all | solution.py:471
  303.6 7.6 %collective-permute-done.22 = bf16[64,2048]{1,0:T(8,128)(2,1)S(1)} collective-permute-done((bf16[64,2048]{1,0:T(8,128)(2,1)S(1)}, bf16[64,2048]{1,0:T(8,128)(2,1)S(1)}, u32[]{:S(2)}, u32[]{:S(2)}) %collective-permute-start.22) | collective-permute-done | bytes 262176 | tf_op jit(solution)/shard_map/ppermute | solution.py:485
  311.2 6.0 %collective-permute-done.23 = bf16[64,2048]{1,0:T(8,128)(2,1)S(1)} collective-permute-done((bf16[64,2048]{1,0:T(8,128)(2,1)S(1)}, bf16[64,2048]{1,0:T(8,128)(2,1)S(1)}, u32[]{:S(2)}, u32[]{:S(2)}) %collective-permute-start.23) | collective-permute-done | bytes 262176 | tf_op jit(solution)/shard_map/ppermute | solution.py:485
  (125 shorter events, 64.9 us)
Async XLA Ops:
  33.9 9.4 %all-to-all-start.2 = ((bf16[8,64,128]{2,1,0:T(8,128)(2,1)}), bf16[8,64,128]{2,1,0:T(8,128)(2,1)S(1)}, u32[]{:S(2)}, u32[]{:S(2)}) async-start(bf16[8,64,128]{2,1,0:T(8,128)(2,1)} %shard_map.166), calls=%async_computation.2 | async-start | bytes 262144 | tf_op jit(solution)/shard_map/all_to_all | solution.py:420
  48.8 19.9 %all-to-all-start.3 = ((bf16[4,64,2048]{2,1,0:T(8,128)(2,1)}), bf16[4,64,2048]{2,1,0:T(8,128)(2,1)S(1)}, u32[]{:S(2)}, u32[]{:S(2)}) async-start(bf16[4,64,2048]{2,1,0:T(8,128)(2,1)} %bitcast.4), calls=%async_computation.3 | async-start | bytes 2097152 | tf_op jit(solution)/shard_map/all_to_all | solution.py:428
  69.1 11.1 %collective-permute-start.7 = (bf16[64,2176]{1,0:T(8,128)(2,1)S(1)}, bf16[64,2176]{1,0:T(8,128)(2,1)S(1)}, u32[]{:S(2)}, u32[]{:S(2)}) collective-permute-start(bf16[64,2176]{1,0:T(8,128)(2,1)S(1)} %get-tuple-element.31.refs_0_), channel_id=1, source_target_pairs={{0,16},{8,24},{16,0},{24,8},{1,17},{9,25},{17,1},{25,9},{2,18},{10... | collective-permute-start | bytes 835592 | tf_op jit(solution)/shard_map/ppermute | solution.py:441
  71.3 12.8 %collective-permute-start = (bf16[64,2176]{1,0:T(8,128)(2,1)S(1)}, bf16[64,2176]{1,0:T(8,128)(2,1)S(1)}, u32[]{:S(2)}, u32[]{:S(2)}) collective-permute-start(bf16[64,2176]{1,0:T(8,128)(2,1)S(1)} %get-tuple-element.31.refs_0_), channel_id=1, source_target_pairs={{0,24},{8,0},{16,8},{24,16},{1,25},{9,1},{17,9},{25,17},{2,26},{10... | collective-permute-start | bytes 835592 | tf_op jit(solution)/shard_map/ppermute | solution.py:441
  86.6 19.5 %all-to-all-start.6 = ((bf16[16,8,2048]{2,1,0:T(8,128)(2,1)}), bf16[16,8,2048]{2,1,0:T(8,128)(2,1)S(1)}, u32[]{:S(2)}, u32[]{:S(2)}) async-start(bf16[16,8,2048]{2,1,0:T(8,128)(2,1)} %bitcast.11), calls=%async_computation.6 | async-start | bytes 1048576 | tf_op jit(solution)/shard_map/all_to_all | solution.py:460
  106.1 20.4 %all-to-all-start.4 = ((bf16[16,8,2048]{2,1,0:T(8,128)(2,1)}), bf16[16,8,2048]{2,1,0:T(8,128)(2,1)S(1)}, u32[]{:S(2)}, u32[]{:S(2)}) async-start(bf16[16,8,2048]{2,1,0:T(8,128)(2,1)} %bitcast.7), calls=%async_computation.4 | async-start | bytes 1048576 | tf_op jit(solution)/shard_map/all_to_all | solution.py:460
  110.3 9.6 %collective-permute-start.15 = (bf16[64,2176]{1,0:T(8,128)(2,1)S(1)}, bf16[64,2176]{1,0:T(8,128)(2,1)S(1)}, u32[]{:S(2)}, u32[]{:S(2)}) collective-permute-start(bf16[64,2176]{1,0:T(8,128)(2,1)S(1)} %get-tuple-element.31.refs_0_), channel_id=1, source_target_pairs={{0,8},{8,16},{16,24},{24,0},{1,9},{9,17},{17,25},{25,1},{2,10},{10... | collective-permute-start | bytes 835592 | tf_op jit(solution)/shard_map/ppermute | solution.py:441
  126.5 20.3 %all-to-all-start.8 = ((bf16[16,8,2048]{2,1,0:T(8,128)(2,1)}), bf16[16,8,2048]{2,1,0:T(8,128)(2,1)}, u32[]{:S(2)}, u32[]{:S(2)}) async-start(bf16[16,8,2048]{2,1,0:T(8,128)(2,1)} %bitcast.15), calls=%async_computation.8 | async-start | bytes 1048576 | tf_op jit(solution)/shard_map/all_to_all | solution.py:460
  130.7 15.8 %collective-permute-start.1 = (bf16[128,2048]{1,0:T(8,128)(2,1)S(1)}, bf16[128,2048]{1,0:T(8,128)(2,1)}, u32[]{:S(2)}, u32[]{:S(2)}) collective-permute-start(bf16[128,2048]{1,0:T(8,128)(2,1)S(1)} %bitcast.33), channel_id=1, source_target_pairs={{0,1},{1,2},{2,3},{3,0},{4,5},{5,6},{6,7},{7,4},{8,9},{9,10},{10,1... | collective-permute-start | bytes 1572872 | tf_op jit(solution)/shard_map/ppermute | solution.py:462
  131.4 18.4 %collective-permute-start.2 = (bf16[128,2048]{1,0:T(8,128)(2,1)S(1)}, bf16[128,2048]{1,0:T(8,128)(2,1)}, u32[]{:S(2)}, u32[]{:S(2)}) collective-permute-start(bf16[128,2048]{1,0:T(8,128)(2,1)S(1)} %bitcast.34), channel_id=1, source_target_pairs={{0,3},{1,0},{2,1},{3,2},{4,7},{5,4},{6,5},{7,6},{8,11},{9,8},{10,9... | collective-permute-start | bytes 1572872 | tf_op jit(solution)/shard_map/ppermute | solution.py:463
  134.0 24.1 %collective-permute-start.8 = (bf16[128,2048]{1,0:T(8,128)(2,1)S(1)}, bf16[128,2048]{1,0:T(8,128)(2,1)}, u32[]{:S(2)}, u32[]{:S(2)}) collective-permute-start(bf16[128,2048]{1,0:T(8,128)(2,1)S(1)} %bitcast.30), channel_id=1, source_target_pairs={{0,3},{1,0},{2,1},{3,2},{4,7},{5,4},{6,5},{7,6},{8,11},{9,8},{10,9... | collective-permute-start | bytes 1572872 | tf_op jit(solution)/shard_map/ppermute | solution.py:462
  146.5 16.2 %collective-permute-start.3 = (bf16[128,2048]{1,0:T(8,128)(2,1)}, bf16[128,2048]{1,0:T(8,128)(2,1)S(1)}, u32[]{:S(2)}, u32[]{:S(2)}) collective-permute-start(bf16[128,2048]{1,0:T(8,128)(2,1)} %collective-permute-done.1.refs_1_), channel_id=1, source_target_pairs={{0,1},{1,2},{2,3},{3,0},{4,5},{5,6},{6,7},{7,4},{8,9},{9,10},{10,1... | collective-permute-start | bytes 1572872 | tf_op jit(solution)/shard_map/ppermute | solution.py:464
  146.5 27.6 %collective-permute-start.9 = (bf16[128,2048]{1,0:T(8,128)(2,1)S(1)}, bf16[128,2048]{1,0:T(8,128)(2,1)}, u32[]{:S(2)}, u32[]{:S(2)}) collective-permute-start(bf16[128,2048]{1,0:T(8,128)(2,1)S(1)} %bitcast.31), channel_id=1, source_target_pairs={{0,1},{1,2},{2,3},{3,0},{4,5},{5,6},{6,7},{7,4},{8,9},{9,10},{10,1... | collective-permute-start | bytes 1572872 | tf_op jit(solution)/shard_map/ppermute | solution.py:463
  146.7 35.7 %collective-permute-start.17 = (bf16[128,2048]{1,0:T(8,128)(2,1)}, bf16[128,2048]{1,0:T(8,128)(2,1)S(1)}, u32[]{:S(2)}, u32[]{:S(2)}) collective-permute-start(bf16[128,2048]{1,0:T(8,128)(2,1)} %bitcast.16.refs_0_), channel_id=1, source_target_pairs={{0,3},{1,0},{2,1},{3,2},{4,7},{5,4},{6,5},{7,6},{8,11},{9,8},{10,9... | collective-permute-start | bytes 1572872 | tf_op jit(solution)/shard_map/ppermute | solution.py:463
  149.8 35.4 %collective-permute-start.16 = (bf16[128,2048]{1,0:T(8,128)(2,1)}, bf16[128,2048]{1,0:T(8,128)(2,1)S(1)}, u32[]{:S(2)}, u32[]{:S(2)}) collective-permute-start(bf16[128,2048]{1,0:T(8,128)(2,1)} %bitcast.16.refs_0_), channel_id=1, source_target_pairs={{0,1},{1,2},{2,3},{3,0},{4,5},{5,6},{6,7},{7,4},{8,9},{9,10},{10,1... | collective-permute-start | bytes 1572872 | tf_op jit(solution)/shard_map/ppermute | solution.py:462
  158.1 73.7 %collective-permute-start.6 = (bf16[128,2048]{1,0:T(8,128)(2,1)}, bf16[128,2048]{1,0:T(8,128)(2,1)S(1)}, u32[]{:S(2)}, u32[]{:S(2)}) collective-permute-start(bf16[128,2048]{1,0:T(8,128)(2,1)} %get-tuple-element.34), channel_id=1, source_target_pairs={{0,1},{1,2},{2,3},{3,0},{4,5},{5,6},{6,7},{7,4},{8,9},{9,10},{10,1... | collective-permute-start | bytes 1572872 | tf_op jit(solution)/shard_map/ppermute | solution.py:469
  162.8 31.7 %collective-permute-start.10 = (bf16[128,2048]{1,0:T(8,128)(2,1)}, bf16[128,2048]{1,0:T(8,128)(2,1)S(1)}, u32[]{:S(2)}, u32[]{:S(2)}) collective-permute-start(bf16[128,2048]{1,0:T(8,128)(2,1)} %collective-permute-done.8.refs_1_), channel_id=1, source_target_pairs={{0,3},{1,0},{2,1},{3,2},{4,7},{5,4},{6,5},{7,6},{8,11},{9,8},{10,9... | collective-permute-start | bytes 1572872 | tf_op jit(solution)/shard_map/ppermute | solution.py:464
  174.1 27.7 %collective-permute-start.4 = (bf16[128,2048]{1,0:T(8,128)(2,1)}, bf16[128,2048]{1,0:T(8,128)(2,1)S(1)}, u32[]{:S(2)}, u32[]{:S(2)}) collective-permute-start(bf16[128,2048]{1,0:T(8,128)(2,1)} %shard_map.171), channel_id=1, source_target_pairs={{0,3},{1,0},{2,1},{3,2},{4,7},{5,4},{6,5},{7,6},{8,11},{9,8},{10,9... | collective-permute-start | bytes 1572872 | tf_op jit(solution)/shard_map/ppermute | solution.py:467
  182.4 63.3 %collective-permute-start.13 = (bf16[128,2048]{1,0:T(8,128)(2,1)}, bf16[128,2048]{1,0:T(8,128)(2,1)}, u32[]{:S(2)}, u32[]{:S(2)}) collective-permute-start(bf16[128,2048]{1,0:T(8,128)(2,1)} %get-tuple-element.37), channel_id=1, source_target_pairs={{0,3},{1,0},{2,1},{3,2},{4,7},{5,4},{6,5},{7,6},{8,11},{9,8},{10,9... | collective-permute-start | bytes 1572872 | tf_op jit(solution)/shard_map/ppermute | solution.py:469
  194.3 68.1 %collective-permute-start.21 = (bf16[128,2048]{1,0:T(8,128)(2,1)}, bf16[128,2048]{1,0:T(8,128)(2,1)}, u32[]{:S(2)}, u32[]{:S(2)}) collective-permute-start(bf16[128,2048]{1,0:T(8,128)(2,1)} %get-tuple-element.42), channel_id=1, source_target_pairs={{0,1},{1,2},{2,3},{3,0},{4,5},{5,6},{6,7},{7,4},{8,9},{9,10},{10,1... | collective-permute-start | bytes 1572872 | tf_op jit(solution)/shard_map/ppermute | solution.py:469
  194.5 27.4 %collective-permute-start.18 = (bf16[128,2048]{1,0:T(8,128)(2,1)}, bf16[128,2048]{1,0:T(8,128)(2,1)S(1)}, u32[]{:S(2)}, u32[]{:S(2)}) collective-permute-start(bf16[128,2048]{1,0:T(8,128)(2,1)} %copy-done.27), channel_id=1, source_target_pairs={{0,1},{1,2},{2,3},{3,0},{4,5},{5,6},{6,7},{7,4},{8,9},{9,10},{10,1... | collective-permute-start | bytes 1572872 | tf_op jit(solution)/shard_map/ppermute | solution.py:464
  201.8 29.1 %collective-permute-start.11 = (bf16[128,2048]{1,0:T(8,128)(2,1)}, bf16[128,2048]{1,0:T(8,128)(2,1)S(1)}, u32[]{:S(2)}, u32[]{:S(2)}) collective-permute-start(bf16[128,2048]{1,0:T(8,128)(2,1)} %shard_map.174), channel_id=1, source_target_pairs={{0,1},{1,2},{2,3},{3,0},{4,5},{5,6},{6,7},{7,4},{8,9},{9,10},{10,1... | collective-permute-start | bytes 1572872 | tf_op jit(solution)/shard_map/ppermute | solution.py:467
  221.9 12.0 %collective-permute-start.5 = (bf16[128,2048]{1,0:T(8,128)(2,1)S(1)}, bf16[128,2048]{1,0:T(8,128)(2,1)S(1)}, u32[]{:S(2)}, u32[]{:S(2)}) collective-permute-start(bf16[128,2048]{1,0:T(8,128)(2,1)S(1)} %add_convert_fusion.5), channel_id=1, source_target_pairs={{0,3},{1,0},{2,1},{3,2},{4,7},{5,4},{6,5},{7,6},{8,11},{9,8},{10,9... | collective-permute-start | bytes 1572872 | tf_op jit(solution)/shard_map/ppermute | solution.py:468
  230.9 12.0 %collective-permute-start.19 = (bf16[128,2048]{1,0:T(8,128)(2,1)}, bf16[128,2048]{1,0:T(8,128)(2,1)}, u32[]{:S(2)}, u32[]{:S(2)}) collective-permute-start(bf16[128,2048]{1,0:T(8,128)(2,1)} %shard_map.178), channel_id=1, source_target_pairs={{0,3},{1,0},{2,1},{3,2},{4,7},{5,4},{6,5},{7,6},{8,11},{9,8},{10,9... | collective-permute-start | bytes 1572872 | tf_op jit(solution)/shard_map/ppermute | solution.py:467
  231.8 13.8 %collective-permute-start.12 = (bf16[128,2048]{1,0:T(8,128)(2,1)}, bf16[128,2048]{1,0:T(8,128)(2,1)}, u32[]{:S(2)}, u32[]{:S(2)}) collective-permute-start(bf16[128,2048]{1,0:T(8,128)(2,1)} %add_convert_fusion.3), channel_id=1, source_target_pairs={{0,1},{1,2},{2,3},{3,0},{4,5},{5,6},{6,7},{7,4},{8,9},{9,10},{10,1... | collective-permute-start | bytes 1572872 | tf_op jit(solution)/shard_map/ppermute | solution.py:468
  234.9 23.2 %all-to-all-start.5 = ((bf16[16,8,2048]{2,1,0:T(8,128)(2,1)}), bf16[16,8,2048]{2,1,0:T(8,128)(2,1)S(1)}, u32[]{:S(2)}, u32[]{:S(2)}) async-start(bf16[16,8,2048]{2,1,0:T(8,128)(2,1)} %fusion), calls=%async_computation.5 | async-start | bytes 1048576 | tf_op jit(solution)/shard_map/all_to_all | solution.py:471
  244.1 18.3 %collective-permute-start.20 = (bf16[128,2048]{1,0:T(8,128)(2,1)S(1)}, bf16[128,2048]{1,0:T(8,128)(2,1)}, u32[]{:S(2)}, u32[]{:S(2)}) collective-permute-start(bf16[128,2048]{1,0:T(8,128)(2,1)S(1)} %add_convert_fusion.1), channel_id=1, source_target_pairs={{0,3},{1,0},{2,1},{3,2},{4,7},{5,4},{6,5},{7,6},{8,11},{9,8},{10,9... | collective-permute-start | bytes 1572872 | tf_op jit(solution)/shard_map/ppermute | solution.py:468
  258.1 20.4 %all-to-all-start.7 = ((bf16[16,8,2048]{2,1,0:T(8,128)(2,1)}), bf16[16,8,2048]{2,1,0:T(8,128)(2,1)S(1)}, u32[]{:S(2)}, u32[]{:S(2)}) async-start(bf16[16,8,2048]{2,1,0:T(8,128)(2,1)} %fusion.1), calls=%async_computation.7 | async-start | bytes 1048576 | tf_op jit(solution)/shard_map/all_to_all | solution.py:471
  278.5 20.2 %all-to-all-start.9 = ((bf16[16,8,2048]{2,1,0:T(8,128)(2,1)}), bf16[16,8,2048]{2,1,0:T(8,128)(2,1)S(1)}, u32[]{:S(2)}, u32[]{:S(2)}) async-start(bf16[16,8,2048]{2,1,0:T(8,128)(2,1)} %fusion.2), calls=%async_computation.9 | async-start | bytes 1048576 | tf_op jit(solution)/shard_map/all_to_all | solution.py:471
  284.7 18.9 %collective-permute-start.14 = (bf16[64,2048]{1,0:T(8,128)(2,1)S(1)}, bf16[64,2048]{1,0:T(8,128)(2,1)S(1)}, u32[]{:S(2)}, u32[]{:S(2)}) collective-permute-start(bf16[64,2048]{1,0:T(8,128)(2,1)S(1)} %get-tuple-element.39), channel_id=1, source_target_pairs={{0,8},{8,16},{16,24},{24,0},{1,9},{9,17},{17,25},{25,1},{2,10},{10... | collective-permute-start | bytes 786440 | tf_op jit(solution)/shard_map/ppermute | solution.py:485
  300.8 10.4 %collective-permute-start.22 = (bf16[64,2048]{1,0:T(8,128)(2,1)S(1)}, bf16[64,2048]{1,0:T(8,128)(2,1)S(1)}, u32[]{:S(2)}, u32[]{:S(2)}) collective-permute-start(bf16[64,2048]{1,0:T(8,128)(2,1)S(1)} %get-tuple-element.43), channel_id=1, source_target_pairs={{0,16},{8,24},{16,0},{24,8},{1,17},{9,25},{17,1},{25,9},{2,18},{10... | collective-permute-start | bytes 786440 | tf_op jit(solution)/shard_map/ppermute | solution.py:485
  303.1 14.1 %collective-permute-start.23 = (bf16[64,2048]{1,0:T(8,128)(2,1)S(1)}, bf16[64,2048]{1,0:T(8,128)(2,1)S(1)}, u32[]{:S(2)}, u32[]{:S(2)}) collective-permute-start(bf16[64,2048]{1,0:T(8,128)(2,1)S(1)} %get-tuple-element.44), channel_id=1, source_target_pairs={{0,24},{8,0},{16,8},{24,16},{1,25},{9,1},{17,9},{25,17},{2,26},{10... | collective-permute-start | bytes 786440 | tf_op jit(solution)/shard_map/ppermute | solution.py:485
  (29 other events, 448.9 us)

commit v2 on v1

--- a/solution.py
+++ b/solution.py
@@ -19,7 +19,8 @@
 CAP = 6
 TILE = 8
 WIDE = 128
-PIECES = 2
+SPARE = TILE - CAP
+WHOLE = (0, 2, 3)
 
 rope_base = 10000.0
 group_eps = 1e-05
@@ -73,9 +74,12 @@
     return first, second, (rest - second.astype(F32)).astype(BF16)
 
 
-def tables(cos_ref, sin_ref, base_ref):
-    cos_own, sin_own = [jnp.concatenate([ref[...]] * 2, axis=1) for ref in (cos_ref, sin_ref)]
-    cos_base, sin_base = base_ref[0:1, :], base_ref[1:2, :]
+def tables(index_ref, own_ref, base_ref):
+    parts = []
+    for table in (own_ref[...], base_ref[pl.ds(index_ref[0], 1), :]):
+        for half in (table[:, :HALF], table[:, HALF:]):
+            parts.append(jnp.concatenate([half, half], axis=1))
+    cos_own, sin_own, cos_base, sin_base = parts
     cosine = cos_base * cos_own - sin_base * sin_own
     sine = sin_base * cos_own + cos_base * sin_own
     return cosine, jnp.where(iota(sine.shape, 1) < HALF, -sine, sine)
@@ -85,17 +89,20 @@
     return values * cosine + pltpu.roll(values, HALF, 1) * sine
 
 
-def state_kernel(k_ref, v_ref, decay_ref, cos_ref, sin_ref, base_ref, out_ref):
-    rows, heads = decay_ref.shape
-    cosine, sine = tables(cos_ref, sin_ref, base_ref)
+def state_kernel(index_ref, k_ref, v_ref, decay_ref, own_ref, base_ref, out_ref):
+    heads, rows = decay_ref.shape
+    cosine, sine = tables(index_ref, own_ref, base_ref)
     lower = (iota((rows, rows), 0) >= iota((rows, rows), 1)).astype(BF16)
-    cumulative = sum(dot(lower, part) for part in three_parts(decay_ref[...]))
+    cumulative = sum(dot(lower, part, 1, 1) for part in three_parts(decay_ref[...]))
     share = out_ref.shape[1] - TILE
     per_head = HEAD_DIM // share
-    for h in range(heads):
-        cols = slice(h * HEAD_DIM, (h + 1) * HEAD_DIM)
+    lane = iota((rows, heads), 1)
+
+    @pl.loop(0, heads)
+    def _(h):
+        cols = pl.ds(pl.multiple_of(h * HEAD_DIM, HEAD_DIM), HEAD_DIM)
         keys = turned(k_ref[:, cols].astype(F32), cosine, sine) * HEAD_DIM ** (-0.5)
-        column = cumulative[:, h : h + 1]
+        column = jnp.sum(jnp.where(lane == h, cumulative, 0.0), axis=1, keepdims=True)
         total = column[rows - 1 : rows, :]
         tail = keys * jnp.exp(total - column)
         state = dot(tail.astype(BF16), v_ref[:, cols], 0, 0)
@@ -143,14 +150,14 @@
         out_ref[j] = (state * jnp.exp(reach_ref[j, 0:1]) + before_ref[j]).astype(BF16)
 
 
-def inner_kernel(q_ref, k_ref, v_ref, decay_ref, cos_ref, sin_ref, base_ref, out_ref, lead_ref, across_ref):
-    rows, heads = decay_ref.shape
-    cosine, sine = tables(cos_ref, sin_ref, base_ref)
+def inner_kernel(index_ref, q_ref, k_ref, v_ref, decay_ref, own_ref, base_ref, out_ref, lead_ref, across_ref):
+    heads, rows = decay_ref.shape
+    cosine, sine = tables(index_ref, own_ref, base_ref)
     causal = iota((rows, rows), 0) >= iota((rows, rows), 1)
     lower = causal.astype(BF16)
     parts = three_parts(decay_ref[...])
-    cumulative = sum(dot(lower, part) for part in parts)
-    across = sum(dot(part, lower, 0, 1) for part in parts)
+    cumulative = sum(dot(lower, part, 1, 1) for part in parts)
+    across = sum(dot(part, lower, 1, 1) for part in parts)
     across_ref[...] = across
     lane = iota((rows, heads), 1)
 
@@ -222,9 +229,12 @@
     line = iota((dests, TILE, block), 1)
     picks = []
     for i, ref in enumerate(blocks):
-        named = (dot(choose, ref[:, width : width + WIDE], 1, 1) > 0.0).astype(F32)
-        slot = dot(named.astype(BF16), earlier).astype(jnp.int32) + (CAP * (chunk + i) - TILE * chunk)
-        slot = jnp.where(named > 0.0, slot, -1)
+        named = dot(choose, ref[:, width : width + WIDE], 1, 1) > 0.0
+        slot = dot(named.astype(F32).astype(BF16), earlier).astype(jnp.int32)
+        if i == 1:
+            slot = slot + (CAP - SPARE * chunk)
+            named = named & (slot >= CAP)
+        slot = jnp.where(named, slot, -1)
         pick = (slot[:, None, :] == line).astype(F32).reshape(dests * TILE, block)
         picks.append(pick.astype(BF16))
     pick = jnp.concatenate(picks, axis=1)
@@ -237,8 +247,8 @@
         out_ref[:, cols] = dot(pick, rows).astype(BF16)
 
 
-def merge_kernel(first_block, place_ref, *refs):
-    count = 2
+def merge_kernel(uses, place_ref, *refs):
+    count = len(uses)
     tables, outs = refs[:count], refs[-count:]
     backs = refs[count:-count]
     block, dests = tables[0].shape[0], backs[0].shape[0] // TILE
@@ -247,78 +257,65 @@
     spread = (iota((dests, dests * TILE), 1) // TILE == iota((dests, dests * TILE), 0)).astype(BF16)
     place_in = iota((block, dests * TILE), 1) % TILE
     mixes = []
-    for i, table_ref in enumerate(tables):
+    for table_ref, own_uses in zip(tables, uses):
         table = table_ref[...]
         high, low = [
             dot(table, (iota((WIDE, dests), 0) == lane_of(iota((WIDE, dests), 1), place, half)).astype(BF16))
             for half in (0, 1)
         ]
-        slot = dot(earlier, (high > 0.0).astype(F32).astype(BF16)) + CAP * (first_block + i)
-        slot_wide = dot(slot.astype(BF16), spread).astype(jnp.int32)
+        rank = dot(earlier, (high > 0.0).astype(F32).astype(BF16))
+        rank = dot(rank.astype(BF16), spread).astype(jnp.int32)
         parts = [dot(part.astype(BF16), spread) for part in (high, low)]
-        chunk_base = first_block // 2
+        lines = []
+        for _, spare in own_uses:
+            if spare is None:
+                lines.append((rank == place_in) & (place_in < CAP))
+            else:
+                lines.append((rank == place_in - (CAP - SPARE * spare)) & (place_in >= CAP))
         mixes.append(
             [
-                jnp.concatenate(
-                    [
-                        jnp.where(slot_wide == place_in + (chunk_base + c) * TILE, part, 0.0).astype(BF16)
-                        for c in range(len(backs))
-                    ],
-                    axis=1,
-                )
+                jnp.concatenate([jnp.where(here, part, 0.0).astype(BF16) for here in lines], axis=1)
                 for part in parts
             ]
         )
-    high = jnp.concatenate([pair[0] for pair in mixes], axis=0)
-    low = jnp.concatenate([pair[1] for pair in mixes], axis=0)
     step = 256
 
     @pl.loop(0, outs[0].shape[1] // step)
     def _(n):
         cols = pl.ds(pl.multiple_of(n * step, step), step)
-        piece = jnp.concatenate([ref[:, cols] for ref in backs], axis=0)
-        total = (dot(high, piece) + dot(low, piece)).astype(BF16)
-        for i, out_ref in enumerate(outs):
-            out_ref[:, cols] = total[i * block : (i + 1) * block]
+        for (high, low), own_uses, out_ref in zip(mixes, uses, outs):
+            piece = jnp.concatenate([backs[i][:, cols] for i, _ in own_uses], axis=0)
+            out_ref[:, cols] = (dot(high, piece) + dot(low, piece)).astype(BF16)
 
 
 def expert_kernel(parts, *refs):
     ins, (gate_ref, up_ref, down_ref) = refs[:parts], refs[parts : parts + 3]
     outs = refs[parts + 3 : -6]
-    all_ref, act_ref, gate_in, up_in, down_in, sems = refs[-6:]
+    all_ref, act_ref, open_ref, up_in, down_in, sems = refs[-6:]
     rows = ins[0].shape[0]
-    fetches = [
-        [
-            pltpu.make_async_copy(
-                source.at[0, pl.ds(j * (target.shape[0] // PIECES), target.shape[0] // PIECES)],
-                target.at[pl.ds(j * (target.shape[0] // PIECES), target.shape[0] // PIECES)],
-                sems.at[i, j],
-            )
-            for j in range(PIECES)
-        ]
-        for i, (source, target) in enumerate(((gate_ref, gate_in), (up_ref, up_in), (down_ref, down_in)))
-    ]
-    for group in fetches:
-        for fetch in group:
-            fetch.start()
+    fetch_up = pltpu.make_async_copy(up_ref.at[0], up_in, sems.at[0])
+    fetch_down = pltpu.make_async_copy(down_ref.at[0], down_in, sems.at[1])
+    fetch_up.start()
+    fetch_down.start()
     for i, ref in enumerate(ins):
         all_ref[i * rows : (i + 1) * rows, :] = ref[...]
-    for fetch in fetches[0]:
-        fetch.wait()
-    for fetch in fetches[1]:
-        fetch.wait()
     half = 256
 
-    @pl.loop(0, gate_in.shape[1] // half)
+    @pl.loop(0, up_in.shape[1] // half)
     def _(n):
         cols = pl.ds(pl.multiple_of(n * half, half), half)
-        gate = jnp.minimum(dot(all_ref[...], gate_in[:, cols]), clamp_limit)
-        gate = gate / (1.0 + jnp.exp(-swish_alpha * gate))
+        gate = jnp.minimum(dot(all_ref[...], gate_ref[0, :, cols]), clamp_limit)
+        open_ref[:, cols] = gate / (1.0 + jnp.exp(-swish_alpha * gate))
+
+    fetch_up.wait()
+
+    @pl.loop(0, up_in.shape[1] // half)
+    def _(n):
+        cols = pl.ds(pl.multiple_of(n * half, half), half)
         up = jnp.clip(dot(all_ref[...], up_in[:, cols]), -clamp_limit, clamp_limit)
-        act_ref[:, cols] = ((up + 1.0) * gate).astype(BF16)
-
-    for fetch in fetches[2]:
-        fetch.wait()
+        act_ref[:, cols] = ((up + 1.0) * open_ref[:, cols]).astype(BF16)
+
+    fetch_down.wait()
     step = 512
 
     @pl.loop(0, down_in.shape[1] // step)
@@ -337,15 +334,15 @@
         [shape((count, width))] * len(rows),
         *rows, *weights,
         flops=6 * total * width * hidden,
-        far=range(len(rows), len(rows) + 3),
-        room=56,
+        far=range(len(rows) + 1, len(rows) + 3),
+        room=50,
         scratch=[
             pltpu.VMEM((total, width), BF16),
             pltpu.VMEM((total, hidden), BF16),
-            pltpu.VMEM((width, hidden), BF16),
+            pltpu.VMEM((total, hidden), F32),
             pltpu.VMEM((width, hidden), BF16),
             pltpu.VMEM((hidden, width), BF16),
-            pltpu.SemaphoreType.DMA((3, PIECES)),
+            pltpu.SemaphoreType.DMA((2,)),
         ],
     )
 
@@ -383,10 +380,13 @@
 
     inverse = rope_base ** (-np.arange(HALF, dtype=np.float64) / HALF)
     inside = np.arange(tok_count, dtype=np.float64)[:, None] * inverse[None]
-    starts = (np.arange(sp_count, dtype=np.float64) * tok_count)[:, None] * np.tile(inverse, 2)[None]
-    cos_own, sin_own = jnp.asarray(np.cos(inside), F32), jnp.asarray(np.sin(inside), F32)
-    base_all = jnp.asarray(np.stack([np.cos(starts), np.sin(starts)], axis=1), F32)
-    base = lax.dynamic_index_in_dim(base_all, sp_index, 0, keepdims=False)
+    starts = (np.arange(sp_count, dtype=np.float64) * tok_count)[:, None] * inverse[None]
+    own_table, base = [
+        jnp.asarray(np.concatenate([np.cos(angle), np.sin(angle)], axis=1), F32)
+        for angle in (inside, starts)
+    ]
+    index = sp_index.astype(jnp.int32).reshape(1)
+    decays = log_decay.T
 
     near_count = lax.axis_size(("x", "c"))
     far_count = lax.axis_size("z")
@@ -394,15 +394,19 @@
     message = call(
         state_kernel,
         shape((near_count, share + TILE, HEAD_DIM)),
-        key_rows, value_rows, log_decay, cos_own, sin_own, base,
+        index, key_rows, value_rows, decays, own_table, base,
         flops=2 * tok_count * local * HEAD_DIM,
+        smem=(0,),
+        room=56,
     )
     spans = lax.all_to_all(message, ("x", "c"), 0, 0, tiled=True)
     inner, lead = call(
         inner_kernel,
         [shape((tok_count, local), F32), shape((tok_count, local))],
-        query_rows, key_rows, value_rows, log_decay, cos_own, sin_own, base,
+        index, query_rows, key_rows, value_rows, decays, own_table, base,
+        smem=(0,),
         flops=4 * tok_count * tok_count * local,
+        room=56,
         scratch=[pltpu.VMEM((heads, tok_count), F32)],
     )
     before, reach, group = call(
@@ -447,12 +451,12 @@
             call(
                 functools.partial(gather_kernel, c),
                 shape((dests * TILE, width)),
-                place, near[c], near[c + 1],
+                place, near[WHOLE[c]], near[1],
                 flops=4 * dests * TILE * rows_own * width,
                 smem=(0,),
             )
         )
-    weights = gate_weight, up_weight, down_weight
+    weights = pltpu.with_memory_space_constraint(gate_weight, pltpu.VMEM), up_weight, down_weight
     ahead, behind = ring(tp_count, 1), ring(tp_count, -1)
     returned = []
     for c, piece in enumerate(outgoing, 1):
@@ -471,17 +475,21 @@
         back = lax.all_to_all(total.reshape(dests, TILE, width), ("z", "c"), 0, 0, tiled=True)
         returned.append(back.reshape(dests * TILE, width))
     tables = [rows[:, width:] for rows in near]
-    merged = []
-    for i in range(2):
-        merged += call(
-            functools.partial(merge_kernel, 2 * i),
-            [shape((rows_own, width))] * 2,
-            place, tables[2 * i], tables[2 * i + 1], returned[i], returned[i + 1],
+
+    def merge(blocks, uses, backs):
+        return call(
+            functools.partial(merge_kernel, uses),
+            [shape((rows_own, width))] * len(blocks),
+            place, *[tables[d] for d in blocks], *backs,
             flops=8 * dests * TILE * rows_own * width,
             smem=(0,),
         )
+
+    merged = {}
+    merged[0], merged[2] = merge((0, 2), (((0, None),), ((1, None),)), returned[:2])
+    merged[1], merged[3] = merge((1, 3), (((0, 0), (1, 1), (2, 2)), ((2, None),)), returned)
     total = updated + merged[0].astype(F32)
-    for d in shifts[1:]:
+    for d in (2, 1, 3):
         total = total + lax.ppermute(merged[d], "x", ring(x_count, d)).astype(F32)
     return total.astype(BF16)
 

time: 321 us -> 310 us (0.966)
  Pallas kernels: 62 us -> 52.2 us
  waiting for transfers between devices: 148 us -> 155 us
  local copies, waits for them, and re-layouts: 12.6 us -> 8.29 us
  starting transfers between devices: 58.8 us -> 54.6 us
    pallas_call x17, Pallas kernels: 62 us -> 52.2 us  [call(): pl.pallas_call(kernel, out_shape=out_shape, in_specs=specs, out_specs=out...]
    all_to_all x3, waiting for transfers between devices: 37.1 us -> 30.8 us  [body(): lax.all_to_all(total.reshape(dests, TILE, width), ('z', 'c'), 0, 0, tiled...]
    ppermute x3, waiting for transfers between devices: 22 us -> 28.1 us  [body(): far = lax.ppermute(one, 'tp', first)]
    ppermute x3, waiting for transfers between devices: 2.89 us -> 8.96 us  [body(): via = lax.ppermute(out_far, 'tp', second)]
    ppermute x3, waiting for transfers between devices: 13.6 us -> 7.6 us  [body(): total = total + lax.ppermute(merged[d], 'x', ring(x_count, d)).astype(F32)]
    unnamed x61 -> x46, local copies, waits for them, and re-layouts: 11.9 us -> 6.05 us
    ppermute x3, waiting for transfers between devices: 4.53 us -> 8.1 us  [body(): two = lax.ppermute(own, 'tp', second)]
    ppermute x3, waiting for transfers between devices: 15.2 us -> 18.4 us  [body(): one = lax.ppermute(own, 'tp', first)]
  transfers between devices with their start and end apart: 32 -> 32, of which waited for: 20 -> 21; matrix products, arithmetic and copies ran while one was open for 3% -> 3% of each run, Pallas kernels for 17% -> 14%
where the time goes in v2:
time: 310 us; the launch traced here: 307 us
  waiting for transfers between devices  155 us (50%)
  starting transfers between devices  54.6 us (18%)
  Pallas kernels  52.2 us (17%)
  blocking collectives  27.2 us (9%)
  other arithmetic  8.76 us (3%)
  local copies, waits for them, and re-layouts  8.29 us (3%)
    pallas_call x17, Pallas kernels, call(): pl.pallas_call(kernel, out_shape=out_shape, in_specs=specs, out_specs=out...  52.2 us
    all_to_all x3, waiting for transfers between devices, body(): lax.all_to_all(total.reshape(dests, TILE, width), ('z', 'c'), 0, 0, tiled...  30.8 us
    ppermute x3, waiting for transfers between devices, body(): far = lax.ppermute(one, 'tp', first)  28.1 us
    ppermute x3, waiting for transfers between devices, body(): near.append(lax.ppermute(extended, 'x', ring(x_count, -d)))  20.4 us
    ppermute x3, waiting for transfers between devices, body(): one = lax.ppermute(own, 'tp', first)  18.4 us
    all_to_all x3, waiting for transfers between devices, body(): lax.all_to_all(piece.reshape(dests, TILE, width), ('z', 'c'), 0, 0, tiled...  17.6 us
    all_to_all x1, blocking collectives, body(): groups = lax.all_to_all(group, 'z', 0, 0, tiled=True)  16.8 us
    all_to_all x1, waiting for transfers between devices, body(): lax.all_to_all(mixed.reshape(tp_count, rows_own, width), 'tp', 0, 0, tile...  14.6 us
  transfers between devices with their start and end apart: 32, of which 21 were waited for; matrix products, arithmetic and copies ran while one was open for 3% of the time, Pallas kernels for 14%

profile of v2, /device:TPU:2, one launch (start us, length us, event | category | flops | bytes accessed | tf_op | source)
XLA Modules:
  0.0 306.6 jit_solution(9261339247161174929)
XLA Ops:
  0.0 3.5 %shard_map.155 = bf16[8,72,128]{2,1,0:T(8,128)(2,1)} custom-call(s32[1]{0:T(128)} %bitcast.index_ref, bf16[256,512]{1,0:T(8,128)(2,1)} %k_ref.3, bf16[256,512]{1,0:T(8,128)(2,1)} %v_ref.3, f32[4,256]{1,0:T(4,128)} %bitcast.31, f32[256,128]{1,0:T(8,128)} %constant.31.clone.own_ref, f32[64,128]{1,0:T(8,128)} %constant.32.clone.base_ref), custom_call_target="tpu_custom_call" | custom-call | flops 33554432 | bytes 692228 | tf_op jit(solution)/shard_map/pallas_call | solution.py:55
  3.5 10.3 %all_to_all.50.in_ref = bf16[8,72,128]{2,1,0:T(8,128)(2,1)S(1)} all-to-all(bf16[8,72,128]{2,1,0:T(8,128)(2,1)} %shard_map.155), channel_id=1, replica_groups=mesh['z'=8,'x'=4,'c'=2,'tp'=4] {'x','c'}, dimensions={0} | all-to-all | bytes 294912 | tf_op jit(solution)/shard_map/all_to_all | solution.py:402
  13.9 16.8 %all_to_all.51.in_ref = bf16[8,72,128]{2,1,0:T(8,128)(2,1)S(1)} all-to-all(bf16[8,72,128]{2,1,0:T(8,128)(2,1)S(1)} %get-tuple-element.27), channel_id=1, replica_groups=mesh['z'=8,'x'=4,'c'=2,'tp'=4] {'z'}, dimensions={0} | all-to-all | bytes 294912 | tf_op jit(solution)/shard_map/all_to_all | solution.py:417
  31.5 4.7 %all-to-all-start.2 = ((bf16[8,64,128]{2,1,0:T(8,128)(2,1)}), bf16[8,64,128]{2,1,0:T(8,128)(2,1)S(1)}, u32[]{:S(2)}, u32[]{:S(2)}) async-start(bf16[8,64,128]{2,1,0:T(8,128)(2,1)} %shard_map.157), calls=%async_computation.2 | async-start | bytes 262144 | tf_op jit(solution)/shard_map/all_to_all | solution.py:424
  36.2 4.0 %shard_map.154 = (f32[256,512]{1,0:T(8,128)}, bf16[256,512]{1,0:T(8,128)(2,1)}) custom-call(s32[1]{0:T(128)} %bitcast.index_ref, bf16[256,512]{1,0:T(8,128)(2,1)} %q_ref.1, bf16[256,512]{1,0:T(8,128)(2,1)} %k_ref.3, bf16[256,512]{1,0:T(8,128)(2,1)} %v_ref.3, f32[4,256]{1,0:T(4,128)} %bitcast.32, f32[256,128]{1,0:T(8,128)} %constant.31.clone.own_ref, ...), custom_call_target="tpu_custom_call" | custom-call | flops 134217728 | bytes 954372 | tf_op jit(solution)/shard_map/pallas_call | solution.py:55
  42.9 3.6 %shard_map.158 = bf16[256,2048]{1,0:T(8,128)(2,1)} custom-call(f32[256,512]{1,0:T(8,128)S(1)} %copy-done.9, bf16[256,512]{1,0:T(8,128)(2,1)S(1)} %copy-done.15, bf16[512,128]{1,0:T(8,128)(2,1)S(1)} %bitcast.28, bf16[256,512]{1,0:T(8,128)(2,1)S(1)} %copy-done.14, f32[1,512]{1,0:T(1,128)S(1)} %bitcast.30, bf16[512,2048]{1,0:T(8,128)(2,1)S(1)} %copy-done.2), custom_call_target="tpu_custom_call" | custom-call | flops 536870912 | bytes 3278848 | tf_op jit(solution)/shard_map/pallas_call | solution.py:55
  46.5 4.6 %all-to-all-start.3 = ((bf16[4,64,2048]{2,1,0:T(8,128)(2,1)}), bf16[4,64,2048]{2,1,0:T(8,128)(2,1)S(1)}, u32[]{:S(2)}, u32[]{:S(2)}) async-start(bf16[4,64,2048]{2,1,0:T(8,128)(2,1)} %bitcast.5), calls=%async_computation.3 | async-start | bytes 2097152 | tf_op jit(solution)/shard_map/all_to_all | solution.py:432
  51.3 14.6 %all-to-all-done.3.sum_ref = bf16[4,64,2048]{2,1,0:T(8,128)(2,1)S(1)} async-done(((bf16[4,64,2048]{2,1,0:T(8,128)(2,1)}), bf16[4,64,2048]{2,1,0:T(8,128)(2,1)S(1)}, u32[]{:S(2)}, u32[]{:S(2)}) %all-to-all-start.3) | async-done | bytes 1048608 | tf_op jit(solution)/shard_map/all_to_all | solution.py:432
  69.2 5.8 %collective-permute-done.1.refs_1_ = bf16[64,2176]{1,0:T(8,128)(2,1)S(1)} collective-permute-done((bf16[64,2176]{1,0:T(8,128)(2,1)S(1)}, bf16[64,2176]{1,0:T(8,128)(2,1)S(1)}, u32[]{:S(2)}, u32[]{:S(2)}) %collective-permute-start.1) | collective-permute-done | bytes 278560 | tf_op jit(solution)/shard_map/ppermute | solution.py:445
  74.9 5.7 %collective-permute-done.refs_0_ = bf16[64,2176]{1,0:T(8,128)(2,1)S(1)} collective-permute-done((bf16[64,2176]{1,0:T(8,128)(2,1)S(1)}, bf16[64,2176]{1,0:T(8,128)(2,1)S(1)}, u32[]{:S(2)}, u32[]{:S(2)}) %collective-permute-start) | collective-permute-done | bytes 278560 | tf_op jit(solution)/shard_map/ppermute | solution.py:445
  83.9 4.2 %all-to-all-start.6 = ((bf16[16,8,2048]{2,1,0:T(8,128)(2,1)}), bf16[16,8,2048]{2,1,0:T(8,128)(2,1)}, u32[]{:S(2)}, u32[]{:S(2)}) async-start(bf16[16,8,2048]{2,1,0:T(8,128)(2,1)} %bitcast.12), calls=%async_computation.6 | async-start | bytes 1048576 | tf_op jit(solution)/shard_map/all_to_all | solution.py:464
  90.6 13.4 %all-to-all-done.6 = bf16[16,8,2048]{2,1,0:T(8,128)(2,1)} async-done(((bf16[16,8,2048]{2,1,0:T(8,128)(2,1)}), bf16[16,8,2048]{2,1,0:T(8,128)(2,1)}, u32[]{:S(2)}, u32[]{:S(2)}) %all-to-all-start.6) | async-done | bytes 524320 | tf_op jit(solution)/shard_map/all_to_all | solution.py:464
  104.0 4.3 %all-to-all-start.4 = ((bf16[16,8,2048]{2,1,0:T(8,128)(2,1)}), bf16[16,8,2048]{2,1,0:T(8,128)(2,1)}, u32[]{:S(2)}, u32[]{:S(2)}) async-start(bf16[16,8,2048]{2,1,0:T(8,128)(2,1)} %bitcast.8), calls=%async_computation.4 | async-start | bytes 1048576 | tf_op jit(solution)/shard_map/all_to_all | solution.py:464
  108.4 8.9 %collective-permute-done.15.refs_0_ = bf16[64,2176]{1,0:T(8,128)(2,1)S(1)} collective-permute-done((bf16[64,2176]{1,0:T(8,128)(2,1)S(1)}, bf16[64,2176]{1,0:T(8,128)(2,1)S(1)}, u32[]{:S(2)}, u32[]{:S(2)}) %collective-permute-start.15) | collective-permute-done | bytes 278560 | tf_op jit(solution)/shard_map/ppermute | solution.py:445
  120.5 3.9 %all-to-all-done.4 = bf16[16,8,2048]{2,1,0:T(8,128)(2,1)} async-done(((bf16[16,8,2048]{2,1,0:T(8,128)(2,1)}), bf16[16,8,2048]{2,1,0:T(8,128)(2,1)}, u32[]{:S(2)}, u32[]{:S(2)}) %all-to-all-start.4) | async-done | bytes 524320 | tf_op jit(solution)/shard_map/all_to_all | solution.py:464
  124.4 4.2 %all-to-all-start.8 = ((bf16[16,8,2048]{2,1,0:T(8,128)(2,1)}), bf16[16,8,2048]{2,1,0:T(8,128)(2,1)}, u32[]{:S(2)}, u32[]{:S(2)}) async-start(bf16[16,8,2048]{2,1,0:T(8,128)(2,1)} %bitcast.16), calls=%async_computation.8 | async-start | bytes 1048576 | tf_op jit(solution)/shard_map/all_to_all | solution.py:464
  132.0 12.5 %collective-permute-done.2.refs_1_ = bf16[128,2048]{1,0:T(8,128)(2,1)} collective-permute-done((bf16[128,2048]{1,0:T(8,128)(2,1)}, bf16[128,2048]{1,0:T(8,128)(2,1)}, u32[]{:S(2)}, u32[]{:S(2)}) %collective-permute-start.2) | collective-permute-done | bytes 524320 | tf_op jit(solution)/shard_map/ppermute | solution.py:466
  147.7 5.7 %shard_map.161 = (bf16[128,2048]{1,0:T(8,128)(2,1)S(1)}, bf16[128,2048]{1,0:T(8,128)(2,1)S(1)}, bf16[128,2048]{1,0:T(8,128)(2,1)S(1)}) custom-call(bf16[128,2048]{1,0:T(8,128)(2,1)} %bitcast.9.refs_0_, bf16[128,2048]{1,0:T(8,128)(2,1)} %collective-permute-done.2.refs_1_, bf16[128,2048]{1,0:T(8,128)(2,1)} %collective-permute-done.3.refs_2_, ...), custom_call_target="tpu_custom_call" | custom-call | flops 2415919104 | bytes 7864320 | tf_op jit(solution)/shard_map/pallas_call | solution.py:55
  155.5 5.2 %collective-permute-done.4.refs_0_ = bf16[128,2048]{1,0:T(8,128)(2,1)S(1)} collective-permute-done((bf16[128,2048]{1,0:T(8,128)(2,1)}, bf16[128,2048]{1,0:T(8,128)(2,1)S(1)}, u32[]{:S(2)}, u32[]{:S(2)}) %collective-permute-start.4) | collective-permute-done | bytes 524320 | tf_op jit(solution)/shard_map/ppermute | solution.py:468
  163.9 8.1 %collective-permute-done.9.refs_2_ = bf16[128,2048]{1,0:T(8,128)(2,1)} collective-permute-done((bf16[128,2048]{1,0:T(8,128)(2,1)}, bf16[128,2048]{1,0:T(8,128)(2,1)}, u32[]{:S(2)}, u32[]{:S(2)}) %collective-permute-start.9) | collective-permute-done | bytes 524320 | tf_op jit(solution)/shard_map/ppermute | solution.py:467
  172.0 6.5 %shard_map.164 = (bf16[128,2048]{1,0:T(8,128)(2,1)S(1)}, bf16[128,2048]{1,0:T(8,128)(2,1)S(1)}, bf16[128,2048]{1,0:T(8,128)(2,1)}) custom-call(bf16[128,2048]{1,0:T(8,128)(2,1)} %bitcast.13.refs_0_, bf16[128,2048]{1,0:T(8,128)(2,1)} %collective-permute-done.8.refs_1_, bf16[128,2048]{1,0:T(8,128)(2,1)} %collective-permute-done.9.refs_2_, ...), custom_call_target="tpu_custom_call" | custom-call | flops 2415919104 | bytes 7864320 | tf_op jit(solution)/shard_map/pallas_call | solution.py:55
  179.3 3.9 %collective-permute-done.16.refs_1_ = bf16[128,2048]{1,0:T(8,128)(2,1)S(1)} collective-permute-done((bf16[128,2048]{1,0:T(8,128)(2,1)}, bf16[128,2048]{1,0:T(8,128)(2,1)S(1)}, u32[]{:S(2)}, u32[]{:S(2)}) %collective-permute-start.16) | collective-permute-done | bytes 524320 | tf_op jit(solution)/shard_map/ppermute | solution.py:466
  184.0 6.4 %shard_map.168 = (bf16[128,2048]{1,0:T(8,128)(2,1)S(1)}, bf16[128,2048]{1,0:T(8,128)(2,1)S(1)}, bf16[128,2048]{1,0:T(8,128)(2,1)}) custom-call(bf16[128,2048]{1,0:T(8,128)(2,1)} %bitcast.17.refs_0_, bf16[128,2048]{1,0:T(8,128)(2,1)} %copy-done.20, bf16[128,2048]{1,0:T(8,128)(2,1)} %copy-done.21, bf16[1,2048,512]{2,1,0:T(8,128)(2,1)S(1)} %copy-done.1, ...), custom_call_target="tpu_custom_call" | custom-call | flops 2415919104 | bytes 7864320 | tf_op jit(solution)/shard_map/pallas_call | solution.py:55
  195.0 22.9 %collective-permute-done.18.refs_0_ = bf16[128,2048]{1,0:T(8,128)(2,1)S(1)} collective-permute-done((bf16[128,2048]{1,0:T(8,128)(2,1)}, bf16[128,2048]{1,0:T(8,128)(2,1)S(1)}, u32[]{:S(2)}, u32[]{:S(2)}) %collective-permute-start.18) | collective-permute-done | bytes 524320 | tf_op jit(solution)/shard_map/ppermute | solution.py:468
  221.2 6.3 %collective-permute-done.11 = bf16[128,2048]{1,0:T(8,128)(2,1)S(1)} collective-permute-done((bf16[128,2048]{1,0:T(8,128)(2,1)S(1)}, bf16[128,2048]{1,0:T(8,128)(2,1)S(1)}, u32[]{:S(2)}, u32[]{:S(2)}) %collective-permute-start.11) | collective-permute-done | bytes 524320 | tf_op jit(solution)/shard_map/ppermute | solution.py:471
  231.6 5.6 %all-to-all-start.5 = ((bf16[16,8,2048]{2,1,0:T(8,128)(2,1)}), bf16[16,8,2048]{2,1,0:T(8,128)(2,1)S(1)}, u32[]{:S(2)}, u32[]{:S(2)}) async-start(bf16[16,8,2048]{2,1,0:T(8,128)(2,1)} %fusion), calls=%async_computation.5 | async-start | bytes 1048576 | tf_op jit(solution)/shard_map/all_to_all | solution.py:475
  245.8 7.4 %all-to-all-done.5 = bf16[16,8,2048]{2,1,0:T(8,128)(2,1)S(1)} async-done(((bf16[16,8,2048]{2,1,0:T(8,128)(2,1)}), bf16[16,8,2048]{2,1,0:T(8,128)(2,1)S(1)}, u32[]{:S(2)}, u32[]{:S(2)}) %all-to-all-start.5) | async-done | bytes 524320 | tf_op jit(solution)/shard_map/all_to_all | solution.py:475
  253.1 4.2 %all-to-all-start.7 = ((bf16[16,8,2048]{2,1,0:T(8,128)(2,1)}), bf16[16,8,2048]{2,1,0:T(8,128)(2,1)S(1)}, u32[]{:S(2)}, u32[]{:S(2)}) async-start(bf16[16,8,2048]{2,1,0:T(8,128)(2,1)} %fusion.1), calls=%async_computation.7 | async-start | bytes 1048576 | tf_op jit(solution)/shard_map/all_to_all | solution.py:475
  259.7 13.9 %all-to-all-done.7 = bf16[16,8,2048]{2,1,0:T(8,128)(2,1)S(1)} async-done(((bf16[16,8,2048]{2,1,0:T(8,128)(2,1)}), bf16[16,8,2048]{2,1,0:T(8,128)(2,1)S(1)}, u32[]{:S(2)}, u32[]{:S(2)}) %all-to-all-start.7) | async-done | bytes 524320 | tf_op jit(solution)/shard_map/all_to_all | solution.py:475
  273.5 4.0 %all-to-all-start.9 = ((bf16[16,8,2048]{2,1,0:T(8,128)(2,1)}), bf16[16,8,2048]{2,1,0:T(8,128)(2,1)S(1)}, u32[]{:S(2)}, u32[]{:S(2)}) async-start(bf16[16,8,2048]{2,1,0:T(8,128)(2,1)} %fusion.2), calls=%async_computation.9 | async-start | bytes 1048576 | tf_op jit(solution)/shard_map/all_to_all | solution.py:475
  284.2 9.5 %all-to-all-done.9 = bf16[16,8,2048]{2,1,0:T(8,128)(2,1)S(1)} async-done(((bf16[16,8,2048]{2,1,0:T(8,128)(2,1)}), bf16[16,8,2048]{2,1,0:T(8,128)(2,1)S(1)}, u32[]{:S(2)}, u32[]{:S(2)}) %all-to-all-start.9) | async-done | bytes 524320 | tf_op jit(solution)/shard_map/all_to_all | solution.py:475
  298.1 6.7 %collective-permute-done.22 = bf16[64,2048]{1,0:T(8,128)(2,1)S(1)} collective-permute-done((bf16[64,2048]{1,0:T(8,128)(2,1)S(1)}, bf16[64,2048]{1,0:T(8,128)(2,1)S(1)}, u32[]{:S(2)}, u32[]{:S(2)}) %collective-permute-start.22) | collective-permute-done | bytes 262176 | tf_op jit(solution)/shard_map/ppermute | solution.py:493
  (109 shorter events, 64.8 us)
Async XLA Ops:
  31.5 9.4 %all-to-all-start.2 = ((bf16[8,64,128]{2,1,0:T(8,128)(2,1)}), bf16[8,64,128]{2,1,0:T(8,128)(2,1)S(1)}, u32[]{:S(2)}, u32[]{:S(2)}) async-start(bf16[8,64,128]{2,1,0:T(8,128)(2,1)} %shard_map.157), calls=%async_computation.2 | async-start | bytes 262144 | tf_op jit(solution)/shard_map/all_to_all | solution.py:424
  46.5 19.5 %all-to-all-start.3 = ((bf16[4,64,2048]{2,1,0:T(8,128)(2,1)}), bf16[4,64,2048]{2,1,0:T(8,128)(2,1)S(1)}, u32[]{:S(2)}, u32[]{:S(2)}) async-start(bf16[4,64,2048]{2,1,0:T(8,128)(2,1)} %bitcast.5), calls=%async_computation.3 | async-start | bytes 2097152 | tf_op jit(solution)/shard_map/all_to_all | solution.py:432
  66.4 8.6 %collective-permute-start.1 = (bf16[64,2176]{1,0:T(8,128)(2,1)S(1)}, bf16[64,2176]{1,0:T(8,128)(2,1)S(1)}, u32[]{:S(2)}, u32[]{:S(2)}) collective-permute-start(bf16[64,2176]{1,0:T(8,128)(2,1)S(1)} %get-tuple-element.31.refs_0_), channel_id=1, source_target_pairs={{0,24},{8,0},{16,8},{24,16},{1,25},{9,1},{17,9},{25,17},{2,26},{10... | collective-permute-start | bytes 835592 | tf_op jit(solution)/shard_map/ppermute | solution.py:445
  67.9 12.8 %collective-permute-start = (bf16[64,2176]{1,0:T(8,128)(2,1)S(1)}, bf16[64,2176]{1,0:T(8,128)(2,1)S(1)}, u32[]{:S(2)}, u32[]{:S(2)}) collective-permute-start(bf16[64,2176]{1,0:T(8,128)(2,1)S(1)} %get-tuple-element.31.refs_0_), channel_id=1, source_target_pairs={{0,16},{8,24},{16,0},{24,8},{1,17},{9,25},{17,1},{25,9},{2,18},{10... | collective-permute-start | bytes 835592 | tf_op jit(solution)/shard_map/ppermute | solution.py:445
  83.9 20.2 %all-to-all-start.6 = ((bf16[16,8,2048]{2,1,0:T(8,128)(2,1)}), bf16[16,8,2048]{2,1,0:T(8,128)(2,1)}, u32[]{:S(2)}, u32[]{:S(2)}) async-start(bf16[16,8,2048]{2,1,0:T(8,128)(2,1)} %bitcast.12), calls=%async_computation.6 | async-start | bytes 1048576 | tf_op jit(solution)/shard_map/all_to_all | solution.py:464
  104.0 20.4 %all-to-all-start.4 = ((bf16[16,8,2048]{2,1,0:T(8,128)(2,1)}), bf16[16,8,2048]{2,1,0:T(8,128)(2,1)}, u32[]{:S(2)}, u32[]{:S(2)}) async-start(bf16[16,8,2048]{2,1,0:T(8,128)(2,1)} %bitcast.8), calls=%async_computation.4 | async-start | bytes 1048576 | tf_op jit(solution)/shard_map/all_to_all | solution.py:464
  108.3 9.0 %collective-permute-start.15 = (bf16[64,2176]{1,0:T(8,128)(2,1)S(1)}, bf16[64,2176]{1,0:T(8,128)(2,1)S(1)}, u32[]{:S(2)}, u32[]{:S(2)}) collective-permute-start(bf16[64,2176]{1,0:T(8,128)(2,1)S(1)} %get-tuple-element.31.refs_0_), channel_id=1, source_target_pairs={{0,8},{8,16},{16,24},{24,0},{1,9},{9,17},{17,25},{25,1},{2,10},{10... | collective-permute-start | bytes 835592 | tf_op jit(solution)/shard_map/ppermute | solution.py:445
  124.4 20.3 %all-to-all-start.8 = ((bf16[16,8,2048]{2,1,0:T(8,128)(2,1)}), bf16[16,8,2048]{2,1,0:T(8,128)(2,1)}, u32[]{:S(2)}, u32[]{:S(2)}) async-start(bf16[16,8,2048]{2,1,0:T(8,128)(2,1)} %bitcast.16), calls=%async_computation.8 | async-start | bytes 1048576 | tf_op jit(solution)/shard_map/all_to_all | solution.py:464
  128.7 15.8 %collective-permute-start.2 = (bf16[128,2048]{1,0:T(8,128)(2,1)}, bf16[128,2048]{1,0:T(8,128)(2,1)}, u32[]{:S(2)}, u32[]{:S(2)}) collective-permute-start(bf16[128,2048]{1,0:T(8,128)(2,1)} %bitcast.9.refs_0_), channel_id=1, source_target_pairs={{0,1},{1,2},{2,3},{3,0},{4,5},{5,6},{6,7},{7,4},{8,9},{9,10},{10,1... | collective-permute-start | bytes 1572872 | tf_op jit(solution)/shard_map/ppermute | solution.py:466
  129.3 18.4 %collective-permute-start.3 = (bf16[128,2048]{1,0:T(8,128)(2,1)}, bf16[128,2048]{1,0:T(8,128)(2,1)}, u32[]{:S(2)}, u32[]{:S(2)}) collective-permute-start(bf16[128,2048]{1,0:T(8,128)(2,1)} %bitcast.9.refs_0_), channel_id=1, source_target_pairs={{0,3},{1,0},{2,1},{3,2},{4,7},{5,4},{6,5},{7,6},{8,11},{9,8},{10,9... | collective-permute-start | bytes 1572872 | tf_op jit(solution)/shard_map/ppermute | solution.py:467
  132.0 23.6 %collective-permute-start.8 = (bf16[128,2048]{1,0:T(8,128)(2,1)}, bf16[128,2048]{1,0:T(8,128)(2,1)}, u32[]{:S(2)}, u32[]{:S(2)}) collective-permute-start(bf16[128,2048]{1,0:T(8,128)(2,1)} %bitcast.13.refs_0_), channel_id=1, source_target_pairs={{0,3},{1,0},{2,1},{3,2},{4,7},{5,4},{6,5},{7,6},{8,11},{9,8},{10,9... | collective-permute-start | bytes 1572872 | tf_op jit(solution)/shard_map/ppermute | solution.py:466
  144.5 16.2 %collective-permute-start.4 = (bf16[128,2048]{1,0:T(8,128)(2,1)}, bf16[128,2048]{1,0:T(8,128)(2,1)S(1)}, u32[]{:S(2)}, u32[]{:S(2)}) collective-permute-start(bf16[128,2048]{1,0:T(8,128)(2,1)} %collective-permute-done.2.refs_1_), channel_id=1, source_target_pairs={{0,1},{1,2},{2,3},{3,0},{4,5},{5,6},{6,7},{7,4},{8,9},{9,10},{10,1... | collective-permute-start | bytes 1572872 | tf_op jit(solution)/shard_map/ppermute | solution.py:468
  144.5 27.6 %collective-permute-start.9 = (bf16[128,2048]{1,0:T(8,128)(2,1)}, bf16[128,2048]{1,0:T(8,128)(2,1)}, u32[]{:S(2)}, u32[]{:S(2)}) collective-permute-start(bf16[128,2048]{1,0:T(8,128)(2,1)} %bitcast.13.refs_0_), channel_id=1, source_target_pairs={{0,1},{1,2},{2,3},{3,0},{4,5},{5,6},{6,7},{7,4},{8,9},{9,10},{10,1... | collective-permute-start | bytes 1572872 | tf_op jit(solution)/shard_map/ppermute | solution.py:467
  144.7 34.6 %collective-permute-start.17 = (bf16[128,2048]{1,0:T(8,128)(2,1)}, bf16[128,2048]{1,0:T(8,128)(2,1)S(1)}, u32[]{:S(2)}, u32[]{:S(2)}) collective-permute-start(bf16[128,2048]{1,0:T(8,128)(2,1)} %bitcast.17.refs_0_), channel_id=1, source_target_pairs={{0,3},{1,0},{2,1},{3,2},{4,7},{5,4},{6,5},{7,6},{8,11},{9,8},{10,9... | collective-permute-start | bytes 1572872 | tf_op jit(solution)/shard_map/ppermute | solution.py:467
  147.7 35.4 %collective-permute-start.16 = (bf16[128,2048]{1,0:T(8,128)(2,1)}, bf16[128,2048]{1,0:T(8,128)(2,1)S(1)}, u32[]{:S(2)}, u32[]{:S(2)}) collective-permute-start(bf16[128,2048]{1,0:T(8,128)(2,1)} %bitcast.17.refs_0_), channel_id=1, source_target_pairs={{0,1},{1,2},{2,3},{3,0},{4,5},{5,6},{6,7},{7,4},{8,9},{9,10},{10,1... | collective-permute-start | bytes 1572872 | tf_op jit(solution)/shard_map/ppermute | solution.py:466
  155.5 73.0 %collective-permute-start.7 = (bf16[128,2048]{1,0:T(8,128)(2,1)S(1)}, bf16[128,2048]{1,0:T(8,128)(2,1)S(1)}, u32[]{:S(2)}, u32[]{:S(2)}) collective-permute-start(bf16[128,2048]{1,0:T(8,128)(2,1)S(1)} %get-tuple-element.34), channel_id=1, source_target_pairs={{0,1},{1,2},{2,3},{3,0},{4,5},{5,6},{6,7},{7,4},{8,9},{9,10},{10,1... | collective-permute-start | bytes 1572872 | tf_op jit(solution)/shard_map/ppermute | solution.py:473
  160.7 29.8 %collective-permute-start.10 = (bf16[128,2048]{1,0:T(8,128)(2,1)}, bf16[128,2048]{1,0:T(8,128)(2,1)S(1)}, u32[]{:S(2)}, u32[]{:S(2)}) collective-permute-start(bf16[128,2048]{1,0:T(8,128)(2,1)} %collective-permute-done.8.refs_1_), channel_id=1, source_target_pairs={{0,3},{1,0},{2,1},{3,2},{4,7},{5,4},{6,5},{7,6},{8,11},{9,8},{10,9... | collective-permute-start | bytes 1572872 | tf_op jit(solution)/shard_map/ppermute | solution.py:468
  172.0 22.0 %collective-permute-start.5 = (bf16[128,2048]{1,0:T(8,128)(2,1)S(1)}, bf16[128,2048]{1,0:T(8,128)(2,1)S(1)}, u32[]{:S(2)}, u32[]{:S(2)}) collective-permute-start(bf16[128,2048]{1,0:T(8,128)(2,1)S(1)} %shard_map.162), channel_id=1, source_target_pairs={{0,3},{1,0},{2,1},{3,2},{4,7},{5,4},{6,5},{7,6},{8,11},{9,8},{10,9... | collective-permute-start | bytes 1572872 | tf_op jit(solution)/shard_map/ppermute | solution.py:471
  179.3 64.2 %collective-permute-start.13 = (bf16[128,2048]{1,0:T(8,128)(2,1)}, bf16[128,2048]{1,0:T(8,128)(2,1)}, u32[]{:S(2)}, u32[]{:S(2)}) collective-permute-start(bf16[128,2048]{1,0:T(8,128)(2,1)} %get-tuple-element.37), channel_id=1, source_target_pairs={{0,3},{1,0},{2,1},{3,2},{4,7},{5,4},{6,5},{7,6},{8,11},{9,8},{10,9... | collective-permute-start | bytes 1572872 | tf_op jit(solution)/shard_map/ppermute | solution.py:473
  190.4 67.0 %collective-permute-start.21 = (bf16[128,2048]{1,0:T(8,128)(2,1)}, bf16[128,2048]{1,0:T(8,128)(2,1)}, u32[]{:S(2)}, u32[]{:S(2)}) collective-permute-start(bf16[128,2048]{1,0:T(8,128)(2,1)} %get-tuple-element.42), channel_id=1, source_target_pairs={{0,1},{1,2},{2,3},{3,0},{4,5},{5,6},{6,7},{7,4},{8,9},{9,10},{10,1... | collective-permute-start | bytes 1572872 | tf_op jit(solution)/shard_map/ppermute | solution.py:473
  190.5 27.4 %collective-permute-start.18 = (bf16[128,2048]{1,0:T(8,128)(2,1)}, bf16[128,2048]{1,0:T(8,128)(2,1)S(1)}, u32[]{:S(2)}, u32[]{:S(2)}) collective-permute-start(bf16[128,2048]{1,0:T(8,128)(2,1)} %copy-done.20), channel_id=1, source_target_pairs={{0,1},{1,2},{2,3},{3,0},{4,5},{5,6},{6,7},{7,4},{8,9},{9,10},{10,1... | collective-permute-start | bytes 1572872 | tf_op jit(solution)/shard_map/ppermute | solution.py:468
  194.0 33.5 %collective-permute-start.11 = (bf16[128,2048]{1,0:T(8,128)(2,1)S(1)}, bf16[128,2048]{1,0:T(8,128)(2,1)S(1)}, u32[]{:S(2)}, u32[]{:S(2)}) collective-permute-start(bf16[128,2048]{1,0:T(8,128)(2,1)S(1)} %shard_map.165), channel_id=1, source_target_pairs={{0,1},{1,2},{2,3},{3,0},{4,5},{5,6},{6,7},{7,4},{8,9},{9,10},{10,1... | collective-permute-start | bytes 1572872 | tf_op jit(solution)/shard_map/ppermute | solution.py:471
  218.0 12.6 %collective-permute-start.6 = (bf16[128,2048]{1,0:T(8,128)(2,1)S(1)}, bf16[128,2048]{1,0:T(8,128)(2,1)S(1)}, u32[]{:S(2)}, u32[]{:S(2)}) collective-permute-start(bf16[128,2048]{1,0:T(8,128)(2,1)S(1)} %add_convert_fusion.5), channel_id=1, source_target_pairs={{0,3},{1,0},{2,1},{3,2},{4,7},{5,4},{6,5},{7,6},{8,11},{9,8},{10,9... | collective-permute-start | bytes 1572872 | tf_op jit(solution)/shard_map/ppermute | solution.py:472
  227.5 12.3 %collective-permute-start.19 = (bf16[128,2048]{1,0:T(8,128)(2,1)S(1)}, bf16[128,2048]{1,0:T(8,128)(2,1)S(1)}, u32[]{:S(2)}, u32[]{:S(2)}) collective-permute-start(bf16[128,2048]{1,0:T(8,128)(2,1)S(1)} %shard_map.169), channel_id=1, source_target_pairs={{0,3},{1,0},{2,1},{3,2},{4,7},{5,4},{6,5},{7,6},{8,11},{9,8},{10,9... | collective-permute-start | bytes 1572872 | tf_op jit(solution)/shard_map/ppermute | solution.py:471
  228.5 15.0 %collective-permute-start.12 = (bf16[128,2048]{1,0:T(8,128)(2,1)}, bf16[128,2048]{1,0:T(8,128)(2,1)}, u32[]{:S(2)}, u32[]{:S(2)}) collective-permute-start(bf16[128,2048]{1,0:T(8,128)(2,1)} %add_convert_fusion.3), channel_id=1, source_target_pairs={{0,1},{1,2},{2,3},{3,0},{4,5},{5,6},{6,7},{7,4},{8,9},{9,10},{10,1... | collective-permute-start | bytes 1572872 | tf_op jit(solution)/shard_map/ppermute | solution.py:472
  231.6 21.6 %all-to-all-start.5 = ((bf16[16,8,2048]{2,1,0:T(8,128)(2,1)}), bf16[16,8,2048]{2,1,0:T(8,128)(2,1)S(1)}, u32[]{:S(2)}, u32[]{:S(2)}) async-start(bf16[16,8,2048]{2,1,0:T(8,128)(2,1)} %fusion), calls=%async_computation.5 | async-start | bytes 1048576 | tf_op jit(solution)/shard_map/all_to_all | solution.py:475
  241.9 15.5 %collective-permute-start.20 = (bf16[128,2048]{1,0:T(8,128)(2,1)S(1)}, bf16[128,2048]{1,0:T(8,128)(2,1)}, u32[]{:S(2)}, u32[]{:S(2)}) collective-permute-start(bf16[128,2048]{1,0:T(8,128)(2,1)S(1)} %add_convert_fusion.1), channel_id=1, source_target_pairs={{0,3},{1,0},{2,1},{3,2},{4,7},{5,4},{6,5},{7,6},{8,11},{9,8},{10,9... | collective-permute-start | bytes 1572872 | tf_op jit(solution)/shard_map/ppermute | solution.py:472
  253.1 20.4 %all-to-all-start.7 = ((bf16[16,8,2048]{2,1,0:T(8,128)(2,1)}), bf16[16,8,2048]{2,1,0:T(8,128)(2,1)S(1)}, u32[]{:S(2)}, u32[]{:S(2)}) async-start(bf16[16,8,2048]{2,1,0:T(8,128)(2,1)} %fusion.1), calls=%async_computation.7 | async-start | bytes 1048576 | tf_op jit(solution)/shard_map/all_to_all | solution.py:475
  273.5 20.2 %all-to-all-start.9 = ((bf16[16,8,2048]{2,1,0:T(8,128)(2,1)}), bf16[16,8,2048]{2,1,0:T(8,128)(2,1)S(1)}, u32[]{:S(2)}, u32[]{:S(2)}) async-start(bf16[16,8,2048]{2,1,0:T(8,128)(2,1)} %fusion.2), calls=%async_computation.9 | async-start | bytes 1048576 | tf_op jit(solution)/shard_map/all_to_all | solution.py:475
  281.7 16.4 %collective-permute-start.14 = (bf16[64,2048]{1,0:T(8,128)(2,1)S(1)}, bf16[64,2048]{1,0:T(8,128)(2,1)S(1)}, u32[]{:S(2)}, u32[]{:S(2)}) collective-permute-start(bf16[64,2048]{1,0:T(8,128)(2,1)S(1)} %get-tuple-element.39), channel_id=1, source_target_pairs={{0,16},{8,24},{16,0},{24,8},{1,17},{9,25},{17,1},{25,9},{2,18},{10... | collective-permute-start | bytes 786440 | tf_op jit(solution)/shard_map/ppermute | solution.py:493
  296.0 8.8 %collective-permute-start.22 = (bf16[64,2048]{1,0:T(8,128)(2,1)S(1)}, bf16[64,2048]{1,0:T(8,128)(2,1)S(1)}, u32[]{:S(2)}, u32[]{:S(2)}) collective-permute-start(bf16[64,2048]{1,0:T(8,128)(2,1)S(1)} %get-tuple-element.43), channel_id=1, source_target_pairs={{0,8},{8,16},{16,24},{24,0},{1,9},{9,17},{17,25},{25,1},{2,10},{10... | collective-permute-start | bytes 786440 | tf_op jit(solution)/shard_map/ppermute | solution.py:493
  296.1 9.6 %collective-permute-start.23 = (bf16[64,2048]{1,0:T(8,128)(2,1)S(1)}, bf16[64,2048]{1,0:T(8,128)(2,1)S(1)}, u32[]{:S(2)}, u32[]{:S(2)}) collective-permute-start(bf16[64,2048]{1,0:T(8,128)(2,1)S(1)} %get-tuple-element.44), channel_id=1, source_target_pairs={{0,24},{8,0},{16,8},{24,16},{1,25},{9,1},{17,9},{25,17},{2,26},{10... | collective-permute-start | bytes 786440 | tf_op jit(solution)/shard_map/ppermute | solution.py:493
  (22 other events, 378.9 us)

commit v3 on v2

--- a/solution.py
+++ b/solution.py
@@ -96,13 +96,10 @@
     cumulative = sum(dot(lower, part, 1, 1) for part in three_parts(decay_ref[...]))
     share = out_ref.shape[1] - TILE
     per_head = HEAD_DIM // share
-    lane = iota((rows, heads), 1)
-
-    @pl.loop(0, heads)
-    def _(h):
-        cols = pl.ds(pl.multiple_of(h * HEAD_DIM, HEAD_DIM), HEAD_DIM)
+    for h in range(heads):
+        cols = slice(h * HEAD_DIM, (h + 1) * HEAD_DIM)
         keys = turned(k_ref[:, cols].astype(F32), cosine, sine) * HEAD_DIM ** (-0.5)
-        column = jnp.sum(jnp.where(lane == h, cumulative, 0.0), axis=1, keepdims=True)
+        column = cumulative[:, h : h + 1]
         total = column[rows - 1 : rows, :]
         tail = keys * jnp.exp(total - column)
         state = dot(tail.astype(BF16), v_ref[:, cols], 0, 0)
@@ -175,9 +172,8 @@
 
 
 def mix_kernel(inner_ref, lead_ref, enter_ref, gate_ref, gain_ref, weight_ref, out_ref, hidden_ref):
-    @pl.loop(0, inner_ref.shape[1] // HEAD_DIM)
-    def _(h):
-        cols = pl.ds(pl.multiple_of(h * HEAD_DIM, HEAD_DIM), HEAD_DIM)
+    for h in range(inner_ref.shape[1] // HEAD_DIM):
+        cols = slice(h * HEAD_DIM, (h + 1) * HEAD_DIM)
         kept = inner_ref[:, cols] + dot(lead_ref[:, cols], enter_ref[cols, :])
         centred = kept - jnp.mean(kept, axis=-1, keepdims=True)
         variance = jnp.mean(centred * centred, axis=-1, keepdims=True)
@@ -185,7 +181,6 @@
         opened = gate / (1.0 + jnp.exp(-gate))
         scaled = centred * lax.rsqrt(variance + group_eps)
         hidden_ref[:, cols] = (scaled * gain_ref[:, cols] * opened).astype(BF16)
-
     step = 512
 
     @pl.loop(0, out_ref.shape[1] // step)
@@ -238,7 +233,7 @@
         pick = (slot[:, None, :] == line).astype(F32).reshape(dests * TILE, block)
         picks.append(pick.astype(BF16))
     pick = jnp.concatenate(picks, axis=1)
-    step = 256
+    step = 512
 
     @pl.loop(0, width // step)
     def _(n):
@@ -278,7 +273,7 @@
                 for part in parts
             ]
         )
-    step = 256
+    step = 512
 
     @pl.loop(0, outs[0].shape[1] // step)
     def _(n):

time: 310 us -> 307 us (level)
  Pallas kernels: 52.2 us -> 48.1 us
    pallas_call x17, Pallas kernels: 52.2 us -> 48.1 us  [call(): pl.pallas_call(kernel, out_shape=out_shape, in_specs=specs, out_specs=out...]
  transfers between devices with their start and end apart: 32 -> 32, of which waited for: 21 -> 21; matrix products, arithmetic and copies ran while one was open for 3% -> 3% of each run, Pallas kernels for 14% -> 13%
where the time goes in v3:
time: 307 us; the launch traced here: 304 us
  waiting for transfers between devices  157 us (51%)
  starting transfers between devices  54.6 us (18%)
  Pallas kernels  48.1 us (16%)
  blocking collectives  27.2 us (9%)
  other arithmetic  8.76 us (3%)
  local copies, waits for them, and re-layouts  8.29 us (3%)
    pallas_call x17, Pallas kernels, call(): pl.pallas_call(kernel, out_shape=out_shape, in_specs=specs, out_specs=out...  48.1 us
    all_to_all x3, waiting for transfers between devices, body(): lax.all_to_all(total.reshape(dests, TILE, width), ('z', 'c'), 0, 0, tiled...  31.3 us
    ppermute x3, waiting for transfers between devices, body(): far = lax.ppermute(one, 'tp', first)  28.1 us
    ppermute x3, waiting for transfers between devices, body(): near.append(lax.ppermute(extended, 'x', ring(x_count, -d)))  20.4 us
    all_to_all x3, waiting for transfers between devices, body(): lax.all_to_all(piece.reshape(dests, TILE, width), ('z', 'c'), 0, 0, tiled...  18.6 us
    ppermute x3, waiting for transfers between devices, body(): one = lax.ppermute(own, 'tp', first)  18.4 us
    all_to_all x1, blocking collectives, body(): groups = lax.all_to_all(group, 'z', 0, 0, tiled=True)  16.8 us
    all_to_all x1, waiting for transfers between devices, body(): lax.all_to_all(mixed.reshape(tp_count, rows_own, width), 'tp', 0, 0, tile...  14.6 us
  transfers between devices with their start and end apart: 32, of which 21 were waited for; matrix products, arithmetic and copies ran while one was open for 3% of the time, Pallas kernels for 13%

profile of v3, /device:TPU:2, one launch (start us, length us, event | category | flops | bytes accessed | tf_op | source)
XLA Modules:
  0.0 304.1 jit_solution(11095022375264007238)
XLA Ops:
  2.8 10.3 %all_to_all.50.in_ref = bf16[8,72,128]{2,1,0:T(8,128)(2,1)S(1)} all-to-all(bf16[8,72,128]{2,1,0:T(8,128)(2,1)} %shard_map.155), channel_id=1, replica_groups=mesh['z'=8,'x'=4,'c'=2,'tp'=4] {'x','c'}, dimensions={0} | all-to-all | bytes 294912 | tf_op jit(solution)/shard_map/all_to_all | solution.py:397
  13.2 16.8 %all_to_all.51.in_ref = bf16[8,72,128]{2,1,0:T(8,128)(2,1)S(1)} all-to-all(bf16[8,72,128]{2,1,0:T(8,128)(2,1)S(1)} %get-tuple-element.27), channel_id=1, replica_groups=mesh['z'=8,'x'=4,'c'=2,'tp'=4] {'z'}, dimensions={0} | all-to-all | bytes 294912 | tf_op jit(solution)/shard_map/all_to_all | solution.py:412
  30.7 4.7 %all-to-all-start.2 = ((bf16[8,64,128]{2,1,0:T(8,128)(2,1)}), bf16[8,64,128]{2,1,0:T(8,128)(2,1)S(1)}, u32[]{:S(2)}, u32[]{:S(2)}) async-start(bf16[8,64,128]{2,1,0:T(8,128)(2,1)} %shard_map.157), calls=%async_computation.2 | async-start | bytes 262144 | tf_op jit(solution)/shard_map/all_to_all | solution.py:419
  35.5 4.0 %shard_map.154 = (f32[256,512]{1,0:T(8,128)}, bf16[256,512]{1,0:T(8,128)(2,1)}) custom-call(s32[1]{0:T(128)} %bitcast.index_ref, bf16[256,512]{1,0:T(8,128)(2,1)} %q_ref.1, bf16[256,512]{1,0:T(8,128)(2,1)} %k_ref.3, bf16[256,512]{1,0:T(8,128)(2,1)} %v_ref.3, f32[4,256]{1,0:T(4,128)} %bitcast.32, f32[256,128]{1,0:T(8,128)} %constant.31.clone.own_ref, ...), custom_call_target="tpu_custom_call" | custom-call | flops 134217728 | bytes 954372 | tf_op jit(solution)/shard_map/pallas_call | solution.py:55
  45.0 4.6 %all-to-all-start.3 = ((bf16[4,64,2048]{2,1,0:T(8,128)(2,1)}), bf16[4,64,2048]{2,1,0:T(8,128)(2,1)S(1)}, u32[]{:S(2)}, u32[]{:S(2)}) async-start(bf16[4,64,2048]{2,1,0:T(8,128)(2,1)} %bitcast.5), calls=%async_computation.3 | async-start | bytes 2097152 | tf_op jit(solution)/shard_map/all_to_all | solution.py:427
  49.8 14.6 %all-to-all-done.3.sum_ref = bf16[4,64,2048]{2,1,0:T(8,128)(2,1)S(1)} async-done(((bf16[4,64,2048]{2,1,0:T(8,128)(2,1)}), bf16[4,64,2048]{2,1,0:T(8,128)(2,1)S(1)}, u32[]{:S(2)}, u32[]{:S(2)}) %all-to-all-start.3) | async-done | bytes 1048608 | tf_op jit(solution)/shard_map/all_to_all | solution.py:427
  67.7 5.8 %collective-permute-done.1.refs_1_ = bf16[64,2176]{1,0:T(8,128)(2,1)S(1)} collective-permute-done((bf16[64,2176]{1,0:T(8,128)(2,1)S(1)}, bf16[64,2176]{1,0:T(8,128)(2,1)S(1)}, u32[]{:S(2)}, u32[]{:S(2)}) %collective-permute-start.1) | collective-permute-done | bytes 278560 | tf_op jit(solution)/shard_map/ppermute | solution.py:440
  73.4 5.7 %collective-permute-done.refs_0_ = bf16[64,2176]{1,0:T(8,128)(2,1)S(1)} collective-permute-done((bf16[64,2176]{1,0:T(8,128)(2,1)S(1)}, bf16[64,2176]{1,0:T(8,128)(2,1)S(1)}, u32[]{:S(2)}, u32[]{:S(2)}) %collective-permute-start) | collective-permute-done | bytes 278560 | tf_op jit(solution)/shard_map/ppermute | solution.py:440
  81.8 4.2 %all-to-all-start.6 = ((bf16[16,8,2048]{2,1,0:T(8,128)(2,1)}), bf16[16,8,2048]{2,1,0:T(8,128)(2,1)}, u32[]{:S(2)}, u32[]{:S(2)}) async-start(bf16[16,8,2048]{2,1,0:T(8,128)(2,1)} %bitcast.12), calls=%async_computation.6 | async-start | bytes 1048576 | tf_op jit(solution)/shard_map/all_to_all | solution.py:459
  88.1 14.0 %all-to-all-done.6 = bf16[16,8,2048]{2,1,0:T(8,128)(2,1)} async-done(((bf16[16,8,2048]{2,1,0:T(8,128)(2,1)}), bf16[16,8,2048]{2,1,0:T(8,128)(2,1)}, u32[]{:S(2)}, u32[]{:S(2)}) %all-to-all-start.6) | async-done | bytes 524320 | tf_op jit(solution)/shard_map/all_to_all | solution.py:459
  102.0 4.3 %all-to-all-start.4 = ((bf16[16,8,2048]{2,1,0:T(8,128)(2,1)}), bf16[16,8,2048]{2,1,0:T(8,128)(2,1)}, u32[]{:S(2)}, u32[]{:S(2)}) async-start(bf16[16,8,2048]{2,1,0:T(8,128)(2,1)} %bitcast.8), calls=%async_computation.4 | async-start | bytes 1048576 | tf_op jit(solution)/shard_map/all_to_all | solution.py:459
  106.4 8.9 %collective-permute-done.15.refs_0_ = bf16[64,2176]{1,0:T(8,128)(2,1)S(1)} collective-permute-done((bf16[64,2176]{1,0:T(8,128)(2,1)S(1)}, bf16[64,2176]{1,0:T(8,128)(2,1)S(1)}, u32[]{:S(2)}, u32[]{:S(2)}) %collective-permute-start.15) | collective-permute-done | bytes 278560 | tf_op jit(solution)/shard_map/ppermute | solution.py:440
  118.0 4.4 %all-to-all-done.4 = bf16[16,8,2048]{2,1,0:T(8,128)(2,1)} async-done(((bf16[16,8,2048]{2,1,0:T(8,128)(2,1)}), bf16[16,8,2048]{2,1,0:T(8,128)(2,1)}, u32[]{:S(2)}, u32[]{:S(2)}) %all-to-all-start.4) | async-done | bytes 524320 | tf_op jit(solution)/shard_map/all_to_all | solution.py:459
  122.4 4.2 %all-to-all-start.8 = ((bf16[16,8,2048]{2,1,0:T(8,128)(2,1)}), bf16[16,8,2048]{2,1,0:T(8,128)(2,1)}, u32[]{:S(2)}, u32[]{:S(2)}) async-start(bf16[16,8,2048]{2,1,0:T(8,128)(2,1)} %bitcast.16), calls=%async_computation.8 | async-start | bytes 1048576 | tf_op jit(solution)/shard_map/all_to_all | solution.py:459
  130.0 12.5 %collective-permute-done.2.refs_1_ = bf16[128,2048]{1,0:T(8,128)(2,1)} collective-permute-done((bf16[128,2048]{1,0:T(8,128)(2,1)}, bf16[128,2048]{1,0:T(8,128)(2,1)}, u32[]{:S(2)}, u32[]{:S(2)}) %collective-permute-start.2) | collective-permute-done | bytes 524320 | tf_op jit(solution)/shard_map/ppermute | solution.py:461
  145.7 5.7 %shard_map.161 = (bf16[128,2048]{1,0:T(8,128)(2,1)S(1)}, bf16[128,2048]{1,0:T(8,128)(2,1)S(1)}, bf16[128,2048]{1,0:T(8,128)(2,1)S(1)}) custom-call(bf16[128,2048]{1,0:T(8,128)(2,1)} %bitcast.9.refs_0_, bf16[128,2048]{1,0:T(8,128)(2,1)} %collective-permute-done.2.refs_1_, bf16[128,2048]{1,0:T(8,128)(2,1)} %collective-permute-done.3.refs_2_, ...), custom_call_target="tpu_custom_call" | custom-call | flops 2415919104 | bytes 7864320 | tf_op jit(solution)/shard_map/pallas_call | solution.py:55
  153.5 5.2 %collective-permute-done.4.refs_0_ = bf16[128,2048]{1,0:T(8,128)(2,1)S(1)} collective-permute-done((bf16[128,2048]{1,0:T(8,128)(2,1)}, bf16[128,2048]{1,0:T(8,128)(2,1)S(1)}, u32[]{:S(2)}, u32[]{:S(2)}) %collective-permute-start.4) | collective-permute-done | bytes 524320 | tf_op jit(solution)/shard_map/ppermute | solution.py:463
  161.9 8.1 %collective-permute-done.9.refs_2_ = bf16[128,2048]{1,0:T(8,128)(2,1)} collective-permute-done((bf16[128,2048]{1,0:T(8,128)(2,1)}, bf16[128,2048]{1,0:T(8,128)(2,1)}, u32[]{:S(2)}, u32[]{:S(2)}) %collective-permute-start.9) | collective-permute-done | bytes 524320 | tf_op jit(solution)/shard_map/ppermute | solution.py:462
  170.0 6.5 %shard_map.164 = (bf16[128,2048]{1,0:T(8,128)(2,1)S(1)}, bf16[128,2048]{1,0:T(8,128)(2,1)S(1)}, bf16[128,2048]{1,0:T(8,128)(2,1)}) custom-call(bf16[128,2048]{1,0:T(8,128)(2,1)} %bitcast.13.refs_0_, bf16[128,2048]{1,0:T(8,128)(2,1)} %collective-permute-done.8.refs_1_, bf16[128,2048]{1,0:T(8,128)(2,1)} %collective-permute-done.9.refs_2_, ...), custom_call_target="tpu_custom_call" | custom-call | flops 2415919104 | bytes 7864320 | tf_op jit(solution)/shard_map/pallas_call | solution.py:55
  177.3 3.9 %collective-permute-done.16.refs_1_ = bf16[128,2048]{1,0:T(8,128)(2,1)S(1)} collective-permute-done((bf16[128,2048]{1,0:T(8,128)(2,1)}, bf16[128,2048]{1,0:T(8,128)(2,1)S(1)}, u32[]{:S(2)}, u32[]{:S(2)}) %collective-permute-start.16) | collective-permute-done | bytes 524320 | tf_op jit(solution)/shard_map/ppermute | solution.py:461
  181.9 6.4 %shard_map.168 = (bf16[128,2048]{1,0:T(8,128)(2,1)S(1)}, bf16[128,2048]{1,0:T(8,128)(2,1)S(1)}, bf16[128,2048]{1,0:T(8,128)(2,1)}) custom-call(bf16[128,2048]{1,0:T(8,128)(2,1)} %bitcast.17.refs_0_, bf16[128,2048]{1,0:T(8,128)(2,1)} %copy-done.20, bf16[128,2048]{1,0:T(8,128)(2,1)} %copy-done.21, bf16[1,2048,512]{2,1,0:T(8,128)(2,1)S(1)} %copy-done.1, ...), custom_call_target="tpu_custom_call" | custom-call | flops 2415919104 | bytes 7864320 | tf_op jit(solution)/shard_map/pallas_call | solution.py:55
  188.7 3.3 %shard_map.165 = bf16[128,2048]{1,0:T(8,128)(2,1)S(1)} custom-call(bf16[128,2048]{1,0:T(8,128)(2,1)S(1)} %collective-permute-done.10.refs_0_, bf16[1,2048,512]{2,1,0:T(8,128)(2,1)S(1)} %copy-done.1, bf16[1,2048,512]{2,1,0:T(8,128)(2,1)} %refs_2_.5, bf16[1,512,2048]{2,1,0:T(8,128)(2,1)} %refs_3_.11), custom_call_target="tpu_custom_call" | custom-call | flops 805306368 | bytes 6815744 | tf_op jit(solution)/shard_map/pallas_call | solution.py:55
  193.0 22.9 %collective-permute-done.18.refs_0_ = bf16[128,2048]{1,0:T(8,128)(2,1)S(1)} collective-permute-done((bf16[128,2048]{1,0:T(8,128)(2,1)}, bf16[128,2048]{1,0:T(8,128)(2,1)S(1)}, u32[]{:S(2)}, u32[]{:S(2)}) %collective-permute-start.18) | collective-permute-done | bytes 524320 | tf_op jit(solution)/shard_map/ppermute | solution.py:463
  215.9 3.2 %shard_map.169 = bf16[128,2048]{1,0:T(8,128)(2,1)S(1)} custom-call(bf16[128,2048]{1,0:T(8,128)(2,1)S(1)} %collective-permute-done.18.refs_0_, bf16[1,2048,512]{2,1,0:T(8,128)(2,1)S(1)} %copy-done.1, bf16[1,2048,512]{2,1,0:T(8,128)(2,1)} %refs_2_.5, bf16[1,512,2048]{2,1,0:T(8,128)(2,1)} %refs_3_.11), custom_call_target="tpu_custom_call" | custom-call | flops 805306368 | bytes 6815744 | tf_op jit(solution)/shard_map/pallas_call | solution.py:55
  219.2 6.3 %collective-permute-done.11 = bf16[128,2048]{1,0:T(8,128)(2,1)S(1)} collective-permute-done((bf16[128,2048]{1,0:T(8,128)(2,1)S(1)}, bf16[128,2048]{1,0:T(8,128)(2,1)S(1)}, u32[]{:S(2)}, u32[]{:S(2)}) %collective-permute-start.11) | collective-permute-done | bytes 524320 | tf_op jit(solution)/shard_map/ppermute | solution.py:466
  229.5 5.6 %all-to-all-start.5 = ((bf16[16,8,2048]{2,1,0:T(8,128)(2,1)}), bf16[16,8,2048]{2,1,0:T(8,128)(2,1)S(1)}, u32[]{:S(2)}, u32[]{:S(2)}) async-start(bf16[16,8,2048]{2,1,0:T(8,128)(2,1)} %fusion), calls=%async_computation.5 | async-start | bytes 1048576 | tf_op jit(solution)/shard_map/all_to_all | solution.py:470
  243.8 7.4 %all-to-all-done.5 = bf16[16,8,2048]{2,1,0:T(8,128)(2,1)S(1)} async-done(((bf16[16,8,2048]{2,1,0:T(8,128)(2,1)}), bf16[16,8,2048]{2,1,0:T(8,128)(2,1)S(1)}, u32[]{:S(2)}, u32[]{:S(2)}) %all-to-all-start.5) | async-done | bytes 524320 | tf_op jit(solution)/shard_map/all_to_all | solution.py:470
  251.1 4.2 %all-to-all-start.7 = ((bf16[16,8,2048]{2,1,0:T(8,128)(2,1)}), bf16[16,8,2048]{2,1,0:T(8,128)(2,1)S(1)}, u32[]{:S(2)}, u32[]{:S(2)}) async-start(bf16[16,8,2048]{2,1,0:T(8,128)(2,1)} %fusion.1), calls=%async_computation.7 | async-start | bytes 1048576 | tf_op jit(solution)/shard_map/all_to_all | solution.py:470
  257.7 13.9 %all-to-all-done.7 = bf16[16,8,2048]{2,1,0:T(8,128)(2,1)S(1)} async-done(((bf16[16,8,2048]{2,1,0:T(8,128)(2,1)}), bf16[16,8,2048]{2,1,0:T(8,128)(2,1)S(1)}, u32[]{:S(2)}, u32[]{:S(2)}) %all-to-all-start.7) | async-done | bytes 524320 | tf_op jit(solution)/shard_map/all_to_all | solution.py:470
  271.5 4.0 %all-to-all-start.9 = ((bf16[16,8,2048]{2,1,0:T(8,128)(2,1)}), bf16[16,8,2048]{2,1,0:T(8,128)(2,1)S(1)}, u32[]{:S(2)}, u32[]{:S(2)}) async-start(bf16[16,8,2048]{2,1,0:T(8,128)(2,1)} %fusion.2), calls=%async_computation.9 | async-start | bytes 1048576 | tf_op jit(solution)/shard_map/all_to_all | solution.py:470
  281.7 10.1 %all-to-all-done.9 = bf16[16,8,2048]{2,1,0:T(8,128)(2,1)S(1)} async-done(((bf16[16,8,2048]{2,1,0:T(8,128)(2,1)}), bf16[16,8,2048]{2,1,0:T(8,128)(2,1)S(1)}, u32[]{:S(2)}, u32[]{:S(2)}) %all-to-all-start.9) | async-done | bytes 524320 | tf_op jit(solution)/shard_map/all_to_all | solution.py:470
  295.6 6.7 %collective-permute-done.22 = bf16[64,2048]{1,0:T(8,128)(2,1)S(1)} collective-permute-done((bf16[64,2048]{1,0:T(8,128)(2,1)S(1)}, bf16[64,2048]{1,0:T(8,128)(2,1)S(1)}, u32[]{:S(2)}, u32[]{:S(2)}) %collective-permute-start.22) | collective-permute-done | bytes 262176 | tf_op jit(solution)/shard_map/ppermute | solution.py:488
  (109 shorter events, 61.3 us)
Async XLA Ops:
  30.7 9.4 %all-to-all-start.2 = ((bf16[8,64,128]{2,1,0:T(8,128)(2,1)}), bf16[8,64,128]{2,1,0:T(8,128)(2,1)S(1)}, u32[]{:S(2)}, u32[]{:S(2)}) async-start(bf16[8,64,128]{2,1,0:T(8,128)(2,1)} %shard_map.157), calls=%async_computation.2 | async-start | bytes 262144 | tf_op jit(solution)/shard_map/all_to_all | solution.py:419
  45.0 19.5 %all-to-all-start.3 = ((bf16[4,64,2048]{2,1,0:T(8,128)(2,1)}), bf16[4,64,2048]{2,1,0:T(8,128)(2,1)S(1)}, u32[]{:S(2)}, u32[]{:S(2)}) async-start(bf16[4,64,2048]{2,1,0:T(8,128)(2,1)} %bitcast.5), calls=%async_computation.3 | async-start | bytes 2097152 | tf_op jit(solution)/shard_map/all_to_all | solution.py:427
  64.9 8.6 %collective-permute-start.1 = (bf16[64,2176]{1,0:T(8,128)(2,1)S(1)}, bf16[64,2176]{1,0:T(8,128)(2,1)S(1)}, u32[]{:S(2)}, u32[]{:S(2)}) collective-permute-start(bf16[64,2176]{1,0:T(8,128)(2,1)S(1)} %get-tuple-element.31.refs_0_), channel_id=1, source_target_pairs={{0,24},{8,0},{16,8},{24,16},{1,25},{9,1},{17,9},{25,17},{2,26},{10... | collective-permute-start | bytes 835592 | tf_op jit(solution)/shard_map/ppermute | solution.py:440
  66.4 12.8 %collective-permute-start = (bf16[64,2176]{1,0:T(8,128)(2,1)S(1)}, bf16[64,2176]{1,0:T(8,128)(2,1)S(1)}, u32[]{:S(2)}, u32[]{:S(2)}) collective-permute-start(bf16[64,2176]{1,0:T(8,128)(2,1)S(1)} %get-tuple-element.31.refs_0_), channel_id=1, source_target_pairs={{0,16},{8,24},{16,0},{24,8},{1,17},{9,25},{17,1},{25,9},{2,18},{10... | collective-permute-start | bytes 835592 | tf_op jit(solution)/shard_map/ppermute | solution.py:440
  81.8 20.2 %all-to-all-start.6 = ((bf16[16,8,2048]{2,1,0:T(8,128)(2,1)}), bf16[16,8,2048]{2,1,0:T(8,128)(2,1)}, u32[]{:S(2)}, u32[]{:S(2)}) async-start(bf16[16,8,2048]{2,1,0:T(8,128)(2,1)} %bitcast.12), calls=%async_computation.6 | async-start | bytes 1048576 | tf_op jit(solution)/shard_map/all_to_all | solution.py:459
  102.0 20.4 %all-to-all-start.4 = ((bf16[16,8,2048]{2,1,0:T(8,128)(2,1)}), bf16[16,8,2048]{2,1,0:T(8,128)(2,1)}, u32[]{:S(2)}, u32[]{:S(2)}) async-start(bf16[16,8,2048]{2,1,0:T(8,128)(2,1)} %bitcast.8), calls=%async_computation.4 | async-start | bytes 1048576 | tf_op jit(solution)/shard_map/all_to_all | solution.py:459
  106.3 9.0 %collective-permute-start.15 = (bf16[64,2176]{1,0:T(8,128)(2,1)S(1)}, bf16[64,2176]{1,0:T(8,128)(2,1)S(1)}, u32[]{:S(2)}, u32[]{:S(2)}) collective-permute-start(bf16[64,2176]{1,0:T(8,128)(2,1)S(1)} %get-tuple-element.31.refs_0_), channel_id=1, source_target_pairs={{0,8},{8,16},{16,24},{24,0},{1,9},{9,17},{17,25},{25,1},{2,10},{10... | collective-permute-start | bytes 835592 | tf_op jit(solution)/shard_map/ppermute | solution.py:440
  122.4 20.3 %all-to-all-start.8 = ((bf16[16,8,2048]{2,1,0:T(8,128)(2,1)}), bf16[16,8,2048]{2,1,0:T(8,128)(2,1)}, u32[]{:S(2)}, u32[]{:S(2)}) async-start(bf16[16,8,2048]{2,1,0:T(8,128)(2,1)} %bitcast.16), calls=%async_computation.8 | async-start | bytes 1048576 | tf_op jit(solution)/shard_map/all_to_all | solution.py:459
  126.6 15.8 %collective-permute-start.2 = (bf16[128,2048]{1,0:T(8,128)(2,1)}, bf16[128,2048]{1,0:T(8,128)(2,1)}, u32[]{:S(2)}, u32[]{:S(2)}) collective-permute-start(bf16[128,2048]{1,0:T(8,128)(2,1)} %bitcast.9.refs_0_), channel_id=1, source_target_pairs={{0,1},{1,2},{2,3},{3,0},{4,5},{5,6},{6,7},{7,4},{8,9},{9,10},{10,1... | collective-permute-start | bytes 1572872 | tf_op jit(solution)/shard_map/ppermute | solution.py:461
  127.3 18.4 %collective-permute-start.3 = (bf16[128,2048]{1,0:T(8,128)(2,1)}, bf16[128,2048]{1,0:T(8,128)(2,1)}, u32[]{:S(2)}, u32[]{:S(2)}) collective-permute-start(bf16[128,2048]{1,0:T(8,128)(2,1)} %bitcast.9.refs_0_), channel_id=1, source_target_pairs={{0,3},{1,0},{2,1},{3,2},{4,7},{5,4},{6,5},{7,6},{8,11},{9,8},{10,9... | collective-permute-start | bytes 1572872 | tf_op jit(solution)/shard_map/ppermute | solution.py:462
  129.9 23.6 %collective-permute-start.8 = (bf16[128,2048]{1,0:T(8,128)(2,1)}, bf16[128,2048]{1,0:T(8,128)(2,1)}, u32[]{:S(2)}, u32[]{:S(2)}) collective-permute-start(bf16[128,2048]{1,0:T(8,128)(2,1)} %bitcast.13.refs_0_), channel_id=1, source_target_pairs={{0,3},{1,0},{2,1},{3,2},{4,7},{5,4},{6,5},{7,6},{8,11},{9,8},{10,9... | collective-permute-start | bytes 1572872 | tf_op jit(solution)/shard_map/ppermute | solution.py:461
  142.4 16.2 %collective-permute-start.4 = (bf16[128,2048]{1,0:T(8,128)(2,1)}, bf16[128,2048]{1,0:T(8,128)(2,1)S(1)}, u32[]{:S(2)}, u32[]{:S(2)}) collective-permute-start(bf16[128,2048]{1,0:T(8,128)(2,1)} %collective-permute-done.2.refs_1_), channel_id=1, source_target_pairs={{0,1},{1,2},{2,3},{3,0},{4,5},{5,6},{6,7},{7,4},{8,9},{9,10},{10,1... | collective-permute-start | bytes 1572872 | tf_op jit(solution)/shard_map/ppermute | solution.py:463
  142.4 27.6 %collective-permute-start.9 = (bf16[128,2048]{1,0:T(8,128)(2,1)}, bf16[128,2048]{1,0:T(8,128)(2,1)}, u32[]{:S(2)}, u32[]{:S(2)}) collective-permute-start(bf16[128,2048]{1,0:T(8,128)(2,1)} %bitcast.13.refs_0_), channel_id=1, source_target_pairs={{0,1},{1,2},{2,3},{3,0},{4,5},{5,6},{6,7},{7,4},{8,9},{9,10},{10,1... | collective-permute-start | bytes 1572872 | tf_op jit(solution)/shard_map/ppermute | solution.py:462
  142.7 34.6 %collective-permute-start.17 = (bf16[128,2048]{1,0:T(8,128)(2,1)}, bf16[128,2048]{1,0:T(8,128)(2,1)S(1)}, u32[]{:S(2)}, u32[]{:S(2)}) collective-permute-start(bf16[128,2048]{1,0:T(8,128)(2,1)} %bitcast.17.refs_0_), channel_id=1, source_target_pairs={{0,3},{1,0},{2,1},{3,2},{4,7},{5,4},{6,5},{7,6},{8,11},{9,8},{10,9... | collective-permute-start | bytes 1572872 | tf_op jit(solution)/shard_map/ppermute | solution.py:462
  145.7 35.4 %collective-permute-start.16 = (bf16[128,2048]{1,0:T(8,128)(2,1)}, bf16[128,2048]{1,0:T(8,128)(2,1)S(1)}, u32[]{:S(2)}, u32[]{:S(2)}) collective-permute-start(bf16[128,2048]{1,0:T(8,128)(2,1)} %bitcast.17.refs_0_), channel_id=1, source_target_pairs={{0,1},{1,2},{2,3},{3,0},{4,5},{5,6},{6,7},{7,4},{8,9},{9,10},{10,1... | collective-permute-start | bytes 1572872 | tf_op jit(solution)/shard_map/ppermute | solution.py:461
  153.5 73.0 %collective-permute-start.7 = (bf16[128,2048]{1,0:T(8,128)(2,1)S(1)}, bf16[128,2048]{1,0:T(8,128)(2,1)S(1)}, u32[]{:S(2)}, u32[]{:S(2)}) collective-permute-start(bf16[128,2048]{1,0:T(8,128)(2,1)S(1)} %get-tuple-element.34), channel_id=1, source_target_pairs={{0,1},{1,2},{2,3},{3,0},{4,5},{5,6},{6,7},{7,4},{8,9},{9,10},{10,1... | collective-permute-start | bytes 1572872 | tf_op jit(solution)/shard_map/ppermute | solution.py:468
  158.7 29.8 %collective-permute-start.10 = (bf16[128,2048]{1,0:T(8,128)(2,1)}, bf16[128,2048]{1,0:T(8,128)(2,1)S(1)}, u32[]{:S(2)}, u32[]{:S(2)}) collective-permute-start(bf16[128,2048]{1,0:T(8,128)(2,1)} %collective-permute-done.8.refs_1_), channel_id=1, source_target_pairs={{0,3},{1,0},{2,1},{3,2},{4,7},{5,4},{6,5},{7,6},{8,11},{9,8},{10,9... | collective-permute-start | bytes 1572872 | tf_op jit(solution)/shard_map/ppermute | solution.py:463
  170.0 22.0 %collective-permute-start.5 = (bf16[128,2048]{1,0:T(8,128)(2,1)S(1)}, bf16[128,2048]{1,0:T(8,128)(2,1)S(1)}, u32[]{:S(2)}, u32[]{:S(2)}) collective-permute-start(bf16[128,2048]{1,0:T(8,128)(2,1)S(1)} %shard_map.162), channel_id=1, source_target_pairs={{0,3},{1,0},{2,1},{3,2},{4,7},{5,4},{6,5},{7,6},{8,11},{9,8},{10,9... | collective-permute-start | bytes 1572872 | tf_op jit(solution)/shard_map/ppermute | solution.py:466
  177.3 64.2 %collective-permute-start.13 = (bf16[128,2048]{1,0:T(8,128)(2,1)}, bf16[128,2048]{1,0:T(8,128)(2,1)}, u32[]{:S(2)}, u32[]{:S(2)}) collective-permute-start(bf16[128,2048]{1,0:T(8,128)(2,1)} %get-tuple-element.37), channel_id=1, source_target_pairs={{0,3},{1,0},{2,1},{3,2},{4,7},{5,4},{6,5},{7,6},{8,11},{9,8},{10,9... | collective-permute-start | bytes 1572872 | tf_op jit(solution)/shard_map/ppermute | solution.py:468
  188.4 67.0 %collective-permute-start.21 = (bf16[128,2048]{1,0:T(8,128)(2,1)}, bf16[128,2048]{1,0:T(8,128)(2,1)}, u32[]{:S(2)}, u32[]{:S(2)}) collective-permute-start(bf16[128,2048]{1,0:T(8,128)(2,1)} %get-tuple-element.42), channel_id=1, source_target_pairs={{0,1},{1,2},{2,3},{3,0},{4,5},{5,6},{6,7},{7,4},{8,9},{9,10},{10,1... | collective-permute-start | bytes 1572872 | tf_op jit(solution)/shard_map/ppermute | solution.py:468
  188.5 27.4 %collective-permute-start.18 = (bf16[128,2048]{1,0:T(8,128)(2,1)}, bf16[128,2048]{1,0:T(8,128)(2,1)S(1)}, u32[]{:S(2)}, u32[]{:S(2)}) collective-permute-start(bf16[128,2048]{1,0:T(8,128)(2,1)} %copy-done.20), channel_id=1, source_target_pairs={{0,1},{1,2},{2,3},{3,0},{4,5},{5,6},{6,7},{7,4},{8,9},{9,10},{10,1... | collective-permute-start | bytes 1572872 | tf_op jit(solution)/shard_map/ppermute | solution.py:463
  192.0 33.5 %collective-permute-start.11 = (bf16[128,2048]{1,0:T(8,128)(2,1)S(1)}, bf16[128,2048]{1,0:T(8,128)(2,1)S(1)}, u32[]{:S(2)}, u32[]{:S(2)}) collective-permute-start(bf16[128,2048]{1,0:T(8,128)(2,1)S(1)} %shard_map.165), channel_id=1, source_target_pairs={{0,1},{1,2},{2,3},{3,0},{4,5},{5,6},{6,7},{7,4},{8,9},{9,10},{10,1... | collective-permute-start | bytes 1572872 | tf_op jit(solution)/shard_map/ppermute | solution.py:466
  215.9 12.6 %collective-permute-start.6 = (bf16[128,2048]{1,0:T(8,128)(2,1)S(1)}, bf16[128,2048]{1,0:T(8,128)(2,1)S(1)}, u32[]{:S(2)}, u32[]{:S(2)}) collective-permute-start(bf16[128,2048]{1,0:T(8,128)(2,1)S(1)} %add_convert_fusion.5), channel_id=1, source_target_pairs={{0,3},{1,0},{2,1},{3,2},{4,7},{5,4},{6,5},{7,6},{8,11},{9,8},{10,9... | collective-permute-start | bytes 1572872 | tf_op jit(solution)/shard_map/ppermute | solution.py:467
  225.5 12.3 %collective-permute-start.19 = (bf16[128,2048]{1,0:T(8,128)(2,1)S(1)}, bf16[128,2048]{1,0:T(8,128)(2,1)S(1)}, u32[]{:S(2)}, u32[]{:S(2)}) collective-permute-start(bf16[128,2048]{1,0:T(8,128)(2,1)S(1)} %shard_map.169), channel_id=1, source_target_pairs={{0,3},{1,0},{2,1},{3,2},{4,7},{5,4},{6,5},{7,6},{8,11},{9,8},{10,9... | collective-permute-start | bytes 1572872 | tf_op jit(solution)/shard_map/ppermute | solution.py:466
  226.5 15.0 %collective-permute-start.12 = (bf16[128,2048]{1,0:T(8,128)(2,1)}, bf16[128,2048]{1,0:T(8,128)(2,1)}, u32[]{:S(2)}, u32[]{:S(2)}) collective-permute-start(bf16[128,2048]{1,0:T(8,128)(2,1)} %add_convert_fusion.3), channel_id=1, source_target_pairs={{0,1},{1,2},{2,3},{3,0},{4,5},{5,6},{6,7},{7,4},{8,9},{9,10},{10,1... | collective-permute-start | bytes 1572872 | tf_op jit(solution)/shard_map/ppermute | solution.py:467
  229.5 21.6 %all-to-all-start.5 = ((bf16[16,8,2048]{2,1,0:T(8,128)(2,1)}), bf16[16,8,2048]{2,1,0:T(8,128)(2,1)S(1)}, u32[]{:S(2)}, u32[]{:S(2)}) async-start(bf16[16,8,2048]{2,1,0:T(8,128)(2,1)} %fusion), calls=%async_computation.5 | async-start | bytes 1048576 | tf_op jit(solution)/shard_map/all_to_all | solution.py:470
  239.9 15.5 %collective-permute-start.20 = (bf16[128,2048]{1,0:T(8,128)(2,1)S(1)}, bf16[128,2048]{1,0:T(8,128)(2,1)}, u32[]{:S(2)}, u32[]{:S(2)}) collective-permute-start(bf16[128,2048]{1,0:T(8,128)(2,1)S(1)} %add_convert_fusion.1), channel_id=1, source_target_pairs={{0,3},{1,0},{2,1},{3,2},{4,7},{5,4},{6,5},{7,6},{8,11},{9,8},{10,9... | collective-permute-start | bytes 1572872 | tf_op jit(solution)/shard_map/ppermute | solution.py:467
  251.1 20.4 %all-to-all-start.7 = ((bf16[16,8,2048]{2,1,0:T(8,128)(2,1)}), bf16[16,8,2048]{2,1,0:T(8,128)(2,1)S(1)}, u32[]{:S(2)}, u32[]{:S(2)}) async-start(bf16[16,8,2048]{2,1,0:T(8,128)(2,1)} %fusion.1), calls=%async_computation.7 | async-start | bytes 1048576 | tf_op jit(solution)/shard_map/all_to_all | solution.py:470
  271.5 20.2 %all-to-all-start.9 = ((bf16[16,8,2048]{2,1,0:T(8,128)(2,1)}), bf16[16,8,2048]{2,1,0:T(8,128)(2,1)S(1)}, u32[]{:S(2)}, u32[]{:S(2)}) async-start(bf16[16,8,2048]{2,1,0:T(8,128)(2,1)} %fusion.2), calls=%async_computation.9 | async-start | bytes 1048576 | tf_op jit(solution)/shard_map/all_to_all | solution.py:470
  279.2 16.4 %collective-permute-start.14 = (bf16[64,2048]{1,0:T(8,128)(2,1)S(1)}, bf16[64,2048]{1,0:T(8,128)(2,1)S(1)}, u32[]{:S(2)}, u32[]{:S(2)}) collective-permute-start(bf16[64,2048]{1,0:T(8,128)(2,1)S(1)} %get-tuple-element.39), channel_id=1, source_target_pairs={{0,16},{8,24},{16,0},{24,8},{1,17},{9,25},{17,1},{25,9},{2,18},{10... | collective-permute-start | bytes 786440 | tf_op jit(solution)/shard_map/ppermute | solution.py:488
  293.5 8.8 %collective-permute-start.22 = (bf16[64,2048]{1,0:T(8,128)(2,1)S(1)}, bf16[64,2048]{1,0:T(8,128)(2,1)S(1)}, u32[]{:S(2)}, u32[]{:S(2)}) collective-permute-start(bf16[64,2048]{1,0:T(8,128)(2,1)S(1)} %get-tuple-element.43), channel_id=1, source_target_pairs={{0,8},{8,16},{16,24},{24,0},{1,9},{9,17},{17,25},{25,1},{2,10},{10... | collective-permute-start | bytes 786440 | tf_op jit(solution)/shard_map/ppermute | solution.py:488
  293.6 9.6 %collective-permute-start.23 = (bf16[64,2048]{1,0:T(8,128)(2,1)S(1)}, bf16[64,2048]{1,0:T(8,128)(2,1)S(1)}, u32[]{:S(2)}, u32[]{:S(2)}) collective-permute-start(bf16[64,2048]{1,0:T(8,128)(2,1)S(1)} %get-tuple-element.44), channel_id=1, source_target_pairs={{0,24},{8,0},{16,8},{24,16},{1,25},{9,1},{17,9},{25,17},{2,26},{10... | collective-permute-start | bytes 786440 | tf_op jit(solution)/shard_map/ppermute | solution.py:488
  (22 other events, 374.7 us)
